TPU v7x, 32 devices: a whole 2x2x4 slice. The times are simulated.
32 devices in a mesh: ep: 8 (over z, core), tp: 4 (over y, x).
Axes of the slice: x: 2, y: 2, z: 4, core: 2. Of those that a mesh axis runs over, the one named last changes fastest.
Arguments:
- tokens: bfloat16 [128, 2048], P('ep'), may hold values from -6 to 6
- old_state: float32 [128, 16, 128, 128], P('ep', 'tp'), may hold values from -2 to 2
- lower_bound: float32 [2048], P('tp'), may hold values from 0.05 to 0.95
- head_gain: float32 [2048], P('tp'), may hold values from 0.1 to 1.9
- norm_gains: float32 [4, 2048], replicated, may hold values from 0.1 to 1.9
- w_query: bfloat16 [2048, 2048], P('ep', 'tp'), may hold values from -0.125 to 0.125
- w_forget: bfloat16 [2048, 2048], P('ep', 'tp'), may hold values from -0.125 to 0.125
- w_value: bfloat16 [2048, 2048], P('ep', 'tp'), may hold values from -0.125 to 0.125
- w_outgate: bfloat16 [2048, 2048], P('ep', 'tp'), may hold values from -0.125 to 0.125
- w_mix_out: bfloat16 [2048, 2048], P('tp', 'ep'), may hold values from -0.125 to 0.125
- routes: int32 [128, 2], P('ep'), may hold values from 0 to 7, all different within a row; in each aligned block of 16 rows (0 to 15, 16 to 31, ...) at most 8 rows name the same one
- route_scores: float32 [128, 2], P('ep'), may hold values from -6 to 6
- w_exp_gate: bfloat16 [8, 2048, 3584], P('ep', None, 'tp'), may hold values from -0.125 to 0.125
- w_exp_up: bfloat16 [8, 2048, 3584], P('ep', None, 'tp'), may hold values from -0.125 to 0.125
- w_exp_down: bfloat16 [8, 3584, 2048], P('ep', 'tp'), may hold values from -0.75 to 0.75
- w_dense_gate: bfloat16 [2048, 6144], P('ep', 'tp'), may hold values from -0.125 to 0.125
- w_dense_up: bfloat16 [2048, 6144], P('ep', 'tp'), may hold values from -0.125 to 0.125
- w_dense_down: bfloat16 [6144, 2048], P('tp', 'ep'), may hold values from -0.75 to 0.75
- dense_mix: bfloat16 [2048], replicated, may hold values from -0.125 to 0.125
Outputs:
- layer_out: bfloat16 [128, 2048], P('ep', 'tp')
- new_state: float32 [128, 16, 128, 128], P('ep', 'tp')
Inputs may be any that keep to these rules, and one draw needn't show every extreme that they name: `routes`: each row names 2 different experts. In each aligned block of 16 rows no expert is named by more than 8 rows, and in every draw some expert is named by exactly 8 rows of some block.
All inputs are finite; a program needn't handle non-finite values.
Results may differ from a plain program's by a relative error of at most 0.025.
Values may be sent and summed in bfloat16 or wider, within the bound.
No kernel may reach another device: no remote copies, remote signals or barrier semaphores. Data moves between devices by JAX's collectives and lax.ppermute only.
A program may use at most 64 MiB of HBM per device.

v0:
```python
import jax
import jax.numpy as jnp
from jax import lax
from jax.sharding import PartitionSpec as P

EPS = 1e-06


def rms_scale(values):
    return lax.rsqrt(jnp.mean(values * values, axis=-1, keepdims=True) + EPS)


def body(
    tokens,
    old_state,
    lower_bound,
    head_gain,
    norm_gains,
    w_query,
    w_forget,
    w_value,
    w_outgate,
    w_mix_out,
    routes,
    route_scores,
    w_exp_gate,
    w_exp_up,
    w_exp_down,
    w_dense_gate,
    w_dense_up,
    w_dense_down,
    dense_mix,
):
    highest = lax.Precision.HIGHEST
    seqs, width = tokens.shape
    column_index = lax.axis_index("tp")
    part_width = width // lax.axis_size("tp")
    resid = tokens.astype(jnp.float32)
    normed = (resid * rms_scale(resid) * norm_gains[0]).astype(jnp.bfloat16)
    in_weights = jnp.concatenate([w_query, w_forget, w_value, w_outgate], axis=1)
    mix_rows = lax.all_to_all(normed, "ep", split_axis=1, concat_axis=0, tiled=True)
    projected = lax.psum_scatter(
        jnp.dot(mix_rows, in_weights, preferred_element_type=jnp.float32).astype(jnp.bfloat16),
        "ep",
        scatter_dimension=0,
        tiled=True,
    ).astype(jnp.float32)
    query_raw, forget_raw, value, out_gate = jnp.split(projected, 4, axis=1)
    heads = old_state.shape[1]
    head_size = old_state.shape[2]
    shape_heads = (seqs, heads, head_size)
    forget = lower_bound + (1.0 - lower_bound) * jax.nn.sigmoid(forget_raw)
    key_in = (1.0 - lower_bound) * jax.nn.sigmoid(-forget_raw)
    new_state = forget.reshape(shape_heads)[..., None] * old_state + key_in.reshape(shape_heads)[
        ..., None
    ] * value.reshape(seqs, heads, 1, head_size)
    query = jax.nn.silu(query_raw).reshape(shape_heads)
    read = jnp.einsum("thk,thkv->thv", query, new_state, precision=highest)
    gated = (
        read
        * rms_scale(read)
        * head_gain.reshape(heads, head_size)
        * jax.nn.silu(out_gate).reshape(shape_heads)
    )
    mixed_heads = gated.reshape(seqs, heads * head_size).astype(jnp.bfloat16)
    mix_part = jnp.dot(
        mixed_heads,
        lax.all_gather(w_mix_out, "ep", axis=1, tiled=True),
        preferred_element_type=jnp.float32,
    ).astype(jnp.bfloat16)
    mix_part = lax.optimization_barrier(mix_part).astype(jnp.float32)
    mix_out = lax.psum(mix_part.astype(jnp.bfloat16), "tp")
    mix_wide = lax.optimization_barrier(mix_out).astype(jnp.float32)
    after_mix = resid + mix_wide * rms_scale(mix_wide) * norm_gains[1]
    ffn_in = (after_mix * rms_scale(after_mix) * norm_gains[2]).astype(jnp.bfloat16)
    experts = lax.axis_size("ep")
    topk = routes.shape[1]
    capacity = max(2, 2 * seqs * topk // experts)
    flat_routes = routes.reshape(-1)
    onehot = (flat_routes[:, None] == jnp.arange(experts, dtype=jnp.int32)[None, :]).astype(
        jnp.int32
    )
    before = jnp.cumsum(onehot, axis=0) - onehot
    slots = jnp.sum(onehot * before, axis=1)
    cells = flat_routes * capacity + slots
    placed = cells[None, :] == jnp.arange(experts * capacity, dtype=jnp.int32)[:, None]
    repeated = jnp.repeat(ffn_in, topk, axis=0)
    outgoing = jnp.dot(placed.astype(jnp.bfloat16), repeated, preferred_element_type=jnp.float32)
    outgoing = outgoing.astype(jnp.bfloat16).reshape(experts, capacity, width)
    arrived = lax.all_to_all(outgoing, "ep", split_axis=0, concat_axis=0, tiled=True)
    sources, items, _ = arrived.shape
    expert_rows = arrived.reshape(sources * items, width)
    gate_pre = jnp.dot(expert_rows, w_exp_gate[0], preferred_element_type=jnp.float32)
    up_pre = jnp.dot(expert_rows, w_exp_up[0], preferred_element_type=jnp.float32)
    hidden = (jax.nn.silu(gate_pre) * up_pre).astype(jnp.bfloat16)
    partial_rows = jnp.dot(hidden, w_exp_down[0], preferred_element_type=jnp.float32).astype(
        jnp.bfloat16
    )
    partial_rows = lax.optimization_barrier(partial_rows).astype(jnp.float32)
    partial_rows = partial_rows.reshape(sources, items, width)
    summed = lax.psum_scatter(
        partial_rows.astype(jnp.bfloat16), "tp", scatter_dimension=2, tiled=True
    )
    returned = lax.all_to_all(summed, "ep", split_axis=0, concat_axis=0, tiled=True)
    first = jax.nn.sigmoid(route_scores[:, 0] - route_scores[:, 1])
    second = jax.nn.sigmoid(route_scores[:, 1] - route_scores[:, 0])
    route_weight = jnp.stack([first, second], axis=1).reshape(-1)
    weight_table = jnp.sum(
        (placed.astype(jnp.float32) * route_weight[None, :]).reshape(
            experts * capacity, seqs, topk
        ),
        axis=2,
    )
    expert_sum = jnp.dot(
        weight_table.T,
        returned.reshape(experts * capacity, part_width).astype(jnp.float32),
        precision=highest,
    )
    dense_weights = jnp.concatenate([w_dense_gate, w_dense_up], axis=1)
    dense_rows = lax.all_to_all(ffn_in, "ep", split_axis=1, concat_axis=0, tiled=True)
    dense_pre = lax.psum_scatter(
        jnp.dot(dense_rows, dense_weights, preferred_element_type=jnp.float32).astype(jnp.bfloat16),
        "ep",
        scatter_dimension=0,
        tiled=True,
    ).astype(jnp.float32)
    dense_gate_pre, dense_up_pre = jnp.split(dense_pre, 2, axis=1)
    dense_hidden = (jax.nn.silu(dense_gate_pre) * dense_up_pre).astype(jnp.bfloat16)
    dense_partial = jnp.dot(
        dense_hidden,
        lax.all_gather(w_dense_down, "ep", axis=1, tiled=True),
        preferred_element_type=jnp.float32,
    )
    dense_out = lax.psum_scatter(
        dense_partial.astype(jnp.bfloat16), "tp", scatter_dimension=1, tiled=True
    ).astype(jnp.float32)
    mix_weight = jax.nn.sigmoid(jnp.dot(ffn_in, dense_mix, preferred_element_type=jnp.float32))
    ffn_out = expert_sum + mix_weight[:, None] * dense_out
    squares = lax.psum(jnp.sum(ffn_out * ffn_out, axis=1), "tp")
    out_scale = lax.rsqrt(squares / width + EPS)
    gain_part = lax.dynamic_slice_in_dim(norm_gains[3], column_index * part_width, part_width, 0)
    resid_part = lax.dynamic_slice_in_dim(after_mix, column_index * part_width, part_width, 1)
    layer_out = (resid_part + ffn_out * out_scale[:, None] * gain_part).astype(jnp.bfloat16)
    return (layer_out, new_state)


def solution(mesh):
    return jax.shard_map(
        body,
        mesh=mesh,
        in_specs=(
            P("ep", None),
            P("ep", "tp", None, None),
            P("tp"),
            P("tp"),
            P(),
            P("ep", "tp"),
            P("ep", "tp"),
            P("ep", "tp"),
            P("ep", "tp"),
            P("tp", "ep"),
            P("ep", None),
            P("ep", None),
            P("ep", None, "tp"),
            P("ep", None, "tp"),
            P("ep", "tp", None),
            P("ep", "tp"),
            P("ep", "tp"),
            P("tp", "ep"),
            P(),
        ),
        out_specs=(P("ep", "tp"), P("ep", "tp", None, None)),
        check_vma=False,
    )
```

profile of v0, /device:TPU:0, one launch (start us, length us, event | category | flops | bytes accessed | tf_op | source)
XLA Modules:
  0.0 319.4 jit_solution(3477213161517081613)
XLA Ops:
  7.2 0.0 reduce-scatter.5.cloned.1.call-start
  7.2 0.9 fusion.58
  8.2 1.0 fusion.42
  9.2 0.9 fusion.44
  10.1 12.1 %all_to_all.48 = bf16[16,8,256]{2,0,1:T(8,128)(2,1)S(1)} all-to-all(bf16[16,8,256]{2,0,1:T(8,128)(2,1)S(1)} %bitcast.82), channel_id=1, replica_groups=mesh['ep'=8,'tp'=4] {'ep'}, dimensions={1} | all-to-all | bytes 131072 | tf_op jit(solution)/shard_map/all_to_all | solution.py:41
  22.2 2.3 convolution_convert_fusion.1
  24.5 0.0 reduce-scatter.5.cloned.1.call-update
  24.5 0.0 all-gather.3.cloned.1.call-start
  24.5 0.7 all-gather.3.cloned.1.call-update
  25.2 0.0 all-reduce.2.cloned.1.call-start
  25.3 0.1 copy.38
  25.4 0.1 eq.35
  25.5 0.1 fusion.53
  25.5 0.1 reduce_window_sum.11
  25.6 0.2 select_reduce_fusion.1
  25.8 28.7 %reduce-scatter.5.cloned.1.call-done = bf16[16,2048]{1,0:T(8,128)(2,1)} async-done(((bf16[128,2048]{1,0:T(8,128)(2,1)}), bf16[16,2048]{1,0:T(8,128)(2,1)}) %reduce-scatter.5.cloned.1.call-update) | async-done | bytes 65552 | tf_op jit(solution)/shard_map/reduce_scatter | solution.py:42
  54.5 0.8 convert_element_type.70
  55.4 0.7 split.26
  56.2 4.4 %multiply_add_fusion = f32[16,4,128,128]{3,2,1,0:T(8,128)S(1)} fusion(f32[16,4,128,128]{3,2,1,0:T(8,128)} %param.20, f32[16,4,128]{2,1,0:T(4,128)S(1)} %mul.223, f32[16,4,128]{2,1,0:T(4,128)S(1)} %mul.221, f32[16,4,128]{2,1,0:T(4,128)S(1)} %mul.217), kind=kLoop, calls=%fused_computation | loop fusion | flops 3145728 | bytes 8486912 | tf_op jit(solution)/shard_map/add | solution.py:54
  60.6 0.0 copy-start
  60.6 0.0 copy-start.5
  60.6 0.0 copy-start.1
  60.7 2.0 copy-done
  62.6 3.7 %fusion.59 = f32[16,4,1,128]{3,2,1,0:T(1,128)S(1)} fusion(f32[16,4,128,1]{2,3,1,0:T(1,128)S(1)} %bitcast.84, f32[16,4,128,128]{3,2,1,0:T(8,128)S(1)} %multiply_add_fusion), kind=kOutput, calls=%fused_computation.92 | convolution fusion | flops 12582912 | bytes 4259840 | tf_op jit(solution)/shard_map/thk,thkv->thv/dot_general | solution.py:58
  66.3 0.1 multiply_reduce_fusion.2
  66.4 0.1 multiply_convert_fusion.1
  66.5 18.5 %all-gather.3.cloned.1.call-done = bf16[512,2048]{1,0:T(8,128)(2,1)} async-done(((bf16[512,256]{1,0:T(8,128)(2,1)}), bf16[512,2048]{1,0:T(8,128)(2,1)}) %all-gather.3.cloned.1.call-update) | async-done | bytes 2097168 | tf_op jit(solution)/shard_map/all_gather | solution.py:68
  85.0 2.6 convolution_convert_fusion.4
  87.6 0.0 all-reduce.2.cloned.1.call-update
  87.6 0.0 reduce-scatter.7.cloned.1.call-start
  87.7 41.1 %all-reduce.2.cloned.1.call-done = bf16[16,2048]{1,0:T(8,128)(2,1)} async-done(((bf16[16,2048]{1,0:T(8,128)(2,1)}), bf16[16,2048]{1,0:T(8,128)(2,1)}) %all-reduce.2.cloned.1.call-update) | async-done | bytes 65552 | tf_op jit(solution)/shard_map/psum | solution.py:72
  128.8 1.0 fusion.40
  129.7 1.0 multiply_reduce_fusion
  130.8 0.1 multiply_convert_fusion
  130.9 0.1 broadcast_in_dim.2
  131.0 0.1 reshape.103
  131.0 0.2 fusion.9
  131.2 14.1 %all_to_all.49 = bf16[8,8,2048]{2,1,0:T(8,128)(2,1)S(1)} all-to-all(bf16[8,8,2048]{2,1,0:T(8,128)(2,1)S(1)} %fusion.9), channel_id=1, replica_groups=mesh['ep'=8,'tp'=4] {'ep'}, dimensions={0} | all-to-all | bytes 524288 | tf_op jit(solution)/shard_map/all_to_all | solution.py:90
  145.4 2.7 fusion.4
  148.1 0.0 copy-start.8
  148.1 5.5 %fusion.6 = bf16[64,2048]{1,0:T(8,128)(2,1)} fusion(bf16[1,896,2048]{2,1,0:T(8,128)(2,1)} %param.33, bf16[1,2048,896]{2,1,0:T(8,128)(2,1)} %param.32, bf16[8,8,2048]{2,1,0:T(8,128)(2,1)S(1)} %all_to_all.49, f32[64,896]{1,0:T(8,128)S(1)} %fusion.4), kind=kOutput, calls=%fused_computation.9 | convolution fusion | flops 470237184 | bytes 8093696 | tf_op jit(solution)/shard_map/dot_general | solution.py:96
  153.6 0.0 reduce-scatter.7.cloned.1.call-update
  153.7 0.0 reduce-scatter.9.cloned.1.call-start
  153.7 8.3 %all_to_all.50 = bf16[16,8,256]{2,0,1:T(8,128)(2,1)S(1)} all-to-all(bf16[16,8,256]{2,0,1:T(8,128)(2,1)S(1)} %bitcast.83), channel_id=1, replica_groups=mesh['ep'=8,'tp'=4] {'ep'}, dimensions={1} | all-to-all | bytes 131072 | tf_op jit(solution)/shard_map/all_to_all | solution.py:120
  162.0 1.3 convolution_convert_fusion
  163.3 0.0 reduce-scatter.9.cloned.1.call-update
  163.3 0.0 all-gather.5.cloned.1.call-start
  163.4 0.5 all-gather.5.cloned.1.call-update
  163.9 0.1 reduce_sum.69
  164.0 0.1 copy.39
  164.2 0.1 select_reduce_fusion
  164.2 11.9 %reduce-scatter.7.cloned.1.call-done = bf16[8,8,512]{2,1,0:T(8,128)(2,1)} async-done(((bf16[8,8,2048]{2,1,0:T(8,128)(2,1)}), bf16[8,8,512]{2,1,0:T(8,128)(2,1)}) %reduce-scatter.7.cloned.1.call-update) | async-done | bytes 65552 | tf_op jit(solution)/shard_map/reduce_scatter | solution.py:101
  176.1 4.6 %all-to-all-start.2 = ((bf16[8,8,512]{2,1,0:T(8,128)(2,1)}), bf16[8,8,512]{2,1,0:T(8,128)(2,1)S(1)}, u32[]{:S(2)}, u32[]{:S(2)}) async-start(bf16[8,8,512]{2,1,0:T(8,128)(2,1)} %reduce-scatter.7.cloned.1.call-done), calls=%async_computation.4 | async-start | bytes 131072 | tf_op jit(solution)/shard_map/all_to_all | solution.py:104
  180.7 0.0 reduce-scatter.11.cloned.1.call-start
  180.8 29.5 %reduce-scatter.9.cloned.1.call-done = bf16[16,3072]{1,0:T(8,128)(2,1)} async-done(((bf16[128,3072]{1,0:T(8,128)(2,1)}), bf16[16,3072]{1,0:T(8,128)(2,1)}) %reduce-scatter.9.cloned.1.call-update) | async-done | bytes 98320 | tf_op jit(solution)/shard_map/reduce_scatter | solution.py:121
  210.3 0.9 convert_element_type.82
  211.2 63.9 %all-gather.5.cloned.1.call-done = bf16[1536,2048]{1,0:T(8,128)(2,1)} async-done(((bf16[1536,256]{1,0:T(8,128)(2,1)}), bf16[1536,2048]{1,0:T(8,128)(2,1)}) %all-gather.5.cloned.1.call-update) | async-done | bytes 6291472 | tf_op jit(solution)/shard_map/all_gather | solution.py:131
  275.1 4.3 %convolution_convert_fusion.3 = bf16[16,2048]{1,0:T(8,128)(2,1)} fusion(bf16[1536,2048]{1,0:T(8,128)(2,1)} %all-gather.5.cloned.1.call-done, f32[16,3072]{1,0:T(8,128)S(1)} %convert_element_type.82), kind=kOutput, calls=%fused_computation.12 | convolution fusion | flops 100843520 | bytes 6553600 | tf_op jit(solution)/shard_map/dot_general | solution.py:129
  279.5 0.0 reduce-scatter.11.cloned.1.call-update
  279.5 0.1 fusion.22
  279.6 22.3 %reduce-scatter.11.cloned.1.call-done = bf16[16,512]{1,0:T(8,128)(2,1)} async-done(((bf16[16,2048]{1,0:T(8,128)(2,1)}), bf16[16,512]{1,0:T(8,128)(2,1)}) %reduce-scatter.11.cloned.1.call-update) | async-done | bytes 16400 | tf_op jit(solution)/shard_map/reduce_scatter | solution.py:134
  301.9 1.0 multiply_reduce_fusion.1
  302.9 8.9 %psum.15 = f32[16]{0:T(128)S(1)} all-reduce(f32[16]{0:T(128)S(1)} %get-tuple-element.14), channel_id=1, replica_groups=mesh['ep'=8,'tp'=4] {'tp'}, use_global_device_ids=true, to_apply=%region_13.14 | all-reduce | flops 16 | bytes 128 | tf_op jit(solution)/shard_map/psum | solution.py:139
  311.8 0.7 add_convert_fusion
  (34 shorter events, 0.3 us)
Async XLA Ops:
  7.2 18.1 %copy-start.4 = (s32[16,2]{0,1:T(2,128)S(1)}, s32[16,2]{0,1:T(2,128)}, u32[]{:S(2)}) copy-start(s32[16,2]{0,1:T(2,128)} %param.29) | copy-start | bytes 388
  7.2 18.6 %copy-start.2 = (f32[512]{0:T(512)S(1)}, f32[512]{0:T(512)}, u32[]{:S(2)}) copy-start(f32[512]{0:T(512)} %param.21) | copy-start | bytes 6148
  7.2 47.3 %reduce-scatter.5.cloned.1.call-start = ((), (), s32[]{:S(2)}) async-start(), calls=%async_computation.8 | async-start | bytes 589824 | tf_op jit(solution)/shard_map/reduce_scatter | solution.py:42
  24.5 60.5 %all-gather.3.cloned.1.call-start = ((), (), s32[]{:S(2)}) async-start(), calls=%async_computation.9 | async-start | bytes 2359296 | tf_op jit(solution)/shard_map/all_gather | solution.py:68
  25.2 103.5 %all-reduce.2.cloned.1.call-start = ((), (), s32[]{:S(2)}) async-start(), calls=%async_computation.10 | async-start | bytes 131072 | tf_op jit(solution)/shard_map/psum | solution.py:72
  60.6 2.0 copy-start
  60.6 5.8 %copy-start.5 = (f32[512]{0:T(512)S(1)}, f32[512]{0:T(512)}, u32[]{:S(2)}) copy-start(f32[512]{0:T(512)} %param.22) | copy-start | bytes 6148
  60.6 69.1 %copy-start.1 = (bf16[16,2048]{1,0:T(8,128)(2,1)S(1)}, bf16[16,2048]{1,0:T(8,128)(2,1)}, u32[]{:S(2)}) copy-start(bf16[16,2048]{1,0:T(8,128)(2,1)} %param.19) | copy-start | bytes 196612
  87.6 88.5 %reduce-scatter.7.cloned.1.call-start = ((), (), s32[]{:S(2)}) async-start(), calls=%async_computation.11 | async-start | bytes 327680 | tf_op jit(solution)/shard_map/reduce_scatter | solution.py:101
  148.1 13.9 %copy-start.7 = (bf16[256,1536]{1,0:T(8,128)(2,1)S(1)}, bf16[256,1536]{1,0:T(8,128)(2,1)}, u32[]{:S(2)}) copy-start(bf16[256,1536]{1,0:T(8,128)(2,1)} %param.35) | copy-start | bytes 2359300
  148.1 13.9 %copy-start.8 = (bf16[256,1536]{1,0:T(8,128)(2,1)S(1)}, bf16[256,1536]{1,0:T(8,128)(2,1)}, u32[]{:S(2)}) copy-start(bf16[256,1536]{1,0:T(8,128)(2,1)} %param.34) | copy-start | bytes 2359300
  153.6 10.3 %copy-start.3 = (bf16[2048]{0:T(1024)(128)(2,1)S(1)}, bf16[2048]{0:T(1024)(128)(2,1)}, u32[]{:S(2)}) copy-start(bf16[2048]{0:T(1024)(128)(2,1)} %param.37) | copy-start | bytes 12292
  153.6 10.5 %copy-start.6 = (f32[16,2]{0,1:T(2,128)S(1)}, f32[16,2]{0,1:T(2,128)}, u32[]{:S(2)}) copy-start(f32[16,2]{0,1:T(2,128)} %param.30) | copy-start | bytes 388
  153.7 56.6 %reduce-scatter.9.cloned.1.call-start = ((), (), s32[]{:S(2)}) async-start(), calls=%async_computation.12 | async-start | bytes 884736 | tf_op jit(solution)/shard_map/reduce_scatter | solution.py:121
  163.3 111.8 %all-gather.5.cloned.1.call-start = ((), (), s32[]{:S(2)}) async-start(), calls=%async_computation.13 | async-start | bytes 7077888 | tf_op jit(solution)/shard_map/all_gather | solution.py:131
  176.1 103.5 %all-to-all-start.2 = ((bf16[8,8,512]{2,1,0:T(8,128)(2,1)}), bf16[8,8,512]{2,1,0:T(8,128)(2,1)S(1)}, u32[]{:S(2)}, u32[]{:S(2)}) async-start(bf16[8,8,512]{2,1,0:T(8,128)(2,1)} %reduce-scatter.7.cloned.1.call-done), calls=%async_computation.4 | async-start | bytes 131072 | tf_op jit(solution)/shard_map/all_to_all | solution.py:104
  180.7 121.2 %reduce-scatter.11.cloned.1.call-start = ((), (), s32[]{:S(2)}) async-start(), calls=%async_computation.14 | async-start | bytes 81920 | tf_op jit(solution)/shard_map/reduce_scatter | solution.py:134
Sparse Core Ops, SparseCore 0:
  24.6 29.8 reduce-scatter.4
  56.1 28.8 all-gather.2
  87.9 40.8 all-reduce.1
  153.8 22.2 reduce-scatter.6
  178.2 31.9 reduce-scatter.8
  211.7 63.3 all-gather.4
  279.6 22.2 reduce-scatter.10
where the time goes:
time: 320 us; the launch traced here: 319 us
  waiting for transfers between devices  217 us (68%)
  blocking collectives  43.4 us (14%)
  matrix products  23.7 us (7%)
  between operations  14.4 us (4%)
  other arithmetic  11.5 us (4%)
  starting transfers between devices  4.89 us (2%)
  local copies, waits for them, and re-layouts  4.25 us (1%)
    all_gather x1, waiting for transfers between devices, body(): lax.all_gather(w_dense_down, 'ep', axis=1, tiled=True)  63.9 us
    psum x1, waiting for transfers between devices, body(): mix_out = lax.psum(mix_part.astype(jnp.bfloat16), 'tp')  41.1 us
    reduce_scatter x1, waiting for transfers between devices, body(): lax.psum_scatter(jnp.dot(dense_rows, dense_weights, preferred_element_typ...  29.5 us
    reduce_scatter x1, waiting for transfers between devices, body(): lax.psum_scatter(jnp.dot(mix_rows, in_weights, preferred_element_type=jnp...  28.7 us
    reduce_scatter x1, waiting for transfers between devices, body(): lax.psum_scatter(dense_partial.astype(jnp.bfloat16), 'tp', scatter_dimens...  22.3 us
    all_gather x1, waiting for transfers between devices, body(): lax.all_gather(w_mix_out, 'ep', axis=1, tiled=True)  18.5 us
    all_to_all x1, blocking collectives, body(): lax.all_to_all(outgoing, 'ep', split_axis=0, concat_axis=0, tiled=True)  14.1 us
    all_to_all x1, blocking collectives, body(): lax.all_to_all(normed, 'ep', split_axis=1, concat_axis=0, tiled=True)  12.1 us
  transfers between devices with their start and end apart: 8, of which 7 were waited for; matrix products, arithmetic and copies ran while one was open for 5% of the time, Pallas kernels for 0%

commit v1 on v0

v1 whole, which is shorter than its diff:
```python
import jax
import jax.numpy as jnp
from jax import lax
from jax.experimental import pallas as pl
from jax.experimental.pallas import tpu as pltpu
from jax.sharding import PartitionSpec as P


EPS = 1e-06
F32 = jnp.float32
BF16 = jnp.bfloat16


def rms_scale(values):
    return lax.rsqrt(jnp.mean(values * values, axis=-1, keepdims=True) + EPS)


def swap(value, axis, step):
    size = lax.axis_size(axis)
    return lax.ppermute(value, axis, [(i, i ^ step) for i in range(size)])


def chip_steps():
    return range(2, lax.axis_size("ep"), 2)


def relative_exchange(even, odd):
    crossed = swap(odd, "ep", 1)
    pairs = jnp.stack([even, crossed], axis=1)
    return [pairs[0]] + [swap(pairs[s // 2], "ep", s) for s in chip_steps()]


def chip_gather(block):
    return [block] + [swap(block, "ep", s) for s in chip_steps()]


def relative_gather(block):
    even = chip_gather(block)
    odd = [swap(item, "ep", 1) for item in even]
    return jnp.stack([item for pair in zip(even, odd) for item in pair])


def chip_send(parts):
    return [swap(part, "ep", s) for part, s in zip(parts, chip_steps())]


def total_of(own, arrived):
    for part in arrived:
        own = own + part.astype(F32)
    return own


def tp_exchange(value):
    return [swap(value, "tp", s) for s in range(1, lax.axis_size("tp"))]


def background_gather(block):
    blocks = [block]
    step = 2
    while step < lax.axis_size("ep"):
        fresh = [swap(block, "ep", step)]
        lower = 2
        while lower < step:
            fresh = fresh + [swap(item, "ep", lower) for item in fresh]
            lower *= 2
        blocks = blocks + fresh
        step *= 2
    odd = [swap(item, "ep", 1) for item in blocks]
    return [item for pair in zip(blocks, odd) for item in pair]


VMEM = pl.BlockSpec(memory_space=pltpu.VMEM)
PARAMS = pltpu.CompilerParams(vmem_limit_bytes=16 << 20)


def call(kernel, out_shape, flops=1 << 20):
    estimate = pl.CostEstimate(flops=flops, bytes_accessed=1 << 20, transcendentals=0)
    return pl.pallas_call(
        kernel, out_shape=out_shape, compiler_params=PARAMS, cost_estimate=estimate
    )


def front_kernel(tokens_ref, gains_ref, even_ref, odd_ref):
    resid = tokens_ref[...].astype(F32)
    chips, _, feats = even_ref.shape
    scale = rms_scale(resid)
    mine = lax.axis_index("ep")
    for j in range(2 * chips):
        cols = pl.ds(pl.multiple_of((mine ^ j) * feats, feats), feats)
        piece = tokens_ref[:, cols].astype(F32) * scale * gains_ref[0:1, cols]
        (odd_ref if j % 2 else even_ref)[j // 2] = piece.astype(BF16)


def front(tokens, norm_gains, ep_size):
    seqs, width = tokens.shape
    feats = width // ep_size
    if feats % 128:
        resid = tokens.astype(F32)
        normed = (resid * rms_scale(resid) * norm_gains[0]).astype(BF16)
        pieces = [
            lax.dynamic_slice_in_dim(normed, (lax.axis_index("ep") ^ j) * feats, feats, 1)
            for j in range(ep_size)
        ]
        return jnp.stack(pieces[::2]), jnp.stack(pieces[1::2])
    shape = jax.ShapeDtypeStruct((ep_size // 2, seqs, width // ep_size), BF16)
    return call(front_kernel, (shape, shape))(tokens, norm_gains)


def project_kernel(pairs, *refs):
    rows_refs, weights = refs[:pairs], refs[pairs:-2]
    keep_ref, send_ref = refs[-2:]
    _, seqs, _ = keep_ref.shape
    feats = weights[0].shape[0]
    rows = jnp.concatenate([ref[...].reshape(2 * seqs, feats) for ref in rows_refs], axis=0)
    start = 0
    for w in weights:
        cols = slice(start, start + w.shape[1])
        part = jnp.dot(rows, w[...], preferred_element_type=F32)
        for s in range(pairs):
            base = 2 * s * seqs
            keep_ref[s, :, cols] = part[base : base + seqs]
            send_ref[s, :, cols] = part[base + seqs : base + 2 * seqs].astype(BF16)
        start = cols.stop


def project(row_pairs, weights):
    chips = len(row_pairs)
    shape = (chips, row_pairs[0].shape[1], sum(w.shape[1] for w in weights))
    return call(
        lambda *refs: project_kernel(chips, *refs),
        (jax.ShapeDtypeStruct(shape, F32), jax.ShapeDtypeStruct(shape, BF16)),
    )(*row_pairs, *weights)


def chip_sum_kernel(keep_ref, crossed_ref, own_ref, *send_refs):
    own_ref[...] = keep_ref[0] + crossed_ref[0].astype(F32)
    for s, ref in enumerate(send_refs):
        ref[...] = (keep_ref[s + 1] + crossed_ref[s + 1].astype(F32)).astype(BF16)


def chip_sum(keep, crossed):
    chips, seqs, width = keep.shape
    sent = jax.ShapeDtypeStruct((seqs, width), BF16)
    out = (jax.ShapeDtypeStruct((seqs, width), F32),) + (sent,) * (chips - 1)
    own, *sends = call(chip_sum_kernel, out)(keep, crossed)
    return own, sends


def mix_kernel(heads_ref, *refs):
    *weights, out_ref = refs
    value = heads_ref[...]
    for j, w in enumerate(weights):
        width = w.shape[1]
        part = jnp.dot(value, w[...], preferred_element_type=F32)
        out_ref[:, j * width : (j + 1) * width] = part.astype(BF16)


def mix_heads(mixed_heads, weights):
    shape = (mixed_heads.shape[0], weights[0].shape[1] * len(weights))
    return call(mix_kernel, jax.ShapeDtypeStruct(shape, BF16))(mixed_heads, *weights)


def middle_kernel(parts, tokens_ref, gains_ref, gate_ref, routes_ref, scores_ref, *refs):
    pieces, (after_ref, packed_ref) = refs[:parts], refs[parts:]
    seqs, width = tokens_ref.shape
    ep_size = lax.axis_size("ep")
    feats = width // ep_size
    mine = lax.axis_index("ep")
    for j in range(ep_size):
        total = pieces[0][:, j * feats : (j + 1) * feats].astype(F32)
        for piece in pieces[1:]:
            total = total + piece[:, j * feats : (j + 1) * feats].astype(F32)
        cols = pl.ds(pl.multiple_of((mine ^ j) * feats, feats), feats)
        after_ref[:, cols] = total.astype(BF16).astype(F32)
    mix_wide = after_ref[...]
    after_mix = tokens_ref[...].astype(F32) + mix_wide * rms_scale(mix_wide) * gains_ref[1:2]
    after_ref[...] = after_mix
    ffn_in = (after_mix * rms_scale(after_mix) * gains_ref[2:3]).astype(BF16)
    packed_ref[:, :width] = ffn_in
    dots = jnp.sum(ffn_in.astype(F32) * gate_ref[...].astype(F32), axis=1, keepdims=True)
    lanes = (packed_ref.shape[1] - width) // 2
    place = lax.broadcasted_iota(jnp.int32, (seqs, lanes), 1)
    extra = jnp.where(place == ep_size, jax.nn.sigmoid(dots), 0.0)
    for k in range(2):
        margin = scores_ref[:, k : k + 1] - scores_ref[:, 1 - k : 2 - k]
        extra = jnp.where(place == routes_ref[:, k : k + 1], jax.nn.sigmoid(margin), extra)
    high = extra.astype(BF16)
    packed_ref[:, width : width + lanes] = high
    packed_ref[:, width + lanes :] = (extra - high.astype(F32)).astype(BF16)


def to_absolute(values, index, ep_size):
    rows, width = values.shape
    values = values.reshape(rows, ep_size, width // ep_size)
    order = index ^ jnp.arange(ep_size, dtype=jnp.int32)
    return jnp.take(values, order, axis=1).reshape(rows, width)


def plain_middle(tokens, norm_gains, dense_mix, routes, route_scores, lanes, pieces):
    ep_size = lax.axis_size("ep")
    total = total_of(pieces[0].astype(F32), pieces[1:])
    mix_wide = to_absolute(total.astype(BF16).astype(F32), lax.axis_index("ep"), ep_size)
    after_mix = tokens.astype(F32) + mix_wide * rms_scale(mix_wide) * norm_gains[1]
    ffn_in = (after_mix * rms_scale(after_mix) * norm_gains[2]).astype(BF16)
    dots = jnp.sum(ffn_in.astype(F32) * dense_mix.astype(F32), axis=1, keepdims=True)
    place = jnp.arange(lanes, dtype=jnp.int32)[None]
    extra = jnp.where(place == ep_size, jax.nn.sigmoid(dots), 0.0)
    for k in range(2):
        margin = route_scores[:, k : k + 1] - route_scores[:, 1 - k : 2 - k]
        extra = jnp.where(place == routes[:, k : k + 1], jax.nn.sigmoid(margin), extra)
    high = extra.astype(BF16)
    low = (extra - high.astype(F32)).astype(BF16)
    return after_mix, jnp.concatenate([ffn_in, high, low], axis=1)


def middle(tokens, norm_gains, dense_mix, routes, route_scores, lanes, pieces):
    seqs, width = tokens.shape
    if (width // lax.axis_size("ep")) % 128:
        return plain_middle(tokens, norm_gains, dense_mix, routes, route_scores, lanes, pieces)
    return call(
        lambda *refs: middle_kernel(len(pieces), *refs),
        (
            jax.ShapeDtypeStruct((seqs, width), F32),
            jax.ShapeDtypeStruct((seqs, width + 2 * lanes), BF16),
        ),
    )(tokens, norm_gains, dense_mix, routes, route_scores, *pieces)


def join_kernel(chips, expert_ref, scale_ref, own_ref, other_ref, *refs):
    hidden, (keep_ref, send_ref) = refs[:chips], refs[chips:]
    _, seqs, _ = keep_ref.shape
    feats = own_ref.shape[1]
    mine = lax.axis_index("ep")
    for s in range(chips):
        rows = 2 * seqs * s
        keep_ref[s] = expert_ref[rows : rows + seqs]
    everything = jnp.concatenate([ref[...] for ref in hidden], axis=0)
    scale = scale_ref[...]
    placed = []
    for weights, column in ((own_ref, mine), (other_ref, mine ^ 1)):
        dense = jnp.dot(everything, weights[...], preferred_element_type=F32) * scale
        cols = pl.ds(pl.multiple_of(column * feats, feats), feats)
        placed.append((cols, dense))
        for s in range(chips):
            rows = 2 * seqs * s
            keep_ref[s, :, cols] += dense[rows : rows + seqs]
    for s in range(chips):
        rows = 2 * seqs * s + seqs
        send_ref[s] = expert_ref[rows : rows + seqs].astype(BF16)
        for cols, dense in placed:
            value = expert_ref[rows : rows + seqs, cols] + dense[rows : rows + seqs]
            send_ref[s, :, cols] = value.astype(BF16)


def plain_join(expert_out, scale, down_own, down_other, hidden, seqs):
    ep_size = lax.axis_size("ep")
    mine = lax.axis_index("ep")
    everything = jnp.concatenate(hidden, axis=0)
    rows, width = expert_out.shape
    total = expert_out.reshape(rows, ep_size, width // ep_size)
    column = jnp.arange(ep_size, dtype=jnp.int32)[None, :, None]
    for weights, place in ((down_own, mine), (down_other, mine ^ 1)):
        dense = jnp.dot(everything, weights, preferred_element_type=F32) * scale
        total = total + jnp.where(column == place, dense[:, None, :], 0.0)
    total = total.reshape(len(hidden), 2, seqs, width)
    return total[:, 0], total[:, 1].astype(BF16)


def join(expert_out, scale, down_own, down_other, hidden, seqs):
    chips, width = len(hidden), expert_out.shape[1]
    shape = (chips, seqs, width)
    if down_own.shape[1] % 128:
        return plain_join(expert_out, scale, down_own, down_other, hidden, seqs)
    return call(
        lambda *refs: join_kernel(chips, *refs),
        (jax.ShapeDtypeStruct(shape, F32), jax.ShapeDtypeStruct(shape, BF16)),
    )(expert_out, scale, down_own, down_other, *hidden)


def finish_kernel(parts, after_ref, gains_ref, *refs):
    pieces, out_ref = refs[:parts], refs[parts]
    total = pieces[0][...].astype(F32)
    for piece in pieces[1:]:
        total = total + piece[...].astype(F32)
    scale = rms_scale(total)
    width = out_ref.shape[1]
    cols = pl.ds(pl.multiple_of(lax.axis_index("tp") * width, width), width)
    mine = pieces[0][:, cols].astype(F32)
    for piece in pieces[1:]:
        mine = mine + piece[:, cols].astype(F32)
    out_ref[...] = (after_ref[:, cols] + mine * scale * gains_ref[3:4, cols]).astype(BF16)


def finish(after_mix, norm_gains, pieces):
    seqs, width = after_mix.shape
    return call(
        lambda *refs: finish_kernel(len(pieces), *refs),
        jax.ShapeDtypeStruct((seqs, width // lax.axis_size("tp")), BF16),
    )(after_mix, norm_gains, *pieces)


def broadcast_column(columns, index, size):
    return jnp.broadcast_to(columns[:, index : index + 1], (size, size))


def read_kernel(arrived, *refs):
    own_ref, recv = refs[0], refs[1 : 1 + arrived]
    bound_ref, gain_ref, state_ref, mixed_ref, gates_ref = refs[1 + arrived :]
    seqs, heads, size, _ = state_ref.shape
    local = heads * size

    def column(kind, head):
        cols = slice(kind * local + head * size, kind * local + (head + 1) * size)
        value = own_ref[:, cols]
        for ref in recv:
            value = value + ref[:, cols].astype(F32)
        return value

    for head in range(heads):
        query_raw, forget_raw, value, out_gate = (column(kind, head) for kind in range(4))
        span = slice(head * size, (head + 1) * size)
        bound = bound_ref[:, span]
        forget = bound + (1.0 - bound) * jax.nn.sigmoid(forget_raw)
        key_in = (1.0 - bound) * jax.nn.sigmoid(-forget_raw)
        query = query_raw * jax.nn.sigmoid(query_raw)
        gates_ref[0, :, span] = forget
        gates_ref[1, :, span] = key_in
        gates_ref[2, :, span] = value
        weight = (query * forget).T
        rows = [
            jnp.sum(
                broadcast_column(weight, t, size) * state_ref[t, head], axis=0, keepdims=True
            )
            for t in range(seqs)
        ]
        read = jnp.concatenate(rows, axis=0)
        read = read + jnp.sum(query * key_in, axis=1, keepdims=True) * value
        gated = read * rms_scale(read) * gain_ref[:, span]
        mixed_ref[:, span] = (gated * (out_gate * jax.nn.sigmoid(out_gate))).astype(BF16)


def read_heads(own, arrived, lower_bound, head_gain, old_state):
    seqs, heads, size, _ = old_state.shape
    return call(
        lambda *refs: read_kernel(len(arrived), *refs),
        (
            jax.ShapeDtypeStruct((seqs, heads * size), BF16),
            jax.ShapeDtypeStruct((3, seqs, heads * size), F32),
        ),
    )(own, *arrived, lower_bound[None], head_gain[None], old_state)


def state_kernel(gates_ref, state_ref, *refs):
    out_ref = refs[-1]
    seqs, size = gates_ref.shape[1:]
    forget = gates_ref[0].T
    key_in = gates_ref[1].T
    for t in range(seqs):
        out_ref[t, 0] = (
            broadcast_column(forget, t, size) * state_ref[t, 0]
            + broadcast_column(key_in, t, size) * gates_ref[2, t : t + 1, :]
        )


def write_state(gates, old_state, first, count, partial=None):
    seqs, _, size, _ = old_state.shape
    block = pl.BlockSpec((seqs, 1, size, size), lambda h: (0, first + h, 0, 0))
    more = () if partial is None else (partial,)
    return pl.pallas_call(
        state_kernel,
        grid=(count,),
        in_specs=[pl.BlockSpec((3, seqs, size), lambda h: (0, 0, first + h)), block]
        + [pl.BlockSpec(memory_space=pl.ANY)] * len(more),
        out_specs=block,
        out_shape=jax.ShapeDtypeStruct(old_state.shape, F32),
        input_output_aliases={2: 0} if more else {},
        compiler_params=PARAMS,
        cost_estimate=pl.CostEstimate(
            flops=4 * old_state.size, bytes_accessed=8 * old_state.size, transcendentals=0
        ),
        name="write_state",
    )(gates, old_state, *more)


def body(
    tokens,
    old_state,
    lower_bound,
    head_gain,
    norm_gains,
    w_query,
    w_forget,
    w_value,
    w_outgate,
    w_mix_out,
    routes,
    route_scores,
    w_exp_gate,
    w_exp_up,
    w_exp_down,
    w_dense_gate,
    w_dense_up,
    w_dense_down,
    dense_mix,
):
    seqs, width = tokens.shape
    ep_index = lax.axis_index("ep")
    core_index = ep_index & 1
    ep_size = lax.axis_size("ep")
    chips = ep_size // 2
    feats = width // ep_size
    all_rows = ep_size * seqs

    mix_weights = background_gather(w_mix_out)

    half_ff = w_dense_gate.shape[1] // 2

    def half(weights, axis, which):
        return lax.dynamic_slice_in_dim(weights, which * half_ff, half_ff, axis)

    other_core = 1 - core_index
    pair = (w_dense_gate, w_dense_up)
    gate_up_out = jnp.concatenate([half(w, 1, other_core) for w in pair], axis=1)
    down_out = half(w_dense_down, 0, other_core)
    gate_up_own = jnp.concatenate([half(w, 1, core_index) for w in pair], axis=1)
    down_own = half(w_dense_down, 0, core_index)
    gate_row = dense_mix.reshape(1, width)
    gate_up_other = swap(gate_up_out, "ep", 1)
    down_other = swap(down_out, "ep", 1)

    lanes = -(-(ep_size + 1) // 128) * 128

    even, odd = front(tokens, norm_gains, ep_size)
    row_pairs = relative_exchange(even, odd)
    keep, send = project(row_pairs, (w_query, w_forget, w_value, w_outgate))
    own, sends = chip_sum(keep, swap(send, "ep", 1))
    arrived = chip_send(sends)
    mixed_heads, gates = read_heads(own, arrived, lower_bound, head_gain, old_state)
    heads = old_state.shape[1]
    early = -(-heads // 2)
    new_state = write_state(gates, old_state, 0, early)
    if heads > early:
        new_state = write_state(gates, old_state, early, heads - early, new_state)
    mix_part = mix_heads(mixed_heads, mix_weights)
    mix_pieces = [mix_part] + tp_exchange(mix_part)
    after_mix, packed = middle(
        tokens, norm_gains, gate_row, routes, route_scores, lanes, mix_pieces
    )

    gathered = relative_gather(packed).reshape(all_rows, packed.shape[1])
    rows = gathered[:, :width]
    side = gathered[:, width : width + lanes].astype(F32) + gathered[:, width + lanes :].astype(F32)
    expert_scale = lax.dynamic_slice_in_dim(side, ep_index, 1, 1)
    dense_scale = side[:, ep_size : ep_size + 1]

    def features(index):
        return lax.dynamic_slice_in_dim(rows, index * feats, feats, 1)

    dense_part = jnp.dot(features(ep_index), gate_up_own, preferred_element_type=F32) + jnp.dot(
        features(ep_index ^ 1), gate_up_other, preferred_element_type=F32
    )
    dense_part = dense_part.reshape(chips, 2 * seqs, -1)
    dense_sent = dense_part[1:].astype(BF16)
    dense_pre = total_of(dense_part[0], chip_send(list(dense_sent)))
    dense_gate_pre, dense_up_pre = jnp.split(dense_pre, 2, axis=1)
    dense_hidden = (jax.nn.silu(dense_gate_pre) * dense_up_pre).astype(BF16)
    all_hidden = chip_gather(dense_hidden)

    gate_pre = jnp.dot(rows, w_exp_gate[0], preferred_element_type=F32)
    gate_pre = lax.optimization_barrier(gate_pre)
    up_pre = jnp.dot(rows, w_exp_up[0], preferred_element_type=F32)
    hidden = (jax.nn.silu(gate_pre) * up_pre).astype(BF16)
    hidden = lax.optimization_barrier(hidden)
    expert_out = jnp.dot(hidden, w_exp_down[0], preferred_element_type=F32) * expert_scale
    expert_out = lax.optimization_barrier(expert_out)
    keep, send = join(expert_out, dense_scale, down_own, down_other, all_hidden, seqs)
    own, sends = chip_sum(keep, swap(send, "ep", 1))
    ffn_part = total_of(own, chip_send(sends)).astype(BF16)
    ffn_pieces = [ffn_part] + tp_exchange(ffn_part)
    return (finish(after_mix, norm_gains, ffn_pieces), new_state)


def solution(mesh):
    return jax.shard_map(
        body,        mesh=mesh,
        in_specs=(
            P("ep", None),
            P("ep", "tp", None, None),
            P("tp"),
            P("tp"),
            P(),
            P("ep", "tp"),
            P("ep", "tp"),
            P("ep", "tp"),
            P("ep", "tp"),
            P("tp", "ep"),
            P("ep", None),
            P("ep", None),
            P("ep", None, "tp"),
            P("ep", None, "tp"),
            P("ep", "tp", None),
            P("ep", "tp"),
            P("ep", "tp"),
            P("tp", "ep"),
            P(),
        ),
        out_specs=(P("ep", "tp"), P("ep", "tp", None, None)),
        check_vma=False,
    )
```

time: 320 us -> 117 us (0.37)
  waiting for transfers between devices: 217 us -> 48.7 us
  blocking collectives: 43.4 us -> 0 us
  starting transfers between devices: 4.89 us -> 42.1 us
  matrix products: 23.7 us -> 4.78 us
  between operations: 14.4 us -> 1.01 us
  other arithmetic: 11.5 us -> 1.06 us
  Pallas kernels: 0 us -> 10 us
  local copies, waits for them, and re-layouts: 4.25 us -> 8.55 us
    reduce_scatter x4 -> x0, waiting for transfers between devices: 92.4 us -> none  [the longest x1 29.5 us: body(): lax.psum_scatter(jnp.dot(dense_rows, dense_weights, preferred_element_typ...]
    all_gather x2 -> x0, waiting for transfers between devices: 82.4 us -> none  [the longest x1 63.9 us: body(): lax.all_gather(w_dense_down, 'ep', axis=1, tiled=True)]
    ppermute x0 -> x40, waiting for transfers between devices: none -> 48.7 us  [swap(): return lax.ppermute(value, axis, [(i, i ^ step) for i in range(size)])]
    ppermute x0 -> x40, starting transfers between devices: none -> 42.1 us  [swap(): return lax.ppermute(value, axis, [(i, i ^ step) for i in range(size)])]
    psum x1 -> x0, waiting for transfers between devices: 41.1 us -> none  [body(): mix_out = lax.psum(mix_part.astype(jnp.bfloat16), 'tp')]
    all_to_all x3 -> x0, blocking collectives: 34.5 us -> none  [the longest x1 14.1 us: body(): lax.all_to_all(outgoing, 'ep', split_axis=0, concat_axis=0, tiled=True)]
    dot_general x10 -> x5, matrix products: 23.7 us -> 4.78 us  [the longest x1 2.76 us: body(): gate_pre = jnp.dot(rows, w_exp_gate[0], preferred_element_type=F32)]
    pallas_call x0 -> x11, Pallas kernels: none -> 10 us  [the longest x2 5.14 us: write_state(): pl.pallas_call(state_kernel, grid=(count,), in_specs=[pl.BlockSpec((3, se...]
  transfers between devices with their start and end apart: 8 -> 40, of which waited for: 7 -> 22; matrix products, arithmetic and copies ran while one was open for 5% -> 8% of each run, Pallas kernels for 0% -> 8%
where the time goes in v1:
time: 117 us; the launch traced here: 116 us
  waiting for transfers between devices  48.7 us (42%)
  starting transfers between devices  42.1 us (36%)
  Pallas kernels  10 us (9%)
  local copies, waits for them, and re-layouts  8.55 us (7%)
  matrix products  4.78 us (4%)
    ppermute x40, waiting for transfers between devices, swap(): return lax.ppermute(value, axis, [(i, i ^ step) for i in range(size)])  48.7 us
    ppermute x40, starting transfers between devices, swap(): return lax.ppermute(value, axis, [(i, i ^ step) for i in range(size)])  42.1 us
    unnamed x45, local copies, waits for them, and re-layouts  5.67 us
    pallas_call x2, Pallas kernels, write_state(): pl.pallas_call(state_kernel, grid=(count,), in_specs=[pl.BlockSpec((3, se...  5.14 us
    dot_general x1, matrix products, body(): gate_pre = jnp.dot(rows, w_exp_gate[0], preferred_element_type=F32)  2.76 us
    dynamic_slice x2, local copies, waits for them, and re-layouts, half(): return lax.dynamic_slice_in_dim(weights, which * half_ff, half_ff, axis)  2.62 us
    pallas_call x1, Pallas kernels, read_heads(): call(lambda *refs: read_kernel(len(arrived), *refs), (jax.ShapeDtypeStruc...  2.54 us
  transfers between devices with their start and end apart: 40, of which 22 were waited for; matrix products, arithmetic and copies ran while one was open for 8% of the time, Pallas kernels for 8%

profile of v1, /device:TPU:0, one launch (start us, length us, event | category | flops | bytes accessed | tf_op | source)
XLA Modules:
  0.0 116.3 jit_solution(17350636127979474182)
XLA Ops:
  0.6 4.1 %collective-permute-start.11 = (bf16[512,256]{1,0:T(8,128)(2,1)}, bf16[512,256]{1,0:T(8,128)(2,1)S(1)}, u32[]{:S(2)}, u32[]{:S(2)}) collective-permute-start(bf16[512,256]{1,0:T(8,128)(2,1)} %refs_0_.2), channel_id=1, source_target_pairs={{0,16},{4,20},{8,24},{12,28},{16,0},{20,4},{24,8},{28,12},{1,17},{... | collective-permute-start | bytes 786440 | tf_op jit(solution)/shard_map/ppermute | solution.py:20
  4.8 0.8 copy-done.2
  5.5 0.8 copy-done.9
  6.6 1.2 %collective-permute-done = bf16[4,16,256]{2,1,0:T(8,128)(2,1)S(1)} collective-permute-done((bf16[4,16,256]{2,1,0:T(8,128)(2,1)S(1)}, bf16[4,16,256]{2,1,0:T(8,128)(2,1)S(1)}, u32[]{:S(2)}, u32[]{:S(2)}) %collective-permute-start) | collective-permute-done | bytes 32800 | tf_op jit(solution)/shard_map/ppermute | solution.py:20
  7.8 1.4 %collective-permute-start.3 = (bf16[2,16,256]{2,1,0:T(8,128)(2,1)S(1)}, bf16[2,16,256]{2,1,0:T(8,128)(2,1)S(1)}, u32[]{:S(2)}, u32[]{:S(2)}) collective-permute-start(bf16[2,16,256]{2,1,0:T(8,128)(2,1)S(1)} %get-tuple-element.49), channel_id=1, source_target_pairs={{0,24},{4,28},{8,16},{12,20},{16,8},{20,12},{24,0},{28,4},{1,25},{... | collective-permute-start | bytes 49160 | tf_op jit(solution)/shard_map/ppermute | solution.py:20
  9.5 2.7 %collective-permute-start.2 = (bf16[2,16,256]{2,1,0:T(8,128)(2,1)S(1)}, bf16[2,16,256]{2,1,0:T(8,128)(2,1)S(1)}, u32[]{:S(2)}, u32[]{:S(2)}) collective-permute-start(bf16[2,16,256]{2,1,0:T(8,128)(2,1)S(1)} %get-tuple-element.52), channel_id=1, source_target_pairs={{0,16},{4,20},{8,24},{12,28},{16,0},{20,4},{24,8},{28,12},{1,17},{... | collective-permute-start | bytes 49160 | tf_op jit(solution)/shard_map/ppermute | solution.py:20
  12.2 1.3 %collective-permute-done.3.refs_3_ = bf16[2,16,256]{2,1,0:T(8,128)(2,1)S(1)} collective-permute-done((bf16[2,16,256]{2,1,0:T(8,128)(2,1)S(1)}, bf16[2,16,256]{2,1,0:T(8,128)(2,1)S(1)}, u32[]{:S(2)}, u32[]{:S(2)}) %collective-permute-start.3) | collective-permute-done | bytes 16416 | tf_op jit(solution)/shard_map/ppermute | solution.py:20
  13.8 4.5 %collective-permute-done.2.refs_2_ = bf16[2,16,256]{2,1,0:T(8,128)(2,1)S(1)} collective-permute-done((bf16[2,16,256]{2,1,0:T(8,128)(2,1)S(1)}, bf16[2,16,256]{2,1,0:T(8,128)(2,1)S(1)}, u32[]{:S(2)}, u32[]{:S(2)}) %collective-permute-start.2) | collective-permute-done | bytes 16416 | tf_op jit(solution)/shard_map/ppermute | solution.py:20
  18.3 0.9 copy-done.4
  19.3 0.9 copy-done.5
  20.2 0.9 copy-done.6
  21.2 0.9 copy-done.7
  22.5 0.8 collective-permute-start.9
  23.3 1.3 %collective-permute-start.13 = (bf16[512,256]{1,0:T(8,128)(2,1)S(1)}, bf16[512,256]{1,0:T(8,128)(2,1)S(1)}, u32[]{:S(2)}, u32[]{:S(2)}) collective-permute-start(bf16[512,256]{1,0:T(8,128)(2,1)S(1)} %collective-permute-done.11.refs_4_), channel_id=1, source_target_pairs={{0,8},{4,12},{8,0},{12,4},{16,24},{20,28},{24,16},{28,20},{1,9},{5... | collective-permute-start | bytes 786440 | tf_op jit(solution)/shard_map/ppermute | solution.py:20
  24.7 0.8 collective-permute-start.5
  25.4 0.5 collective-permute-start.12
  26.0 6.0 %collective-permute-done.9.refs_2_ = bf16[512,256]{1,0:T(8,128)(2,1)S(1)} collective-permute-done((bf16[512,256]{1,0:T(8,128)(2,1)}, bf16[512,256]{1,0:T(8,128)(2,1)S(1)}, u32[]{:S(2)}, u32[]{:S(2)}) %collective-permute-start.9) | collective-permute-done | bytes 262176 | tf_op jit(solution)/shard_map/ppermute | solution.py:20
  31.9 6.5 %collective-permute-done.5.refs_1_ = bf16[16,2048]{1,0:T(8,128)(2,1)S(1)} collective-permute-done((bf16[16,2048]{1,0:T(8,128)(2,1)S(1)}, bf16[16,2048]{1,0:T(8,128)(2,1)S(1)}, u32[]{:S(2)}, u32[]{:S(2)}) %collective-permute-start.5) | collective-permute-done | bytes 65568 | tf_op jit(solution)/shard_map/ppermute | solution.py:20
  38.4 2.4 %collective-permute-start.6 = (bf16[16,2048]{1,0:T(8,128)(2,1)S(1)}, bf16[16,2048]{1,0:T(8,128)(2,1)S(1)}, u32[]{:S(2)}, u32[]{:S(2)}) collective-permute-start(bf16[16,2048]{1,0:T(8,128)(2,1)S(1)} %get-tuple-element.26), channel_id=1, source_target_pairs={{0,16},{4,20},{8,24},{12,28},{16,0},{20,4},{24,8},{28,12},{1,17},{... | collective-permute-start | bytes 196616 | tf_op jit(solution)/shard_map/ppermute | solution.py:20
  40.8 1.5 %constant_dynamic-slice_fusion = (bf16[256,768]{1,0:T(8,128)(2,1)S(1)}, bf16[256,768]{1,0:T(8,128)(2,1)S(1)}, bf16[256,768]{1,0:T(8,128)(2,1)S(1)}, bf16[256,768]{1,0:T(8,128)(2,1)S(1)}) fusion(bf16[256,1536]{1,0:T(8,128)(2,1)} %param.35, s32[]{:T(128)S(6)} %select_n.21, s32[]{:T(128)S(6)} %select_n.20, bf16[256,1536]{1,0:T(8,128)(2,1)} %param.34), kind=kLoop, calls=%fused_computation.47 | loop fusion | bytes 3145736 | tf_op jit(solution)/shard_map/dynamic_slice | solution.py:419
  42.3 2.2 %collective-permute-done.6.refs_2_ = bf16[16,2048]{1,0:T(8,128)(2,1)S(1)} collective-permute-done((bf16[16,2048]{1,0:T(8,128)(2,1)S(1)}, bf16[16,2048]{1,0:T(8,128)(2,1)S(1)}, u32[]{:S(2)}, u32[]{:S(2)}) %collective-permute-start.6) | collective-permute-done | bytes 65568 | tf_op jit(solution)/shard_map/ppermute | solution.py:20
  44.5 3.1 %collective-permute-start.7 = (bf16[16,2048]{1,0:T(8,128)(2,1)S(1)}, bf16[16,2048]{1,0:T(8,128)(2,1)S(1)}, u32[]{:S(2)}, u32[]{:S(2)}) collective-permute-start(bf16[16,2048]{1,0:T(8,128)(2,1)S(1)} %get-tuple-element.27), channel_id=1, source_target_pairs={{0,24},{4,28},{8,16},{12,20},{16,8},{20,12},{24,0},{28,4},{1,25},{... | collective-permute-start | bytes 196616 | tf_op jit(solution)/shard_map/ppermute | solution.py:20
  47.6 1.2 %constant_dynamic-slice_fusion.4 = (bf16[768,256]{1,0:T(8,128)(2,1)S(1)}, bf16[768,256]{1,0:T(8,128)(2,1)S(1)}) fusion(bf16[1536,256]{1,0:T(8,128)(2,1)} %param.36, s32[]{:T(128)S(6)} %select_n.21, s32[]{:T(128)S(6)} %select_n.20), kind=kLoop, calls=%fused_computation.53 | loop fusion | bytes 1572872 | tf_op jit(solution)/shard_map/dynamic_slice | solution.py:419
  48.8 1.8 %collective-permute-done.7.refs_3_ = bf16[16,2048]{1,0:T(8,128)(2,1)S(1)} collective-permute-done((bf16[16,2048]{1,0:T(8,128)(2,1)S(1)}, bf16[16,2048]{1,0:T(8,128)(2,1)S(1)}, u32[]{:S(2)}, u32[]{:S(2)}) %collective-permute-start.7) | collective-permute-done | bytes 65568 | tf_op jit(solution)/shard_map/ppermute | solution.py:20
  50.6 2.5 %shard_map.197 = (bf16[16,512]{1,0:T(8,128)(2,1)S(1)}, f32[3,16,512]{2,1,0:T(8,128)S(1)}) custom-call(f32[16,2048]{1,0:T(8,128)S(1)} %get-tuple-element.24.refs_0_, bf16[16,2048]{1,0:T(8,128)(2,1)S(1)} %collective-permute-done.5.refs_1_, bf16[16,2048]{1,0:T(8,128)(2,1)S(1)} %collective-permute-done.6.refs_2_, ...), custom_call_target="tpu_custom_call" | custom-call | flops 1048576 | bytes 1048576 | tf_op jit(solution)/shard_map/pallas_call | solution.py:344
  53.2 0.4 shard_map.198.refs_5_
  53.6 2.5 %collective-permute-start.17 = (bf16[16,2048]{1,0:T(8,128)(2,1)S(1)}, bf16[16,2048]{1,0:T(8,128)(2,1)S(1)}, u32[]{:S(2)}, u32[]{:S(2)}) collective-permute-start(bf16[16,2048]{1,0:T(8,128)(2,1)S(1)} %shard_map.198.refs_5_), channel_id=1, source_target_pairs={{0,3},{1,2},{2,1},{3,0},{4,7},{5,6},{6,5},{7,4},{8,11},{9,10},{10,... | collective-permute-start | bytes 196616 | tf_op jit(solution)/shard_map/ppermute | solution.py:20
  56.1 0.5 collective-permute-start.16
  56.6 0.5 collective-permute-start.15
  57.1 0.9 pad_maximum_fusion
  58.2 0.8 collective-permute-done.17.refs_8_
  59.0 1.4 %collective-permute-done.16.refs_7_ = bf16[16,2048]{1,0:T(8,128)(2,1)S(1)} collective-permute-done((bf16[16,2048]{1,0:T(8,128)(2,1)S(1)}, bf16[16,2048]{1,0:T(8,128)(2,1)S(1)}, u32[]{:S(2)}, u32[]{:S(2)}) %collective-permute-start.16) | collective-permute-done | bytes 65568 | tf_op jit(solution)/shard_map/ppermute | solution.py:20
  60.4 0.4 collective-permute-done.15.refs_6_
  60.9 0.4 shard_map.199
  61.3 3.2 %collective-permute-start.23 = (bf16[16,2304]{1,0:T(8,128)(2,1)S(1)}, bf16[16,2304]{1,0:T(8,128)(2,1)S(1)}, u32[]{:S(2)}, u32[]{:S(2)}) collective-permute-start(bf16[16,2304]{1,0:T(8,128)(2,1)S(1)} %get-tuple-element.30), channel_id=1, source_target_pairs={{0,24},{4,28},{8,16},{12,20},{16,8},{20,12},{24,0},{28,4},{1,25},{... | collective-permute-start | bytes 221192 | tf_op jit(solution)/shard_map/ppermute | solution.py:20
  64.4 1.3 %collective-permute-start.19 = (bf16[16,2304]{1,0:T(8,128)(2,1)S(1)}, bf16[16,2304]{1,0:T(8,128)(2,1)S(1)}, u32[]{:S(2)}, u32[]{:S(2)}) collective-permute-start(bf16[16,2304]{1,0:T(8,128)(2,1)S(1)} %get-tuple-element.30), channel_id=1, source_target_pairs={{0,8},{4,12},{8,0},{12,4},{16,24},{20,28},{24,16},{28,20},{1,9},{5... | collective-permute-start | bytes 221192 | tf_op jit(solution)/shard_map/ppermute | solution.py:20
  65.7 1.8 %collective-permute-done.23 = bf16[16,2304]{1,0:T(8,128)(2,1)S(1)} collective-permute-done((bf16[16,2304]{1,0:T(8,128)(2,1)S(1)}, bf16[16,2304]{1,0:T(8,128)(2,1)S(1)}, u32[]{:S(2)}, u32[]{:S(2)}) %collective-permute-start.23) | collective-permute-done | bytes 73760 | tf_op jit(solution)/shard_map/ppermute | solution.py:20
  67.6 2.4 %collective-permute-done.21 = bf16[16,2304]{1,0:T(8,128)(2,1)S(1)} collective-permute-done((bf16[16,2304]{1,0:T(8,128)(2,1)S(1)}, bf16[16,2304]{1,0:T(8,128)(2,1)S(1)}, u32[]{:S(2)}, u32[]{:S(2)}) %collective-permute-start.21) | collective-permute-done | bytes 73760 | tf_op jit(solution)/shard_map/ppermute | solution.py:20
  69.9 0.3 collective-permute-done.19
  70.8 0.9 collective-permute-done.20
  71.9 2.8 %fusion.4 = f32[128,896]{1,0:T(8,128)S(1)} fusion(bf16[1,2048,896]{2,1,0:T(8,128)(2,1)} %param.31, bf16[128,2304]{1,0:T(8,128)(2,1)S(1)} %bitcast.50), kind=kOutput, calls=%fused_computation.4 | convolution fusion | flops 469762048 | bytes 4653056 | tf_op jit(solution)/shard_map/dot_general | solution.py:469
  75.3 0.6 collective-permute-start.27
  75.9 2.3 %collective-permute-start.29 = (bf16[32,1536]{1,0:T(8,128)(2,1)S(1)}, bf16[32,1536]{1,0:T(8,128)(2,1)S(1)}, u32[]{:S(2)}, u32[]{:S(2)}) collective-permute-start(bf16[32,1536]{1,0:T(8,128)(2,1)S(1)} %get-tuple-element.45), channel_id=1, source_target_pairs={{0,24},{4,28},{8,16},{12,20},{16,8},{20,12},{24,0},{28,4},{1,25},{... | collective-permute-start | bytes 294920 | tf_op jit(solution)/shard_map/ppermute | solution.py:20
  78.2 0.6 collective-permute-start.28
  78.8 0.7 fusion.12
  79.7 0.6 collective-permute-done.27
  80.4 3.7 %collective-permute-done.29 = bf16[32,1536]{1,0:T(8,128)(2,1)S(1)} collective-permute-done((bf16[32,1536]{1,0:T(8,128)(2,1)S(1)}, bf16[32,1536]{1,0:T(8,128)(2,1)S(1)}, u32[]{:S(2)}, u32[]{:S(2)}) %collective-permute-start.29) | collective-permute-done | bytes 98336 | tf_op jit(solution)/shard_map/ppermute | solution.py:20
  84.0 3.8 %collective-permute-done.28 = bf16[32,1536]{1,0:T(8,128)(2,1)S(1)} collective-permute-done((bf16[32,1536]{1,0:T(8,128)(2,1)S(1)}, bf16[32,1536]{1,0:T(8,128)(2,1)S(1)}, u32[]{:S(2)}, u32[]{:S(2)}) %collective-permute-start.28) | collective-permute-done | bytes 98336 | tf_op jit(solution)/shard_map/ppermute | solution.py:20
  87.9 2.2 %collective-permute-start.32 = (bf16[32,768]{1,0:T(8,128)(2,1)S(1)}, bf16[32,768]{1,0:T(8,128)(2,1)S(1)}, u32[]{:S(2)}, u32[]{:S(2)}) collective-permute-start(bf16[32,768]{1,0:T(8,128)(2,1)S(1)} %fusion.21.refs_4_), channel_id=1, source_target_pairs={{0,24},{4,28},{8,16},{12,20},{16,8},{20,12},{24,0},{28,4},{1,25},{... | collective-permute-start | bytes 147464 | tf_op jit(solution)/shard_map/ppermute | solution.py:20
  90.2 2.2 %collective-permute-start.30 = (bf16[32,768]{1,0:T(8,128)(2,1)S(1)}, bf16[32,768]{1,0:T(8,128)(2,1)S(1)}, u32[]{:S(2)}, u32[]{:S(2)}) collective-permute-start(bf16[32,768]{1,0:T(8,128)(2,1)S(1)} %fusion.21.refs_4_), channel_id=1, source_target_pairs={{0,8},{4,12},{8,0},{12,4},{16,24},{20,28},{24,16},{28,20},{1,9},{5... | collective-permute-start | bytes 147464 | tf_op jit(solution)/shard_map/ppermute | solution.py:20
  92.4 0.7 fusion.6.refs_0_
  93.2 0.8 collective-permute-done.32.refs_7_
  93.9 1.4 %collective-permute-done.31.refs_6_ = bf16[32,768]{1,0:T(8,128)(2,1)S(1)} collective-permute-done((bf16[32,768]{1,0:T(8,128)(2,1)S(1)}, bf16[32,768]{1,0:T(8,128)(2,1)S(1)}, u32[]{:S(2)}, u32[]{:S(2)}) %collective-permute-start.31) | collective-permute-done | bytes 49184 | tf_op jit(solution)/shard_map/ppermute | solution.py:20
  95.7 1.5 %collective-permute-done.33.crossed_ref = bf16[4,16,2048]{2,1,0:T(8,128)(2,1)S(1)} collective-permute-done((bf16[4,16,2048]{2,1,0:T(8,128)(2,1)S(1)}, bf16[4,16,2048]{2,1,0:T(8,128)(2,1)S(1)}, u32[]{:S(2)}, u32[]{:S(2)}) %collective-permute-start.33) | collective-permute-done | bytes 262176 | tf_op jit(solution)/shard_map/ppermute | solution.py:20
  97.3 1.2 %collective-permute-start.34 = (bf16[16,2048]{1,0:T(8,128)(2,1)S(1)}, bf16[16,2048]{1,0:T(8,128)(2,1)S(1)}, u32[]{:S(2)}, u32[]{:S(2)}) collective-permute-start(bf16[16,2048]{1,0:T(8,128)(2,1)S(1)} %get-tuple-element.34), channel_id=1, source_target_pairs={{0,8},{4,12},{8,0},{12,4},{16,24},{20,28},{24,16},{28,20},{1,9},{5... | collective-permute-start | bytes 196616 | tf_op jit(solution)/shard_map/ppermute | solution.py:20
  98.5 1.4 %collective-permute-start.35 = (bf16[16,2048]{1,0:T(8,128)(2,1)S(1)}, bf16[16,2048]{1,0:T(8,128)(2,1)S(1)}, u32[]{:S(2)}, u32[]{:S(2)}) collective-permute-start(bf16[16,2048]{1,0:T(8,128)(2,1)S(1)} %get-tuple-element.35), channel_id=1, source_target_pairs={{0,16},{4,20},{8,24},{12,28},{16,0},{20,4},{24,8},{28,12},{1,17},{... | collective-permute-start | bytes 196616 | tf_op jit(solution)/shard_map/ppermute | solution.py:20
  99.9 1.8 %collective-permute-start.36 = (bf16[16,2048]{1,0:T(8,128)(2,1)S(1)}, bf16[16,2048]{1,0:T(8,128)(2,1)S(1)}, u32[]{:S(2)}, u32[]{:S(2)}) collective-permute-start(bf16[16,2048]{1,0:T(8,128)(2,1)S(1)} %get-tuple-element.36), channel_id=1, source_target_pairs={{0,24},{4,28},{8,16},{12,20},{16,8},{20,12},{24,0},{28,4},{1,25},{... | collective-permute-start | bytes 196616 | tf_op jit(solution)/shard_map/ppermute | solution.py:20
  101.8 5.0 %collective-permute-done.35 = bf16[16,2048]{1,0:T(8,128)(2,1)S(1)} collective-permute-done((bf16[16,2048]{1,0:T(8,128)(2,1)S(1)}, bf16[16,2048]{1,0:T(8,128)(2,1)S(1)}, u32[]{:S(2)}, u32[]{:S(2)}) %collective-permute-start.35) | collective-permute-done | bytes 65568 | tf_op jit(solution)/shard_map/ppermute | solution.py:20
  106.8 1.6 %collective-permute-start.39 = (bf16[16,2048]{1,0:T(8,128)(2,1)S(1)}, bf16[16,2048]{1,0:T(8,128)(2,1)S(1)}, u32[]{:S(2)}, u32[]{:S(2)}) collective-permute-start(bf16[16,2048]{1,0:T(8,128)(2,1)S(1)} %add_convert_fusion.refs_2_), channel_id=1, source_target_pairs={{0,3},{1,2},{2,1},{3,0},{4,7},{5,6},{6,5},{7,4},{8,11},{9,10},{10,... | collective-permute-start | bytes 196616 | tf_op jit(solution)/shard_map/ppermute | solution.py:20
  108.4 1.5 %collective-permute-start.38 = (bf16[16,2048]{1,0:T(8,128)(2,1)S(1)}, bf16[16,2048]{1,0:T(8,128)(2,1)S(1)}, u32[]{:S(2)}, u32[]{:S(2)}) collective-permute-start(bf16[16,2048]{1,0:T(8,128)(2,1)S(1)} %add_convert_fusion.refs_2_), channel_id=1, source_target_pairs={{0,2},{1,3},{2,0},{3,1},{4,6},{5,7},{6,4},{7,5},{8,10},{9,11},{10,... | collective-permute-start | bytes 196616 | tf_op jit(solution)/shard_map/ppermute | solution.py:20
  109.8 0.5 collective-permute-start.37
  110.4 2.6 %write_state.2.refs_0_ = f32[16,4,128,128]{3,2,1,0:T(8,128)} custom-call(f32[3,16,512]{2,1,0:T(8,128)S(1)} %get-tuple-element.37.gates_ref, f32[16,4,128,128]{3,2,1,0:T(8,128)S(1)} %copy-done.1), custom_call_target="tpu_custom_call" | custom-call | flops 4194304 | bytes 8388608 | tf_op jit(solution)/shard_map/write_state/pallas_call | solution.py:369
  112.9 2.6 %write_state.3 = f32[16,4,128,128]{3,2,1,0:T(8,128)} custom-call(f32[3,16,512]{2,1,0:T(8,128)S(1)} %get-tuple-element.37.gates_ref, f32[16,4,128,128]{3,2,1,0:T(8,128)S(1)} %copy-done.1, f32[16,4,128,128]{3,2,1,0:T(8,128)} %write_state.2.refs_0_), custom_call_target="tpu_custom_call", output_to_operand_aliasing={{}: (2, {})} | custom-call | flops 4194304 | bytes 8388608 | tf_op jit(solution)/shard_map/write_state/pallas_call | solution.py:369
  115.5 0.7 shard_map.202
  (90 shorter events, 3.5 us)
Async XLA Ops:
  0.6 22.6 %collective-permute-start.11 = (bf16[512,256]{1,0:T(8,128)(2,1)}, bf16[512,256]{1,0:T(8,128)(2,1)S(1)}, u32[]{:S(2)}, u32[]{:S(2)}) collective-permute-start(bf16[512,256]{1,0:T(8,128)(2,1)} %refs_0_.2), channel_id=1, source_target_pairs={{0,16},{4,20},{8,24},{12,28},{16,0},{20,4},{24,8},{28,12},{1,17},{... | collective-permute-start | bytes 786440 | tf_op jit(solution)/shard_map/ppermute | solution.py:20
  4.8 0.8 copy-start.2
  5.5 0.8 copy-start.9
  6.4 44.2 %copy-start.11 = (f32[512]{0:T(512)S(1)}, f32[512]{0:T(512)}, u32[]{:S(2)}) copy-start(f32[512]{0:T(512)} %param.21) | copy-start | bytes 6148
  6.4 44.2 %copy-start.12 = (f32[512]{0:T(512)S(1)}, f32[512]{0:T(512)}, u32[]{:S(2)}) copy-start(f32[512]{0:T(512)} %param.22) | copy-start | bytes 6148
  6.5 1.3 %collective-permute-start = (bf16[4,16,256]{2,1,0:T(8,128)(2,1)S(1)}, bf16[4,16,256]{2,1,0:T(8,128)(2,1)S(1)}, u32[]{:S(2)}, u32[]{:S(2)}) collective-permute-start(bf16[4,16,256]{2,1,0:T(8,128)(2,1)S(1)} %get-tuple-element.21), channel_id=1, source_target_pairs={{0,4},{4,0},{8,12},{12,8},{16,20},{20,16},{24,28},{28,24},{1,5},{5... | collective-permute-start | bytes 98312 | tf_op jit(solution)/shard_map/ppermute | solution.py:20
  7.8 5.8 %collective-permute-start.3 = (bf16[2,16,256]{2,1,0:T(8,128)(2,1)S(1)}, bf16[2,16,256]{2,1,0:T(8,128)(2,1)S(1)}, u32[]{:S(2)}, u32[]{:S(2)}) collective-permute-start(bf16[2,16,256]{2,1,0:T(8,128)(2,1)S(1)} %get-tuple-element.49), channel_id=1, source_target_pairs={{0,24},{4,28},{8,16},{12,20},{16,8},{20,12},{24,0},{28,4},{1,25},{... | collective-permute-start | bytes 49160 | tf_op jit(solution)/shard_map/ppermute | solution.py:20
  9.2 4.7 %collective-permute-start.1 = (bf16[2,16,256]{2,1,0:T(8,128)(2,1)S(1)}, bf16[2,16,256]{2,1,0:T(8,128)(2,1)S(1)}, u32[]{:S(2)}, u32[]{:S(2)}) collective-permute-start(bf16[2,16,256]{2,1,0:T(8,128)(2,1)S(1)} %get-tuple-element.51), channel_id=1, source_target_pairs={{0,8},{4,12},{8,0},{12,4},{16,24},{20,28},{24,16},{28,20},{1,9},{5... | collective-permute-start | bytes 49160 | tf_op jit(solution)/shard_map/ppermute | solution.py:20
  9.5 8.8 %collective-permute-start.2 = (bf16[2,16,256]{2,1,0:T(8,128)(2,1)S(1)}, bf16[2,16,256]{2,1,0:T(8,128)(2,1)S(1)}, u32[]{:S(2)}, u32[]{:S(2)}) collective-permute-start(bf16[2,16,256]{2,1,0:T(8,128)(2,1)S(1)} %get-tuple-element.52), channel_id=1, source_target_pairs={{0,16},{4,20},{8,24},{12,28},{16,0},{20,4},{24,8},{28,12},{1,17},{... | collective-permute-start | bytes 49160 | tf_op jit(solution)/shard_map/ppermute | solution.py:20
  18.3 1.0 copy-start.4
  19.3 0.9 copy-start.5
  20.2 0.9 copy-start.6
  21.2 0.9 copy-start.7
  22.4 2.2 %collective-permute-start.4 = (bf16[4,16,2048]{2,1,0:T(8,128)(2,1)S(1)}, bf16[4,16,2048]{2,1,0:T(8,128)(2,1)S(1)}, u32[]{:S(2)}, u32[]{:S(2)}) collective-permute-start(bf16[4,16,2048]{2,1,0:T(8,128)(2,1)S(1)} %get-tuple-element.23), channel_id=1, source_target_pairs={{0,4},{4,0},{8,12},{12,8},{16,20},{20,16},{24,28},{28,24},{1,5},{5... | collective-permute-start | bytes 786440 | tf_op jit(solution)/shard_map/ppermute | solution.py:20
  22.5 9.5 %collective-permute-start.9 = (bf16[512,256]{1,0:T(8,128)(2,1)}, bf16[512,256]{1,0:T(8,128)(2,1)S(1)}, u32[]{:S(2)}, u32[]{:S(2)}) collective-permute-start(bf16[512,256]{1,0:T(8,128)(2,1)} %refs_0_.2), channel_id=1, source_target_pairs={{0,8},{4,12},{8,0},{12,4},{16,24},{20,28},{24,16},{28,20},{1,9},{5... | collective-permute-start | bytes 786440 | tf_op jit(solution)/shard_map/ppermute | solution.py:20
  23.3 17.5 %collective-permute-start.13 = (bf16[512,256]{1,0:T(8,128)(2,1)S(1)}, bf16[512,256]{1,0:T(8,128)(2,1)S(1)}, u32[]{:S(2)}, u32[]{:S(2)}) collective-permute-start(bf16[512,256]{1,0:T(8,128)(2,1)S(1)} %collective-permute-done.11.refs_4_), channel_id=1, source_target_pairs={{0,8},{4,12},{8,0},{12,4},{16,24},{20,28},{24,16},{28,20},{1,9},{5... | collective-permute-start | bytes 786440 | tf_op jit(solution)/shard_map/ppermute | solution.py:20
  24.7 13.8 %collective-permute-start.5 = (bf16[16,2048]{1,0:T(8,128)(2,1)S(1)}, bf16[16,2048]{1,0:T(8,128)(2,1)S(1)}, u32[]{:S(2)}, u32[]{:S(2)}) collective-permute-start(bf16[16,2048]{1,0:T(8,128)(2,1)S(1)} %get-tuple-element.25), channel_id=1, source_target_pairs={{0,8},{4,12},{8,0},{12,4},{16,24},{20,28},{24,16},{28,20},{1,9},{5... | collective-permute-start | bytes 196616 | tf_op jit(solution)/shard_map/ppermute | solution.py:20
  25.4 27.7 %collective-permute-start.8 = (bf16[512,256]{1,0:T(8,128)(2,1)}, bf16[512,256]{1,0:T(8,128)(2,1)S(1)}, u32[]{:S(2)}, u32[]{:S(2)}) collective-permute-start(bf16[512,256]{1,0:T(8,128)(2,1)} %refs_0_.2), channel_id=1, source_target_pairs={{0,4},{4,0},{8,12},{12,8},{16,20},{20,16},{24,28},{28,24},{1,5},{5... | collective-permute-start | bytes 786440 | tf_op jit(solution)/shard_map/ppermute | solution.py:20
  25.4 25.1 %copy-start = (f32[16,4,128,128]{3,2,1,0:T(8,128)S(1)}, f32[16,4,128,128]{3,2,1,0:T(8,128)}, u32[]{:S(2)}) copy-start(f32[16,4,128,128]{3,2,1,0:T(8,128)} %state_ref.3) | copy-start | bytes 12582916
  25.4 27.8 %collective-permute-start.12 = (bf16[512,256]{1,0:T(8,128)(2,1)S(1)}, bf16[512,256]{1,0:T(8,128)(2,1)S(1)}, u32[]{:S(2)}, u32[]{:S(2)}) collective-permute-start(bf16[512,256]{1,0:T(8,128)(2,1)S(1)} %collective-permute-done.11.refs_4_), channel_id=1, source_target_pairs={{0,4},{4,0},{8,12},{12,8},{16,20},{20,16},{24,28},{28,24},{1,5},{5... | collective-permute-start | bytes 786440 | tf_op jit(solution)/shard_map/ppermute | solution.py:20
  31.9 21.3 %collective-permute-start.10 = (bf16[512,256]{1,0:T(8,128)(2,1)S(1)}, bf16[512,256]{1,0:T(8,128)(2,1)S(1)}, u32[]{:S(2)}, u32[]{:S(2)}) collective-permute-start(bf16[512,256]{1,0:T(8,128)(2,1)S(1)} %collective-permute-done.9.refs_2_), channel_id=1, source_target_pairs={{0,4},{4,0},{8,12},{12,8},{16,20},{20,16},{24,28},{28,24},{1,5},{5... | collective-permute-start | bytes 786440 | tf_op jit(solution)/shard_map/ppermute | solution.py:20
  38.4 6.1 %collective-permute-start.6 = (bf16[16,2048]{1,0:T(8,128)(2,1)S(1)}, bf16[16,2048]{1,0:T(8,128)(2,1)S(1)}, u32[]{:S(2)}, u32[]{:S(2)}) collective-permute-start(bf16[16,2048]{1,0:T(8,128)(2,1)S(1)} %get-tuple-element.26), channel_id=1, source_target_pairs={{0,16},{4,20},{8,24},{12,28},{16,0},{20,4},{24,8},{28,12},{1,17},{... | collective-permute-start | bytes 196616 | tf_op jit(solution)/shard_map/ppermute | solution.py:20
  40.8 12.4 %collective-permute-start.14 = (bf16[512,256]{1,0:T(8,128)(2,1)S(1)}, bf16[512,256]{1,0:T(8,128)(2,1)S(1)}, u32[]{:S(2)}, u32[]{:S(2)}) collective-permute-start(bf16[512,256]{1,0:T(8,128)(2,1)S(1)} %collective-permute-done.13.refs_6_), channel_id=1, source_target_pairs={{0,4},{4,0},{8,12},{12,8},{16,20},{20,16},{24,28},{28,24},{1,5},{5... | collective-permute-start | bytes 786440 | tf_op jit(solution)/shard_map/ppermute | solution.py:20
  42.3 10.9 %copy-start.8 = (bf16[512,256]{1,0:T(8,128)(2,1)S(1)}, bf16[512,256]{1,0:T(8,128)(2,1)}, u32[]{:S(2)}) copy-start(bf16[512,256]{1,0:T(8,128)(2,1)} %refs_0_.2) | copy-start | bytes 786436
  44.5 6.1 %collective-permute-start.7 = (bf16[16,2048]{1,0:T(8,128)(2,1)S(1)}, bf16[16,2048]{1,0:T(8,128)(2,1)S(1)}, u32[]{:S(2)}, u32[]{:S(2)}) collective-permute-start(bf16[16,2048]{1,0:T(8,128)(2,1)S(1)} %get-tuple-element.27), channel_id=1, source_target_pairs={{0,24},{4,28},{8,16},{12,20},{16,8},{20,12},{24,0},{28,4},{1,25},{... | collective-permute-start | bytes 196616 | tf_op jit(solution)/shard_map/ppermute | solution.py:20
  50.6 42.6 %collective-permute-start.25 = (bf16[768,256]{1,0:T(8,128)(2,1)S(1)}, bf16[768,256]{1,0:T(8,128)(2,1)S(1)}, u32[]{:S(2)}, u32[]{:S(2)}) collective-permute-start(bf16[768,256]{1,0:T(8,128)(2,1)S(1)} %get-tuple-element.42), channel_id=1, source_target_pairs={{0,4},{4,0},{8,12},{12,8},{16,20},{20,16},{24,28},{28,24},{1,5},{5... | collective-permute-start | bytes 1179656 | tf_op jit(solution)/shard_map/ppermute | solution.py:20
  50.6 7.5 %copy-start.15 = (s32[16,2]{0,1:T(2,128)S(1)}, s32[16,2]{0,1:T(2,128)}, u32[]{:S(2)}) copy-start(s32[16,2]{0,1:T(2,128)} %param.29) | copy-start | bytes 388
  50.6 7.5 %copy-start.16 = (f32[16,2]{0,1:T(2,128)S(1)}, f32[16,2]{0,1:T(2,128)}, u32[]{:S(2)}) copy-start(f32[16,2]{0,1:T(2,128)} %param.30) | copy-start | bytes 388
  50.6 7.6 %copy-start.14 = (bf16[2048]{0:T(1024)(128)(2,1)S(1)}, bf16[2048]{0:T(1024)(128)(2,1)}, u32[]{:S(2)}) copy-start(bf16[2048]{0:T(1024)(128)(2,1)} %param.37) | copy-start | bytes 12292
  50.6 10.2 %copy-start.3 = (f32[4,2048]{1,0:T(4,128)S(1)}, f32[4,2048]{1,0:T(4,128)}, u32[]{:S(2)}) copy-start(f32[4,2048]{1,0:T(4,128)} %refs_1_.3) | copy-start | bytes 98308
  50.6 10.2 %copy-start.10 = (bf16[16,2048]{1,0:T(8,128)(2,1)S(1)}, bf16[16,2048]{1,0:T(8,128)(2,1)}, u32[]{:S(2)}) copy-start(bf16[16,2048]{1,0:T(8,128)(2,1)} %refs_0_.3) | copy-start | bytes 196612
  53.6 5.4 %collective-permute-start.17 = (bf16[16,2048]{1,0:T(8,128)(2,1)S(1)}, bf16[16,2048]{1,0:T(8,128)(2,1)S(1)}, u32[]{:S(2)}, u32[]{:S(2)}) collective-permute-start(bf16[16,2048]{1,0:T(8,128)(2,1)S(1)} %shard_map.198.refs_5_), channel_id=1, source_target_pairs={{0,3},{1,2},{2,1},{3,0},{4,7},{5,6},{6,5},{7,4},{8,11},{9,10},{10,... | collective-permute-start | bytes 196616 | tf_op jit(solution)/shard_map/ppermute | solution.py:20
  56.1 4.3 %collective-permute-start.16 = (bf16[16,2048]{1,0:T(8,128)(2,1)S(1)}, bf16[16,2048]{1,0:T(8,128)(2,1)S(1)}, u32[]{:S(2)}, u32[]{:S(2)}) collective-permute-start(bf16[16,2048]{1,0:T(8,128)(2,1)S(1)} %shard_map.198.refs_5_), channel_id=1, source_target_pairs={{0,2},{1,3},{2,0},{3,1},{4,6},{5,7},{6,4},{7,5},{8,10},{9,11},{10,... | collective-permute-start | bytes 196616 | tf_op jit(solution)/shard_map/ppermute | solution.py:20
  56.6 4.3 %collective-permute-start.15 = (bf16[16,2048]{1,0:T(8,128)(2,1)S(1)}, bf16[16,2048]{1,0:T(8,128)(2,1)S(1)}, u32[]{:S(2)}, u32[]{:S(2)}) collective-permute-start(bf16[16,2048]{1,0:T(8,128)(2,1)S(1)} %shard_map.198.refs_5_), channel_id=1, source_target_pairs={{0,1},{1,0},{2,3},{3,2},{4,5},{5,4},{6,7},{7,6},{8,9},{9,8},{10,11... | collective-permute-start | bytes 196616 | tf_op jit(solution)/shard_map/ppermute | solution.py:20
  61.3 6.3 %collective-permute-start.23 = (bf16[16,2304]{1,0:T(8,128)(2,1)S(1)}, bf16[16,2304]{1,0:T(8,128)(2,1)S(1)}, u32[]{:S(2)}, u32[]{:S(2)}) collective-permute-start(bf16[16,2304]{1,0:T(8,128)(2,1)S(1)} %get-tuple-element.30), channel_id=1, source_target_pairs={{0,24},{4,28},{8,16},{12,20},{16,8},{20,12},{24,0},{28,4},{1,25},{... | collective-permute-start | bytes 221192 | tf_op jit(solution)/shard_map/ppermute | solution.py:20
  64.4 5.5 %collective-permute-start.21 = (bf16[16,2304]{1,0:T(8,128)(2,1)S(1)}, bf16[16,2304]{1,0:T(8,128)(2,1)S(1)}, u32[]{:S(2)}, u32[]{:S(2)}) collective-permute-start(bf16[16,2304]{1,0:T(8,128)(2,1)S(1)} %get-tuple-element.30), channel_id=1, source_target_pairs={{0,16},{4,20},{8,24},{12,28},{16,0},{20,4},{24,8},{28,12},{1,17},{... | collective-permute-start | bytes 221192 | tf_op jit(solution)/shard_map/ppermute | solution.py:20
  64.4 5.8 %collective-permute-start.19 = (bf16[16,2304]{1,0:T(8,128)(2,1)S(1)}, bf16[16,2304]{1,0:T(8,128)(2,1)S(1)}, u32[]{:S(2)}, u32[]{:S(2)}) collective-permute-start(bf16[16,2304]{1,0:T(8,128)(2,1)S(1)} %get-tuple-element.30), channel_id=1, source_target_pairs={{0,8},{4,12},{8,0},{12,4},{16,24},{20,28},{24,16},{28,20},{1,9},{5... | collective-permute-start | bytes 221192 | tf_op jit(solution)/shard_map/ppermute | solution.py:20
  65.7 4.8 %collective-permute-start.18 = (bf16[16,2304]{1,0:T(8,128)(2,1)S(1)}, bf16[16,2304]{1,0:T(8,128)(2,1)S(1)}, u32[]{:S(2)}, u32[]{:S(2)}) collective-permute-start(bf16[16,2304]{1,0:T(8,128)(2,1)S(1)} %get-tuple-element.30), channel_id=1, source_target_pairs={{0,4},{4,0},{8,12},{12,8},{16,20},{20,16},{24,28},{28,24},{1,5},{5... | collective-permute-start | bytes 221192 | tf_op jit(solution)/shard_map/ppermute | solution.py:20
  67.6 7.4 %collective-permute-start.26 = (bf16[256,1536]{1,0:T(8,128)(2,1)}, bf16[256,1536]{1,0:T(8,128)(2,1)S(1)}, u32[]{:S(2)}, u32[]{:S(2)}) collective-permute-start(bf16[256,1536]{1,0:T(8,128)(2,1)} %pad_maximum_fusion), channel_id=1, source_target_pairs={{0,4},{4,0},{8,12},{12,8},{16,20},{20,16},{24,28},{28,24},{1,5},{5... | collective-permute-start | bytes 2359304 | tf_op jit(solution)/shard_map/ppermute | solution.py:20
  69.9 1.8 %collective-permute-start.24 = (bf16[16,2304]{1,0:T(8,128)(2,1)S(1)}, bf16[16,2304]{1,0:T(8,128)(2,1)S(1)}, u32[]{:S(2)}, u32[]{:S(2)}) collective-permute-start(bf16[16,2304]{1,0:T(8,128)(2,1)S(1)} %collective-permute-done.23), channel_id=1, source_target_pairs={{0,4},{4,0},{8,12},{12,8},{16,20},{20,16},{24,28},{28,24},{1,5},{5... | collective-permute-start | bytes 221192 | tf_op jit(solution)/shard_map/ppermute | solution.py:20
  70.3 1.5 %collective-permute-start.22 = (bf16[16,2304]{1,0:T(8,128)(2,1)S(1)}, bf16[16,2304]{1,0:T(8,128)(2,1)S(1)}, u32[]{:S(2)}, u32[]{:S(2)}) collective-permute-start(bf16[16,2304]{1,0:T(8,128)(2,1)S(1)} %collective-permute-done.21), channel_id=1, source_target_pairs={{0,4},{4,0},{8,12},{12,8},{16,20},{20,16},{24,28},{28,24},{1,5},{5... | collective-permute-start | bytes 221192 | tf_op jit(solution)/shard_map/ppermute | solution.py:20
  70.5 1.3 %collective-permute-start.20 = (bf16[16,2304]{1,0:T(8,128)(2,1)S(1)}, bf16[16,2304]{1,0:T(8,128)(2,1)S(1)}, u32[]{:S(2)}, u32[]{:S(2)}) collective-permute-start(bf16[16,2304]{1,0:T(8,128)(2,1)S(1)} %collective-permute-done.19), channel_id=1, source_target_pairs={{0,4},{4,0},{8,12},{12,8},{16,20},{20,16},{24,28},{28,24},{1,5},{5... | collective-permute-start | bytes 221192 | tf_op jit(solution)/shard_map/ppermute | solution.py:20
  74.6 4.2 %copy-start.17 = (bf16[1,2048,896]{2,1,0:T(8,128)(2,1)S(1)}, bf16[1,2048,896]{2,1,0:T(8,128)(2,1)}, u32[]{:S(2)}) copy-start(bf16[1,2048,896]{2,1,0:T(8,128)(2,1)} %param.32) | copy-start | bytes 11010052
  75.3 17.1 %copy-start.13 = (bf16[1,896,2048]{2,1,0:T(8,128)(2,1)S(1)}, bf16[1,896,2048]{2,1,0:T(8,128)(2,1)}, u32[]{:S(2)}) copy-start(bf16[1,896,2048]{2,1,0:T(8,128)(2,1)} %param.33) | copy-start | bytes 11010052
  75.3 5.1 %collective-permute-start.27 = (bf16[32,1536]{1,0:T(8,128)(2,1)S(1)}, bf16[32,1536]{1,0:T(8,128)(2,1)S(1)}, u32[]{:S(2)}, u32[]{:S(2)}) collective-permute-start(bf16[32,1536]{1,0:T(8,128)(2,1)S(1)} %get-tuple-element.44), channel_id=1, source_target_pairs={{0,8},{4,12},{8,0},{12,4},{16,24},{20,28},{24,16},{28,20},{1,9},{5... | collective-permute-start | bytes 294920 | tf_op jit(solution)/shard_map/ppermute | solution.py:20
  75.9 8.1 %collective-permute-start.29 = (bf16[32,1536]{1,0:T(8,128)(2,1)S(1)}, bf16[32,1536]{1,0:T(8,128)(2,1)S(1)}, u32[]{:S(2)}, u32[]{:S(2)}) collective-permute-start(bf16[32,1536]{1,0:T(8,128)(2,1)S(1)} %get-tuple-element.45), channel_id=1, source_target_pairs={{0,24},{4,28},{8,16},{12,20},{16,8},{20,12},{24,0},{28,4},{1,25},{... | collective-permute-start | bytes 294920 | tf_op jit(solution)/shard_map/ppermute | solution.py:20
  78.2 9.7 %collective-permute-start.28 = (bf16[32,1536]{1,0:T(8,128)(2,1)S(1)}, bf16[32,1536]{1,0:T(8,128)(2,1)S(1)}, u32[]{:S(2)}, u32[]{:S(2)}) collective-permute-start(bf16[32,1536]{1,0:T(8,128)(2,1)S(1)} %get-tuple-element.46), channel_id=1, source_target_pairs={{0,16},{4,20},{8,24},{12,28},{16,0},{20,4},{24,8},{28,12},{1,17},{... | collective-permute-start | bytes 294920 | tf_op jit(solution)/shard_map/ppermute | solution.py:20
  87.9 6.0 %collective-permute-start.32 = (bf16[32,768]{1,0:T(8,128)(2,1)S(1)}, bf16[32,768]{1,0:T(8,128)(2,1)S(1)}, u32[]{:S(2)}, u32[]{:S(2)}) collective-permute-start(bf16[32,768]{1,0:T(8,128)(2,1)S(1)} %fusion.21.refs_4_), channel_id=1, source_target_pairs={{0,24},{4,28},{8,16},{12,20},{16,8},{20,12},{24,0},{28,4},{1,25},{... | collective-permute-start | bytes 147464 | tf_op jit(solution)/shard_map/ppermute | solution.py:20
  90.2 5.2 %collective-permute-start.31 = (bf16[32,768]{1,0:T(8,128)(2,1)S(1)}, bf16[32,768]{1,0:T(8,128)(2,1)S(1)}, u32[]{:S(2)}, u32[]{:S(2)}) collective-permute-start(bf16[32,768]{1,0:T(8,128)(2,1)S(1)} %fusion.21.refs_4_), channel_id=1, source_target_pairs={{0,16},{4,20},{8,24},{12,28},{16,0},{20,4},{24,8},{28,12},{1,17},{... | collective-permute-start | bytes 147464 | tf_op jit(solution)/shard_map/ppermute | solution.py:20
  90.2 5.2 %collective-permute-start.30 = (bf16[32,768]{1,0:T(8,128)(2,1)S(1)}, bf16[32,768]{1,0:T(8,128)(2,1)S(1)}, u32[]{:S(2)}, u32[]{:S(2)}) collective-permute-start(bf16[32,768]{1,0:T(8,128)(2,1)S(1)} %fusion.21.refs_4_), channel_id=1, source_target_pairs={{0,8},{4,12},{8,0},{12,4},{16,24},{20,28},{24,16},{28,20},{1,9},{5... | collective-permute-start | bytes 147464 | tf_op jit(solution)/shard_map/ppermute | solution.py:20
  92.4 18.0 %copy-start.1 = (f32[16,4,128,128]{3,2,1,0:T(8,128)S(1)}, f32[16,4,128,128]{3,2,1,0:T(8,128)}, u32[]{:S(2)}) copy-start(f32[16,4,128,128]{3,2,1,0:T(8,128)} %state_ref.3) | copy-start | bytes 12582916
  95.6 1.6 %collective-permute-start.33 = (bf16[4,16,2048]{2,1,0:T(8,128)(2,1)S(1)}, bf16[4,16,2048]{2,1,0:T(8,128)(2,1)S(1)}, u32[]{:S(2)}, u32[]{:S(2)}) collective-permute-start(bf16[4,16,2048]{2,1,0:T(8,128)(2,1)S(1)} %get-tuple-element.32), channel_id=1, source_target_pairs={{0,4},{4,0},{8,12},{12,8},{16,20},{20,16},{24,28},{28,24},{1,5},{5... | collective-permute-start | bytes 786440 | tf_op jit(solution)/shard_map/ppermute | solution.py:20
  97.3 4.5 %collective-permute-start.34 = (bf16[16,2048]{1,0:T(8,128)(2,1)S(1)}, bf16[16,2048]{1,0:T(8,128)(2,1)S(1)}, u32[]{:S(2)}, u32[]{:S(2)}) collective-permute-start(bf16[16,2048]{1,0:T(8,128)(2,1)S(1)} %get-tuple-element.34), channel_id=1, source_target_pairs={{0,8},{4,12},{8,0},{12,4},{16,24},{20,28},{24,16},{28,20},{1,9},{5... | collective-permute-start | bytes 196616 | tf_op jit(solution)/shard_map/ppermute | solution.py:20
  98.5 8.3 %collective-permute-start.35 = (bf16[16,2048]{1,0:T(8,128)(2,1)S(1)}, bf16[16,2048]{1,0:T(8,128)(2,1)S(1)}, u32[]{:S(2)}, u32[]{:S(2)}) collective-permute-start(bf16[16,2048]{1,0:T(8,128)(2,1)S(1)} %get-tuple-element.35), channel_id=1, source_target_pairs={{0,16},{4,20},{8,24},{12,28},{16,0},{20,4},{24,8},{28,12},{1,17},{... | collective-permute-start | bytes 196616 | tf_op jit(solution)/shard_map/ppermute | solution.py:20
  99.9 6.9 %collective-permute-start.36 = (bf16[16,2048]{1,0:T(8,128)(2,1)S(1)}, bf16[16,2048]{1,0:T(8,128)(2,1)S(1)}, u32[]{:S(2)}, u32[]{:S(2)}) collective-permute-start(bf16[16,2048]{1,0:T(8,128)(2,1)S(1)} %get-tuple-element.36), channel_id=1, source_target_pairs={{0,24},{4,28},{8,16},{12,20},{16,8},{20,12},{24,0},{28,4},{1,25},{... | collective-permute-start | bytes 196616 | tf_op jit(solution)/shard_map/ppermute | solution.py:20
  106.8 8.7 %collective-permute-start.39 = (bf16[16,2048]{1,0:T(8,128)(2,1)S(1)}, bf16[16,2048]{1,0:T(8,128)(2,1)S(1)}, u32[]{:S(2)}, u32[]{:S(2)}) collective-permute-start(bf16[16,2048]{1,0:T(8,128)(2,1)S(1)} %add_convert_fusion.refs_2_), channel_id=1, source_target_pairs={{0,3},{1,2},{2,1},{3,0},{4,7},{5,6},{6,5},{7,4},{8,11},{9,10},{10,... | collective-permute-start | bytes 196616 | tf_op jit(solution)/shard_map/ppermute | solution.py:20
  108.4 7.1 %collective-permute-start.38 = (bf16[16,2048]{1,0:T(8,128)(2,1)S(1)}, bf16[16,2048]{1,0:T(8,128)(2,1)S(1)}, u32[]{:S(2)}, u32[]{:S(2)}) collective-permute-start(bf16[16,2048]{1,0:T(8,128)(2,1)S(1)} %add_convert_fusion.refs_2_), channel_id=1, source_target_pairs={{0,2},{1,3},{2,0},{3,1},{4,6},{5,7},{6,4},{7,5},{8,10},{9,11},{10,... | collective-permute-start | bytes 196616 | tf_op jit(solution)/shard_map/ppermute | solution.py:20
  109.8 5.7 %collective-permute-start.37 = (bf16[16,2048]{1,0:T(8,128)(2,1)S(1)}, bf16[16,2048]{1,0:T(8,128)(2,1)S(1)}, u32[]{:S(2)}, u32[]{:S(2)}) collective-permute-start(bf16[16,2048]{1,0:T(8,128)(2,1)S(1)} %add_convert_fusion.refs_2_), channel_id=1, source_target_pairs={{0,1},{1,0},{2,3},{3,2},{4,5},{5,4},{6,7},{7,6},{8,9},{9,8},{10,11... | collective-permute-start | bytes 196616 | tf_op jit(solution)/shard_map/ppermute | solution.py:20

commit v2 on v1

--- a/solution.py
+++ b/solution.py
@@ -34,10 +34,9 @@
     return [block] + [swap(block, "ep", s) for s in chip_steps()]
 
 
-def relative_gather(block):
+def pair_gather(block):
     even = chip_gather(block)
-    odd = [swap(item, "ep", 1) for item in even]
-    return jnp.stack([item for pair in zip(even, odd) for item in pair])
+    return [(item, swap(item, "ep", 1)) for item in even]
 
 
 def chip_send(parts):
@@ -70,6 +69,28 @@
 
 
 VMEM = pl.BlockSpec(memory_space=pltpu.VMEM)
+FAR = pl.BlockSpec(memory_space=pltpu.HBM)
+
+
+def far(*values):
+    return tuple(pltpu.with_memory_space_constraint(value, pltpu.HBM) for value in values)
+
+
+def near(values):
+    return [pltpu.with_memory_space_constraint(value, pltpu.VMEM) for value in values]
+
+
+def fetch(sources, targets, sems):
+    copies = [
+        pltpu.make_async_copy(source, target, sems.at[i])
+        for i, (source, target) in enumerate(zip(sources, targets))
+    ]
+    for copy in copies:
+        copy.start()
+    for copy in copies:
+        copy.wait()
+
+
 PARAMS = pltpu.CompilerParams(vmem_limit_bytes=16 << 20)
 
 
@@ -80,10 +101,11 @@
     )
 
 
-def front_kernel(tokens_ref, gains_ref, even_ref, odd_ref):
-    resid = tokens_ref[...].astype(F32)
+def front_kernel(tokens_in, gains_in, bound_in, gain_in, even_ref, odd_ref, tokens_ref, gains_ref, heads_ref, sems):
+    targets = (tokens_ref, gains_ref, heads_ref.at[0:1], heads_ref.at[1:2])
+    fetch((tokens_in, gains_in, bound_in, gain_in), targets, sems)
     chips, _, feats = even_ref.shape
-    scale = rms_scale(resid)
+    scale = rms_scale(tokens_ref[...].astype(F32))
     mine = lax.axis_index("ep")
     for j in range(2 * chips):
         cols = pl.ds(pl.multiple_of((mine ^ j) * feats, feats), feats)
@@ -91,7 +113,7 @@
         (odd_ref if j % 2 else even_ref)[j // 2] = piece.astype(BF16)
 
 
-def front(tokens, norm_gains, ep_size):
+def front(tokens, norm_gains, lower_bound, head_gain, ep_size):
     seqs, width = tokens.shape
     feats = width // ep_size
     if feats % 128:
@@ -101,9 +123,58 @@
             lax.dynamic_slice_in_dim(normed, (lax.axis_index("ep") ^ j) * feats, feats, 1)
             for j in range(ep_size)
         ]
-        return jnp.stack(pieces[::2]), jnp.stack(pieces[1::2])
-    shape = jax.ShapeDtypeStruct((ep_size // 2, seqs, width // ep_size), BF16)
-    return call(front_kernel, (shape, shape))(tokens, norm_gains)
+        head_rows = jnp.stack([lower_bound, head_gain])
+        return jnp.stack(pieces[::2]), jnp.stack(pieces[1::2]), tokens, norm_gains, head_rows
+    shape = jax.ShapeDtypeStruct((ep_size // 2, seqs, feats), BF16)
+    return pl.pallas_call(
+        front_kernel,
+        in_specs=[FAR] * 4,
+        out_shape=(
+            shape,
+            shape,
+            jax.ShapeDtypeStruct(tokens.shape, tokens.dtype),
+            jax.ShapeDtypeStruct(norm_gains.shape, F32),
+            jax.ShapeDtypeStruct((2, lower_bound.shape[0]), F32),
+        ),
+        scratch_shapes=[pltpu.SemaphoreType.DMA((4,))],
+        compiler_params=PARAMS,
+        name="front",
+    )(*far(tokens, norm_gains, lower_bound[None], head_gain[None]))
+
+
+def table_kernel(routes_in, scores_in, gate_in, table_ref, gate_ref, routes_ref, scores_ref, sems):
+    fetch((routes_in, scores_in, gate_in), (routes_ref, scores_ref, gate_ref), sems)
+    seqs = table_ref.shape[0]
+    place = lax.broadcasted_iota(jnp.int32, table_ref.shape, 1)
+    across = lax.broadcasted_iota(jnp.int32, (seqs, seqs), 1)
+    diagonal = across == lax.broadcasted_iota(jnp.int32, (seqs, seqs), 0)
+
+    def upright(row):
+        return jnp.sum(jnp.where(diagonal, row, 0.0), axis=1, keepdims=True)
+
+    table = jnp.zeros(table_ref.shape, F32)
+    for k in range(2):
+        margin = scores_ref[k : k + 1, :] - scores_ref[1 - k : 2 - k, :]
+        expert = upright(routes_ref[k : k + 1, :].astype(F32)).astype(jnp.int32)
+        table = jnp.where(place == expert, upright(jax.nn.sigmoid(margin)), table)
+    table_ref[...] = table
+
+
+def route_table(routes, route_scores, dense_mix, lanes):
+    shape = jax.ShapeDtypeStruct((routes.shape[0], lanes), F32)
+    gate = dense_mix.reshape(-1, 128)
+    shapes = (shape, jax.ShapeDtypeStruct(gate.shape, gate.dtype))
+    operands = (routes.T, route_scores.T, gate)
+    return pl.pallas_call(
+        table_kernel,
+        in_specs=[FAR] * 3,
+        out_shape=shapes,
+        scratch_shapes=[pltpu.VMEM(x.shape, x.dtype) for x in operands[:2]]
+        + [pltpu.SemaphoreType.DMA((3,))],
+        compiler_params=PARAMS,
+        cost_estimate=pl.CostEstimate(flops=1 << 34, bytes_accessed=1 << 20, transcendentals=0),
+        name="table",
+    )(*far(*operands))
 
 
 def project_kernel(pairs, *refs):
@@ -160,7 +231,7 @@
     return call(mix_kernel, jax.ShapeDtypeStruct(shape, BF16))(mixed_heads, *weights)
 
 
-def middle_kernel(parts, tokens_ref, gains_ref, gate_ref, routes_ref, scores_ref, *refs):
+def middle_kernel(parts, tokens_ref, gains_ref, gate_ref, table_ref, *refs):
     pieces, (after_ref, packed_ref) = refs[:parts], refs[parts:]
     seqs, width = tokens_ref.shape
     ep_size = lax.axis_size("ep")
@@ -177,13 +248,14 @@
     after_ref[...] = after_mix
     ffn_in = (after_mix * rms_scale(after_mix) * gains_ref[2:3]).astype(BF16)
     packed_ref[:, :width] = ffn_in
-    dots = jnp.sum(ffn_in.astype(F32) * gate_ref[...].astype(F32), axis=1, keepdims=True)
-    lanes = (packed_ref.shape[1] - width) // 2
+    lanes = table_ref.shape[1]
+    products = jnp.zeros((seqs, 128), F32)
+    for j in range(width // 128):
+        piece = packed_ref[:, j * 128 : (j + 1) * 128].astype(F32)
+        products = products + piece * gate_ref[j : j + 1, :].astype(F32)
+    dots = jnp.sum(products, axis=1, keepdims=True)
     place = lax.broadcasted_iota(jnp.int32, (seqs, lanes), 1)
-    extra = jnp.where(place == ep_size, jax.nn.sigmoid(dots), 0.0)
-    for k in range(2):
-        margin = scores_ref[:, k : k + 1] - scores_ref[:, 1 - k : 2 - k]
-        extra = jnp.where(place == routes_ref[:, k : k + 1], jax.nn.sigmoid(margin), extra)
+    extra = jnp.where(place == ep_size, jax.nn.sigmoid(dots), table_ref[...])
     high = extra.astype(BF16)
     packed_ref[:, width : width + lanes] = high
     packed_ref[:, width + lanes :] = (extra - high.astype(F32)).astype(BF16)
@@ -196,85 +268,125 @@
     return jnp.take(values, order, axis=1).reshape(rows, width)
 
 
-def plain_middle(tokens, norm_gains, dense_mix, routes, route_scores, lanes, pieces):
+def plain_middle(tokens, norm_gains, dense_mix, table, pieces):
     ep_size = lax.axis_size("ep")
     total = total_of(pieces[0].astype(F32), pieces[1:])
     mix_wide = to_absolute(total.astype(BF16).astype(F32), lax.axis_index("ep"), ep_size)
     after_mix = tokens.astype(F32) + mix_wide * rms_scale(mix_wide) * norm_gains[1]
     ffn_in = (after_mix * rms_scale(after_mix) * norm_gains[2]).astype(BF16)
-    dots = jnp.sum(ffn_in.astype(F32) * dense_mix.astype(F32), axis=1, keepdims=True)
-    place = jnp.arange(lanes, dtype=jnp.int32)[None]
-    extra = jnp.where(place == ep_size, jax.nn.sigmoid(dots), 0.0)
-    for k in range(2):
-        margin = route_scores[:, k : k + 1] - route_scores[:, 1 - k : 2 - k]
-        extra = jnp.where(place == routes[:, k : k + 1], jax.nn.sigmoid(margin), extra)
+    dots = jnp.sum(ffn_in.astype(F32) * dense_mix.reshape(1, -1).astype(F32), axis=1, keepdims=True)
+    place = jnp.arange(table.shape[1], dtype=jnp.int32)[None]
+    extra = jnp.where(place == ep_size, jax.nn.sigmoid(dots), table)
     high = extra.astype(BF16)
     low = (extra - high.astype(F32)).astype(BF16)
     return after_mix, jnp.concatenate([ffn_in, high, low], axis=1)
 
 
-def middle(tokens, norm_gains, dense_mix, routes, route_scores, lanes, pieces):
+def middle(tokens, norm_gains, dense_mix, table, pieces):
     seqs, width = tokens.shape
+    lanes = table.shape[1]
     if (width // lax.axis_size("ep")) % 128:
-        return plain_middle(tokens, norm_gains, dense_mix, routes, route_scores, lanes, pieces)
+        return plain_middle(tokens, norm_gains, dense_mix, table, pieces)
     return call(
         lambda *refs: middle_kernel(len(pieces), *refs),
         (
             jax.ShapeDtypeStruct((seqs, width), F32),
             jax.ShapeDtypeStruct((seqs, width + 2 * lanes), BF16),
         ),
-    )(tokens, norm_gains, dense_mix, routes, route_scores, *pieces)
-
-
-def join_kernel(chips, expert_ref, scale_ref, own_ref, other_ref, *refs):
-    hidden, (keep_ref, send_ref) = refs[:chips], refs[chips:]
-    _, seqs, _ = keep_ref.shape
+    )(tokens, norm_gains, dense_mix, table, *near(pieces))
+
+
+def dense_kernel(feats, even_ref, odd_ref, *refs):
+    *weights, out_ref = refs
+    half = out_ref.shape[1] // 2
+    mine = lax.axis_index("ep")
+    units = pl.ds(pl.multiple_of((mine & 1) * half, half), half)
+
+    def features(index):
+        cols = pl.ds(pl.multiple_of(index * feats, feats), feats)
+        return jnp.concatenate([even_ref[:, cols], odd_ref[:, cols]], axis=0)
+
+    own, other = features(mine), features(mine ^ 1)
+    for k in range(2):
+        part = jnp.dot(own, weights[k][:, units], preferred_element_type=F32) + jnp.dot(
+            other, weights[2 + k][:, units], preferred_element_type=F32
+        )
+        out_ref[:, k * half : (k + 1) * half] = part.astype(out_ref.dtype)
+
+
+def dense_part(even, odd, weights, dtype):
+    feats, units = weights[0].shape
+    half = units // 2
+    if half % 128 or feats % 128:
+        mine = lax.axis_index("ep")
+        rows = jnp.concatenate([even, odd], axis=0)
+        own, other = (
+            lax.dynamic_slice_in_dim(rows, index * feats, feats, 1) for index in (mine, mine ^ 1)
+        )
+        picked = [lax.dynamic_slice_in_dim(w, (mine & 1) * half, half, 1) for w in weights]
+        parts = [
+            jnp.dot(own, picked[k], preferred_element_type=F32)
+            + jnp.dot(other, picked[2 + k], preferred_element_type=F32)
+            for k in range(2)
+        ]
+        return jnp.concatenate(parts, axis=1).astype(dtype)
+    return call(
+        lambda *refs: dense_kernel(feats, *refs),
+        jax.ShapeDtypeStruct((2 * even.shape[0], units), dtype),
+    )(even, odd, *weights)
+
+
+def join_kernel(first, expert_ref, scale_ref, own_ref, other_ref, hidden_ref, keep_ref, send_ref):
+    seqs = keep_ref.shape[0]
+    half = own_ref.shape[0] // 2
     feats = own_ref.shape[1]
     mine = lax.axis_index("ep")
-    for s in range(chips):
-        rows = 2 * seqs * s
-        keep_ref[s] = expert_ref[rows : rows + seqs]
-    everything = jnp.concatenate([ref[...] for ref in hidden], axis=0)
-    scale = scale_ref[...]
-    placed = []
+    units = pl.ds(pl.multiple_of((mine & 1) * half, half), half)
+    rows = slice(first, first + seqs)
+    others = slice(first + seqs, first + 2 * seqs)
+    keep_ref[...] = expert_ref[rows]
+    send_ref[...] = expert_ref[others].astype(BF16)
+    scale = scale_ref[first : first + 2 * seqs]
     for weights, column in ((own_ref, mine), (other_ref, mine ^ 1)):
-        dense = jnp.dot(everything, weights[...], preferred_element_type=F32) * scale
+        dense = jnp.dot(hidden_ref[...], weights[units, :], preferred_element_type=F32) * scale
         cols = pl.ds(pl.multiple_of(column * feats, feats), feats)
-        placed.append((cols, dense))
-        for s in range(chips):
-            rows = 2 * seqs * s
-            keep_ref[s, :, cols] += dense[rows : rows + seqs]
-    for s in range(chips):
-        rows = 2 * seqs * s + seqs
-        send_ref[s] = expert_ref[rows : rows + seqs].astype(BF16)
-        for cols, dense in placed:
-            value = expert_ref[rows : rows + seqs, cols] + dense[rows : rows + seqs]
-            send_ref[s, :, cols] = value.astype(BF16)
-
-
-def plain_join(expert_out, scale, down_own, down_other, hidden, seqs):
+        keep_ref[:, cols] += dense[:seqs]
+        send_ref[:, cols] = (expert_ref[others, cols] + dense[seqs:]).astype(BF16)
+
+
+def plain_join(rows, scale, down_own, down_other, hidden, seqs):
     ep_size = lax.axis_size("ep")
     mine = lax.axis_index("ep")
-    everything = jnp.concatenate(hidden, axis=0)
-    rows, width = expert_out.shape
-    total = expert_out.reshape(rows, ep_size, width // ep_size)
+    count, width = rows.shape
+    total = rows.reshape(count, ep_size, width // ep_size)
     column = jnp.arange(ep_size, dtype=jnp.int32)[None, :, None]
     for weights, place in ((down_own, mine), (down_other, mine ^ 1)):
-        dense = jnp.dot(everything, weights, preferred_element_type=F32) * scale
+        half = weights.shape[0] // 2
+        picked = lax.dynamic_slice_in_dim(weights, (mine & 1) * half, half, 0)
+        dense = jnp.dot(hidden, picked, preferred_element_type=F32) * scale
         total = total + jnp.where(column == place, dense[:, None, :], 0.0)
-    total = total.reshape(len(hidden), 2, seqs, width)
-    return total[:, 0], total[:, 1].astype(BF16)
-
-
-def join(expert_out, scale, down_own, down_other, hidden, seqs):
-    chips, width = len(hidden), expert_out.shape[1]
-    shape = (chips, seqs, width)
+    total = total.reshape(count, width)
+    return total[:seqs], total[seqs:].astype(BF16)
+
+
+def join(expert_out, scale, down_own, down_other, hidden, chip, seqs):
+    first = 2 * seqs * chip
     if down_own.shape[1] % 128:
-        return plain_join(expert_out, scale, down_own, down_other, hidden, seqs)
+        rows = slice(first, first + 2 * seqs)
+        return plain_join(expert_out[rows], scale[rows], down_own, down_other, hidden, seqs)
+    shape = (seqs, expert_out.shape[1])
     return call(
-        lambda *refs: join_kernel(chips, *refs),
+        lambda *refs: join_kernel(first, *refs),
         (jax.ShapeDtypeStruct(shape, F32), jax.ShapeDtypeStruct(shape, BF16)),
-    )(expert_out, scale, down_own, down_other, *hidden)
+    )(expert_out, scale, down_own, down_other, hidden)
+
+
+def core_sum_kernel(keep_ref, crossed_ref, out_ref):
+    out_ref[...] = (keep_ref[...] + crossed_ref[...].astype(F32)).astype(out_ref.dtype)
+
+
+def core_sum(keep, crossed, dtype):
+    return call(core_sum_kernel, jax.ShapeDtypeStruct(keep.shape, dtype))(keep, crossed)
 
 
 def finish_kernel(parts, after_ref, gains_ref, *refs):
@@ -296,7 +408,7 @@
     return call(
         lambda *refs: finish_kernel(len(pieces), *refs),
         jax.ShapeDtypeStruct((seqs, width // lax.axis_size("tp")), BF16),
-    )(after_mix, norm_gains, *pieces)
+    )(*near([after_mix, norm_gains, *pieces]))
 
 
 def broadcast_column(columns, index, size):
@@ -305,7 +417,7 @@
 
 def read_kernel(arrived, *refs):
     own_ref, recv = refs[0], refs[1 : 1 + arrived]
-    bound_ref, gain_ref, state_ref, mixed_ref, gates_ref = refs[1 + arrived :]
+    rows_ref, state_ref, mixed_ref, gates_ref = refs[1 + arrived :]
     seqs, heads, size, _ = state_ref.shape
     local = heads * size
 
@@ -319,7 +431,7 @@
     for head in range(heads):
         query_raw, forget_raw, value, out_gate = (column(kind, head) for kind in range(4))
         span = slice(head * size, (head + 1) * size)
-        bound = bound_ref[:, span]
+        bound = rows_ref[0:1, span]
         forget = bound + (1.0 - bound) * jax.nn.sigmoid(forget_raw)
         key_in = (1.0 - bound) * jax.nn.sigmoid(-forget_raw)
         query = query_raw * jax.nn.sigmoid(query_raw)
@@ -335,11 +447,11 @@
         ]
         read = jnp.concatenate(rows, axis=0)
         read = read + jnp.sum(query * key_in, axis=1, keepdims=True) * value
-        gated = read * rms_scale(read) * gain_ref[:, span]
+        gated = read * rms_scale(read) * rows_ref[1:2, span]
         mixed_ref[:, span] = (gated * (out_gate * jax.nn.sigmoid(out_gate))).astype(BF16)
 
 
-def read_heads(own, arrived, lower_bound, head_gain, old_state):
+def read_heads(own, arrived, head_rows, old_state):
     seqs, heads, size, _ = old_state.shape
     return call(
         lambda *refs: read_kernel(len(arrived), *refs),
@@ -347,7 +459,7 @@
             jax.ShapeDtypeStruct((seqs, heads * size), BF16),
             jax.ShapeDtypeStruct((3, seqs, heads * size), F32),
         ),
-    )(own, *arrived, lower_bound[None], head_gain[None], old_state)
+    )(*near([own, *arrived, head_rows]), old_state)
 
 
 def state_kernel(gates_ref, state_ref, *refs):
@@ -379,7 +491,7 @@
             flops=4 * old_state.size, bytes_accessed=8 * old_state.size, transcendentals=0
         ),
         name="write_state",
-    )(gates, old_state, *more)
+    )(gates, *(far(old_state) if partial is None else (old_state,)), *more)
 
 
 def body(
@@ -405,37 +517,25 @@
 ):
     seqs, width = tokens.shape
     ep_index = lax.axis_index("ep")
-    core_index = ep_index & 1
     ep_size = lax.axis_size("ep")
-    chips = ep_size // 2
-    feats = width // ep_size
-    all_rows = ep_size * seqs
 
     mix_weights = background_gather(w_mix_out)
 
-    half_ff = w_dense_gate.shape[1] // 2
-
-    def half(weights, axis, which):
-        return lax.dynamic_slice_in_dim(weights, which * half_ff, half_ff, axis)
-
-    other_core = 1 - core_index
-    pair = (w_dense_gate, w_dense_up)
-    gate_up_out = jnp.concatenate([half(w, 1, other_core) for w in pair], axis=1)
-    down_out = half(w_dense_down, 0, other_core)
-    gate_up_own = jnp.concatenate([half(w, 1, core_index) for w in pair], axis=1)
-    down_own = half(w_dense_down, 0, core_index)
-    gate_row = dense_mix.reshape(1, width)
-    gate_up_other = swap(gate_up_out, "ep", 1)
-    down_other = swap(down_out, "ep", 1)
-
+    dense_weights = (w_dense_gate, w_dense_up) + tuple(
+        swap(w, "ep", 1) for w in (w_dense_gate, w_dense_up)
+    )
+    down_other = swap(w_dense_down, "ep", 1)
     lanes = -(-(ep_size + 1) // 128) * 128
 
-    even, odd = front(tokens, norm_gains, ep_size)
+    table, gate = route_table(routes, route_scores, dense_mix, lanes)
+    even, odd, tokens, norm_gains, head_rows = front(
+        tokens, norm_gains, lower_bound, head_gain, ep_size
+    )
     row_pairs = relative_exchange(even, odd)
     keep, send = project(row_pairs, (w_query, w_forget, w_value, w_outgate))
     own, sends = chip_sum(keep, swap(send, "ep", 1))
     arrived = chip_send(sends)
-    mixed_heads, gates = read_heads(own, arrived, lower_bound, head_gain, old_state)
+    mixed_heads, gates = read_heads(own, arrived, head_rows, old_state)
     heads = old_state.shape[1]
     early = -(-heads // 2)
     new_state = write_state(gates, old_state, 0, early)
@@ -443,25 +543,20 @@
         new_state = write_state(gates, old_state, early, heads - early, new_state)
     mix_part = mix_heads(mixed_heads, mix_weights)
     mix_pieces = [mix_part] + tp_exchange(mix_part)
-    after_mix, packed = middle(
-        tokens, norm_gains, gate_row, routes, route_scores, lanes, mix_pieces
-    )
-
-    gathered = relative_gather(packed).reshape(all_rows, packed.shape[1])
+    after_mix, packed = middle(tokens, norm_gains, gate, table, mix_pieces)
+
+    row_pairs = pair_gather(packed)
+    dense_parts = []
+    for s, (even, odd) in enumerate(row_pairs):
+        dense_parts.append(dense_part(even, odd, dense_weights, BF16 if s else F32))
+    dense_pre = total_of(dense_parts[0], chip_send(dense_parts[1:]))
+
+    gathered = jnp.concatenate([item for pair in row_pairs for item in pair], axis=0)
     rows = gathered[:, :width]
     side = gathered[:, width : width + lanes].astype(F32) + gathered[:, width + lanes :].astype(F32)
     expert_scale = lax.dynamic_slice_in_dim(side, ep_index, 1, 1)
     dense_scale = side[:, ep_size : ep_size + 1]
 
-    def features(index):
-        return lax.dynamic_slice_in_dim(rows, index * feats, feats, 1)
-
-    dense_part = jnp.dot(features(ep_index), gate_up_own, preferred_element_type=F32) + jnp.dot(
-        features(ep_index ^ 1), gate_up_other, preferred_element_type=F32
-    )
-    dense_part = dense_part.reshape(chips, 2 * seqs, -1)
-    dense_sent = dense_part[1:].astype(BF16)
-    dense_pre = total_of(dense_part[0], chip_send(list(dense_sent)))
     dense_gate_pre, dense_up_pre = jnp.split(dense_pre, 2, axis=1)
     dense_hidden = (jax.nn.silu(dense_gate_pre) * dense_up_pre).astype(BF16)
     all_hidden = chip_gather(dense_hidden)
@@ -473,9 +568,13 @@
     hidden = lax.optimization_barrier(hidden)
     expert_out = jnp.dot(hidden, w_exp_down[0], preferred_element_type=F32) * expert_scale
     expert_out = lax.optimization_barrier(expert_out)
-    keep, send = join(expert_out, dense_scale, down_own, down_other, all_hidden, seqs)
-    own, sends = chip_sum(keep, swap(send, "ep", 1))
-    ffn_part = total_of(own, chip_send(sends)).astype(BF16)
+    sums = []
+    for chip, hidden_rows in enumerate(all_hidden):
+        keep, send = join(
+            expert_out, dense_scale, w_dense_down, down_other, hidden_rows, chip, seqs
+        )
+        sums.append(core_sum(keep, swap(send, "ep", 1), BF16 if chip else F32))
+    ffn_part = total_of(sums[0], chip_send(sums[1:])).astype(BF16)
     ffn_pieces = [ffn_part] + tp_exchange(ffn_part)
     return (finish(after_mix, norm_gains, ffn_pieces), new_state)
 

time: 117 us -> 122 us (1.043)
  Pallas kernels: 10 us -> 20.7 us
  matrix products: 4.78 us -> 2.17 us
  local copies, waits for them, and re-layouts: 8.55 us -> 6.27 us
  waiting for transfers between devices: 48.7 us -> 50.9 us
  starting transfers between devices: 42.1 us -> 40.6 us
    pallas_call x2 -> x14, Pallas kernels: 0.4 us -> 9.12 us  [the longest x4 6.13 us: dense_part(): call(lambda *refs: dense_kernel(feats, *refs), jax.ShapeDtypeStruct((2 *...]
    dynamic_slice x2 -> x0, local copies, waits for them, and re-layouts: 2.62 us -> none  [half(): return lax.dynamic_slice_in_dim(weights, which * half_ff, half_ff, axis)]
    ppermute x40 -> x44, waiting for transfers between devices: 48.7 us -> 50.9 us  [swap(): return lax.ppermute(value, axis, [(i, i ^ step) for i in range(size)])]
    dot_general x1, matrix products: 2.76 us -> 0.71 us  [body(): gate_pre = jnp.dot(rows, w_exp_gate[0], preferred_element_type=F32)]
    ppermute x40 -> x44, starting transfers between devices: 42.1 us -> 40.6 us  [swap(): return lax.ppermute(value, axis, [(i, i ^ step) for i in range(size)])]
    pallas_call x2, Pallas kernels: 5.14 us -> 6.36 us  [write_state(): pl.pallas_call(state_kernel, grid=(count,), in_specs=[pl.BlockSpec((3, se...]
    unnamed x45 -> x33, local copies, waits for them, and re-layouts: 5.67 us -> 6.08 us
  transfers between devices with their start and end apart: 40 -> 44, of which waited for: 22 -> 17; matrix products, arithmetic and copies ran while one was open for 8% -> 2% of each run, Pallas kernels for 8% -> 16%
where the time goes in v2:
time: 122 us
  waiting for transfers between devices  50.9 us (42%)
  starting transfers between devices  40.6 us (33%)
  Pallas kernels  20.7 us (17%)
  local copies, waits for them, and re-layouts  6.27 us (5%)
  matrix products  2.17 us (2%)
    ppermute x44, waiting for transfers between devices, swap(): return lax.ppermute(value, axis, [(i, i ^ step) for i in range(size)])  50.9 us
    ppermute x44, starting transfers between devices, swap(): return lax.ppermute(value, axis, [(i, i ^ step) for i in range(size)])  40.6 us
    pallas_call x2, Pallas kernels, write_state(): pl.pallas_call(state_kernel, grid=(count,), in_specs=[pl.BlockSpec((3, se...  6.36 us
    pallas_call x4, Pallas kernels, dense_part(): call(lambda *refs: dense_kernel(feats, *refs), jax.ShapeDtypeStruct((2 *...  6.13 us
    unnamed x33, local copies, waits for them, and re-layouts  6.08 us
    pallas_call x1, Pallas kernels, read_heads(): call(lambda *refs: read_kernel(len(arrived), *refs), (jax.ShapeDtypeStruc...  2.54 us
  transfers between devices with their start and end apart: 44, of which 17 were waited for; matrix products, arithmetic and copies ran while one was open for 2% of the time, Pallas kernels for 16%

profile of v2, /device:TPU:0, one launch (start us, length us, event | category | flops | bytes accessed | tf_op | source)
XLA Modules:
  0.0 121.8 jit_solution(3546599436816505994)
XLA Ops:
  0.6 4.1 %collective-permute-start.11 = (bf16[512,256]{1,0:T(8,128)(2,1)}, bf16[512,256]{1,0:T(8,128)(2,1)S(1)}, u32[]{:S(2)}, u32[]{:S(2)}) collective-permute-start(bf16[512,256]{1,0:T(8,128)(2,1)} %refs_0_.1), channel_id=1, source_target_pairs={{0,16},{4,20},{8,24},{12,28},{16,0},{20,4},{24,8},{28,12},{1,17},{... | collective-permute-start | bytes 786440 | tf_op jit(solution)/shard_map/ppermute | solution.py:20
  4.8 1.0 front.1
  5.9 1.6 %collective-permute-start.9 = (bf16[512,256]{1,0:T(8,128)(2,1)}, bf16[512,256]{1,0:T(8,128)(2,1)S(1)}, u32[]{:S(2)}, u32[]{:S(2)}) collective-permute-start(bf16[512,256]{1,0:T(8,128)(2,1)} %refs_0_.1), channel_id=1, source_target_pairs={{0,8},{4,12},{8,0},{12,4},{16,24},{20,28},{24,16},{28,20},{1,9},{5... | collective-permute-start | bytes 786440 | tf_op jit(solution)/shard_map/ppermute | solution.py:20
  7.5 9.5 %collective-permute-done.11.refs_4_ = bf16[512,256]{1,0:T(8,128)(2,1)S(1)} collective-permute-done((bf16[512,256]{1,0:T(8,128)(2,1)}, bf16[512,256]{1,0:T(8,128)(2,1)S(1)}, u32[]{:S(2)}, u32[]{:S(2)}) %collective-permute-start.11) | collective-permute-done | bytes 262176 | tf_op jit(solution)/shard_map/ppermute | solution.py:20
  17.0 0.8 collective-permute-start.13
  17.8 2.8 %collective-permute-start.3 = (bf16[2,16,256]{2,1,0:T(8,128)(2,1)S(1)}, bf16[2,16,256]{2,1,0:T(8,128)(2,1)S(1)}, u32[]{:S(2)}, u32[]{:S(2)}) collective-permute-start(bf16[2,16,256]{2,1,0:T(8,128)(2,1)S(1)} %get-tuple-element.54), channel_id=1, source_target_pairs={{0,24},{4,28},{8,16},{12,20},{16,8},{20,12},{24,0},{28,4},{1,25},{... | collective-permute-start | bytes 49160 | tf_op jit(solution)/shard_map/ppermute | solution.py:20
  20.6 1.1 collective-permute-start.1
  21.8 0.5 collective-permute-start.2
  22.2 5.4 %collective-permute-done.3.refs_3_ = bf16[2,16,256]{2,1,0:T(8,128)(2,1)S(1)} collective-permute-done((bf16[2,16,256]{2,1,0:T(8,128)(2,1)S(1)}, bf16[2,16,256]{2,1,0:T(8,128)(2,1)S(1)}, u32[]{:S(2)}, u32[]{:S(2)}) %collective-permute-start.3) | collective-permute-done | bytes 16416 | tf_op jit(solution)/shard_map/ppermute | solution.py:20
  27.7 0.9 copy-done.5
  28.6 0.9 copy-done.6
  29.6 0.9 copy-done.7
  30.5 0.9 copy-done.8
  31.9 0.5 collective-permute-start.8
  32.5 0.4 collective-permute-start.10
  33.0 0.4 collective-permute-done.4.crossed_ref
  33.4 1.0 collective-permute-start.5
  34.4 3.4 %collective-permute-done.5.refs_1_ = bf16[16,2048]{1,0:T(8,128)(2,1)S(1)} collective-permute-done((bf16[16,2048]{1,0:T(8,128)(2,1)S(1)}, bf16[16,2048]{1,0:T(8,128)(2,1)S(1)}, u32[]{:S(2)}, u32[]{:S(2)}) %collective-permute-start.5) | collective-permute-done | bytes 65568 | tf_op jit(solution)/shard_map/ppermute | solution.py:20
  37.8 0.8 collective-permute-start.6
  38.6 5.1 %collective-permute-done.6.refs_2_ = bf16[16,2048]{1,0:T(8,128)(2,1)S(1)} collective-permute-done((bf16[16,2048]{1,0:T(8,128)(2,1)S(1)}, bf16[16,2048]{1,0:T(8,128)(2,1)S(1)}, u32[]{:S(2)}, u32[]{:S(2)}) %collective-permute-start.6) | collective-permute-done | bytes 65568 | tf_op jit(solution)/shard_map/ppermute | solution.py:20
  43.6 1.7 %collective-permute-start.7 = (bf16[16,2048]{1,0:T(8,128)(2,1)S(1)}, bf16[16,2048]{1,0:T(8,128)(2,1)S(1)}, u32[]{:S(2)}, u32[]{:S(2)}) collective-permute-start(bf16[16,2048]{1,0:T(8,128)(2,1)S(1)} %get-tuple-element.38), channel_id=1, source_target_pairs={{0,24},{4,28},{8,16},{12,20},{16,8},{20,12},{24,0},{28,4},{1,25},{... | collective-permute-start | bytes 196616 | tf_op jit(solution)/shard_map/ppermute | solution.py:20
  45.3 4.4 %collective-permute-done.7.refs_3_ = bf16[16,2048]{1,0:T(8,128)(2,1)S(1)} collective-permute-done((bf16[16,2048]{1,0:T(8,128)(2,1)S(1)}, bf16[16,2048]{1,0:T(8,128)(2,1)S(1)}, u32[]{:S(2)}, u32[]{:S(2)}) %collective-permute-start.7) | collective-permute-done | bytes 65568 | tf_op jit(solution)/shard_map/ppermute | solution.py:20
  49.7 2.2 %copy-done = f32[16,4,128,128]{3,2,1,0:T(8,128)S(1)} copy-done((f32[16,4,128,128]{3,2,1,0:T(8,128)S(1)}, f32[16,4,128,128]{3,2,1,0:T(8,128)}, u32[]{:S(2)}) %copy-start) | copy-done | bytes 4194328
  51.9 2.5 %shard_map.196 = (bf16[16,512]{1,0:T(8,128)(2,1)S(1)}, f32[3,16,512]{2,1,0:T(8,128)S(1)}) custom-call(f32[16,2048]{1,0:T(8,128)S(1)} %get-tuple-element.35.refs_0_, bf16[16,2048]{1,0:T(8,128)(2,1)S(1)} %collective-permute-done.5.refs_1_, bf16[16,2048]{1,0:T(8,128)(2,1)S(1)} %collective-permute-done.6.refs_2_, ...), custom_call_target="tpu_custom_call" | custom-call | flops 1048576 | bytes 1048576 | tf_op jit(solution)/shard_map/pallas_call | solution.py:456
  54.5 0.6 collective-permute-start.27
  55.1 0.4 shard_map.197.refs_4_
  55.4 2.5 %collective-permute-start.17 = (bf16[16,2048]{1,0:T(8,128)(2,1)S(1)}, bf16[16,2048]{1,0:T(8,128)(2,1)S(1)}, u32[]{:S(2)}, u32[]{:S(2)}) collective-permute-start(bf16[16,2048]{1,0:T(8,128)(2,1)S(1)} %shard_map.197.refs_4_), channel_id=1, source_target_pairs={{0,3},{1,2},{2,1},{3,0},{4,7},{5,6},{6,5},{7,4},{8,11},{9,10},{10,... | collective-permute-start | bytes 196616 | tf_op jit(solution)/shard_map/ppermute | solution.py:20
  57.9 0.5 collective-permute-start.16
  58.4 0.5 collective-permute-start.15
  59.0 1.0 table.1
  59.9 0.7 collective-permute-done.17.refs_7_
  60.7 1.5 %collective-permute-done.16.refs_6_ = bf16[16,2048]{1,0:T(8,128)(2,1)S(1)} collective-permute-done((bf16[16,2048]{1,0:T(8,128)(2,1)S(1)}, bf16[16,2048]{1,0:T(8,128)(2,1)S(1)}, u32[]{:S(2)}, u32[]{:S(2)}) %collective-permute-start.16) | collective-permute-done | bytes 65568 | tf_op jit(solution)/shard_map/ppermute | solution.py:20
  62.2 0.6 collective-permute-done.15.refs_5_
  62.8 1.2 shard_map.198
  64.0 1.7 %collective-permute-start.23 = (bf16[16,2304]{1,0:T(8,128)(2,1)S(1)}, bf16[16,2304]{1,0:T(8,128)(2,1)S(1)}, u32[]{:S(2)}, u32[]{:S(2)}) collective-permute-start(bf16[16,2304]{1,0:T(8,128)(2,1)S(1)} %get-tuple-element.42.refs_0_), channel_id=1, source_target_pairs={{0,24},{4,28},{8,16},{12,20},{16,8},{20,12},{24,0},{28,4},{1,25},{... | collective-permute-start | bytes 221192 | tf_op jit(solution)/shard_map/ppermute | solution.py:20
  65.8 5.1 %collective-permute-done.19.refs_0_ = bf16[16,2304]{1,0:T(8,128)(2,1)S(1)} collective-permute-done((bf16[16,2304]{1,0:T(8,128)(2,1)S(1)}, bf16[16,2304]{1,0:T(8,128)(2,1)S(1)}, u32[]{:S(2)}, u32[]{:S(2)}) %collective-permute-start.19) | collective-permute-done | bytes 73760 | tf_op jit(solution)/shard_map/ppermute | solution.py:20
  70.9 0.7 collective-permute-start.21
  71.6 0.6 collective-permute-start.25
  72.3 4.1 %collective-permute-done.21.refs_0_ = bf16[16,2304]{1,0:T(8,128)(2,1)S(1)} collective-permute-done((bf16[16,2304]{1,0:T(8,128)(2,1)S(1)}, bf16[16,2304]{1,0:T(8,128)(2,1)S(1)}, u32[]{:S(2)}, u32[]{:S(2)}) %collective-permute-start.21) | collective-permute-done | bytes 73760 | tf_op jit(solution)/shard_map/ppermute | solution.py:20
  76.4 1.5 %shard_map.199 = f32[32,1536]{1,0:T(8,128)S(1)} custom-call(bf16[16,2304]{1,0:T(8,128)(2,1)S(1)} %get-tuple-element.42.refs_0_, bf16[16,2304]{1,0:T(8,128)(2,1)S(1)} %collective-permute-done.18.refs_1_, bf16[256,1536]{1,0:T(8,128)(2,1)S(1)} %copy-done.2, bf16[256,1536]{1,0:T(8,128)(2,1)S(1)} %copy-done.3, ...), custom_call_target="tpu_custom_call" | custom-call | flops 1048576 | bytes 1048576 | tf_op jit(solution)/shard_map/pallas_call | solution.py:333
  78.0 0.7 fusion.4
  78.7 1.5 %shard_map.200 = bf16[32,1536]{1,0:T(8,128)(2,1)S(1)} custom-call(bf16[16,2304]{1,0:T(8,128)(2,1)S(1)} %collective-permute-done.19.refs_0_, bf16[16,2304]{1,0:T(8,128)(2,1)S(1)} %collective-permute-done.20.refs_1_, bf16[256,1536]{1,0:T(8,128)(2,1)S(1)} %copy-done.2, bf16[256,1536]{1,0:T(8,128)(2,1)S(1)} %copy-done.3, ...), custom_call_target="tpu_custom_call" | custom-call | flops 1048576 | bytes 1048576 | tf_op jit(solution)/shard_map/pallas_call | solution.py:333
  80.3 1.6 %shard_map.201 = bf16[32,1536]{1,0:T(8,128)(2,1)S(1)} custom-call(bf16[16,2304]{1,0:T(8,128)(2,1)S(1)} %collective-permute-done.21.refs_0_, bf16[16,2304]{1,0:T(8,128)(2,1)S(1)} %collective-permute-done.22.refs_1_, bf16[256,1536]{1,0:T(8,128)(2,1)S(1)} %copy-done.2, bf16[256,1536]{1,0:T(8,128)(2,1)S(1)} %copy-done.3, ...), custom_call_target="tpu_custom_call" | custom-call | flops 1048576 | bytes 1048576 | tf_op jit(solution)/shard_map/pallas_call | solution.py:333
  82.0 2.6 %collective-permute-start.29 = (bf16[32,1536]{1,0:T(8,128)(2,1)S(1)}, bf16[32,1536]{1,0:T(8,128)(2,1)S(1)}, u32[]{:S(2)}, u32[]{:S(2)}) collective-permute-start(bf16[32,1536]{1,0:T(8,128)(2,1)S(1)} %shard_map.201), channel_id=1, source_target_pairs={{0,16},{4,20},{8,24},{12,28},{16,0},{20,4},{24,8},{28,12},{1,17},{... | collective-permute-start | bytes 294920 | tf_op jit(solution)/shard_map/ppermute | solution.py:20
  84.5 1.5 %shard_map.202 = bf16[32,1536]{1,0:T(8,128)(2,1)S(1)} custom-call(bf16[16,2304]{1,0:T(8,128)(2,1)S(1)} %collective-permute-done.23.refs_0_, bf16[16,2304]{1,0:T(8,128)(2,1)S(1)} %collective-permute-done.24.refs_1_, bf16[256,1536]{1,0:T(8,128)(2,1)S(1)} %copy-done.2, bf16[256,1536]{1,0:T(8,128)(2,1)S(1)} %copy-done.3, ...), custom_call_target="tpu_custom_call" | custom-call | flops 1048576 | bytes 1048576 | tf_op jit(solution)/shard_map/pallas_call | solution.py:333
  86.0 1.8 %collective-permute-start.30 = (bf16[32,1536]{1,0:T(8,128)(2,1)S(1)}, bf16[32,1536]{1,0:T(8,128)(2,1)S(1)}, u32[]{:S(2)}, u32[]{:S(2)}) collective-permute-start(bf16[32,1536]{1,0:T(8,128)(2,1)S(1)} %shard_map.202), channel_id=1, source_target_pairs={{0,24},{4,28},{8,16},{12,20},{16,8},{20,12},{24,0},{28,4},{1,25},{... | collective-permute-start | bytes 294920 | tf_op jit(solution)/shard_map/ppermute | solution.py:20
  87.8 0.7 multiply_convert_fusion
  88.7 4.1 %collective-permute-done.29 = bf16[32,1536]{1,0:T(8,128)(2,1)S(1)} collective-permute-done((bf16[32,1536]{1,0:T(8,128)(2,1)S(1)}, bf16[32,1536]{1,0:T(8,128)(2,1)S(1)}, u32[]{:S(2)}, u32[]{:S(2)}) %collective-permute-start.29) | collective-permute-done | bytes 98336 | tf_op jit(solution)/shard_map/ppermute | solution.py:20
  92.9 2.2 %collective-permute-start.38 = (bf16[32,768]{1,0:T(8,128)(2,1)S(1)}, bf16[32,768]{1,0:T(8,128)(2,1)S(1)}, u32[]{:S(2)}, u32[]{:S(2)}) collective-permute-start(bf16[32,768]{1,0:T(8,128)(2,1)S(1)} %fusion.11.refs_4_), channel_id=1, source_target_pairs={{0,24},{4,28},{8,16},{12,20},{16,8},{20,12},{24,0},{28,4},{1,25},{... | collective-permute-start | bytes 147464 | tf_op jit(solution)/shard_map/ppermute | solution.py:20
  95.1 1.5 %collective-permute-start.35 = (bf16[32,768]{1,0:T(8,128)(2,1)S(1)}, bf16[32,768]{1,0:T(8,128)(2,1)S(1)}, u32[]{:S(2)}, u32[]{:S(2)}) collective-permute-start(bf16[32,768]{1,0:T(8,128)(2,1)S(1)} %fusion.11.refs_4_), channel_id=1, source_target_pairs={{0,16},{4,20},{8,24},{12,28},{16,0},{20,4},{24,8},{28,12},{1,17},{... | collective-permute-start | bytes 147464 | tf_op jit(solution)/shard_map/ppermute | solution.py:20
  96.6 0.7 collective-permute-start.32
  97.3 0.7 fusion.6.refs_0_
  98.1 1.0 collective-permute-done.38.refs_4_
  99.4 0.8 collective-permute-done.35.refs_4_
  102.0 2.7 %collective-permute-start.40 = (bf16[16,2048]{1,0:T(8,128)(2,1)S(1)}, bf16[16,2048]{1,0:T(8,128)(2,1)S(1)}, u32[]{:S(2)}, u32[]{:S(2)}) collective-permute-start(bf16[16,2048]{1,0:T(8,128)(2,1)S(1)} %shard_map.210), channel_id=1, source_target_pairs={{0,24},{4,28},{8,16},{12,20},{16,8},{20,12},{24,0},{28,4},{1,25},{... | collective-permute-start | bytes 196616 | tf_op jit(solution)/shard_map/ppermute | solution.py:20
  104.8 1.8 %collective-permute-start.34 = (bf16[16,2048]{1,0:T(8,128)(2,1)S(1)}, bf16[16,2048]{1,0:T(8,128)(2,1)S(1)}, u32[]{:S(2)}, u32[]{:S(2)}) collective-permute-start(bf16[16,2048]{1,0:T(8,128)(2,1)S(1)} %shard_map.206), channel_id=1, source_target_pairs={{0,8},{4,12},{8,0},{12,4},{16,24},{20,28},{24,16},{28,20},{1,9},{5... | collective-permute-start | bytes 196616 | tf_op jit(solution)/shard_map/ppermute | solution.py:20
  106.6 2.3 %collective-permute-done.40 = bf16[16,2048]{1,0:T(8,128)(2,1)S(1)} collective-permute-done((bf16[16,2048]{1,0:T(8,128)(2,1)S(1)}, bf16[16,2048]{1,0:T(8,128)(2,1)S(1)}, u32[]{:S(2)}, u32[]{:S(2)}) %collective-permute-start.40) | collective-permute-done | bytes 65568 | tf_op jit(solution)/shard_map/ppermute | solution.py:20
  108.9 2.2 %collective-permute-done.37 = bf16[16,2048]{1,0:T(8,128)(2,1)S(1)} collective-permute-done((bf16[16,2048]{1,0:T(8,128)(2,1)S(1)}, bf16[16,2048]{1,0:T(8,128)(2,1)S(1)}, u32[]{:S(2)}, u32[]{:S(2)}) %collective-permute-start.37) | collective-permute-done | bytes 65568 | tf_op jit(solution)/shard_map/ppermute | solution.py:20
  111.2 1.6 %collective-permute-start.43 = (bf16[16,2048]{1,0:T(8,128)(2,1)S(1)}, bf16[16,2048]{1,0:T(8,128)(2,1)S(1)}, u32[]{:S(2)}, u32[]{:S(2)}) collective-permute-start(bf16[16,2048]{1,0:T(8,128)(2,1)S(1)} %add_convert_fusion.refs_2_), channel_id=1, source_target_pairs={{0,3},{1,2},{2,1},{3,0},{4,7},{5,6},{6,5},{7,4},{8,11},{9,10},{10,... | collective-permute-start | bytes 196616 | tf_op jit(solution)/shard_map/ppermute | solution.py:20
  112.7 1.1 collective-permute-start.42
  113.8 0.9 collective-permute-start.41
  114.7 3.8 %write_state.2.refs_0_ = f32[16,4,128,128]{3,2,1,0:T(8,128)} custom-call(f32[3,16,512]{2,1,0:T(8,128)S(1)} %get-tuple-element.51.gates_ref, f32[16,4,128,128]{3,2,1,0:T(8,128)} %state_ref.3), custom_call_target="tpu_custom_call" | custom-call | flops 4194304 | bytes 8388608 | tf_op jit(solution)/shard_map/write_state/pallas_call | solution.py:481
  118.5 2.6 %write_state.3 = f32[16,4,128,128]{3,2,1,0:T(8,128)} custom-call(f32[3,16,512]{2,1,0:T(8,128)S(1)} %get-tuple-element.51.gates_ref, f32[16,4,128,128]{3,2,1,0:T(8,128)S(1)} %copy-done.1, f32[16,4,128,128]{3,2,1,0:T(8,128)} %write_state.2.refs_0_), custom_call_target="tpu_custom_call", output_to_operand_aliasing={{}: (2, {})} | custom-call | flops 4194304 | bytes 8388608 | tf_op jit(solution)/shard_map/write_state/pallas_call | solution.py:481
  121.1 0.7 shard_map.211
  (89 shorter events, 3.4 us)
Async XLA Ops:
  0.6 53.8 %copy-start.3 = (bf16[256,1536]{1,0:T(8,128)(2,1)S(1)}, bf16[256,1536]{1,0:T(8,128)(2,1)}, u32[]{:S(2)}) copy-start(bf16[256,1536]{1,0:T(8,128)(2,1)} %refs_3_.7) | copy-start | bytes 2359300
  0.6 16.4 %collective-permute-start.11 = (bf16[512,256]{1,0:T(8,128)(2,1)}, bf16[512,256]{1,0:T(8,128)(2,1)S(1)}, u32[]{:S(2)}, u32[]{:S(2)}) collective-permute-start(bf16[512,256]{1,0:T(8,128)(2,1)} %refs_0_.1), channel_id=1, source_target_pairs={{0,16},{4,20},{8,24},{12,28},{16,0},{20,4},{24,8},{28,12},{1,17},{... | collective-permute-start | bytes 786440 | tf_op jit(solution)/shard_map/ppermute | solution.py:20
  5.8 12.0 %collective-permute-start = (bf16[4,16,256]{2,1,0:T(8,128)(2,1)S(1)}, bf16[4,16,256]{2,1,0:T(8,128)(2,1)S(1)}, u32[]{:S(2)}, u32[]{:S(2)}) collective-permute-start(bf16[4,16,256]{2,1,0:T(8,128)(2,1)S(1)} %get-tuple-element.32), channel_id=1, source_target_pairs={{0,4},{4,0},{8,12},{12,8},{16,20},{20,16},{24,28},{28,24},{1,5},{5... | collective-permute-start | bytes 98312 | tf_op jit(solution)/shard_map/ppermute | solution.py:20
  5.9 26.6 %collective-permute-start.9 = (bf16[512,256]{1,0:T(8,128)(2,1)}, bf16[512,256]{1,0:T(8,128)(2,1)S(1)}, u32[]{:S(2)}, u32[]{:S(2)}) collective-permute-start(bf16[512,256]{1,0:T(8,128)(2,1)} %refs_0_.1), channel_id=1, source_target_pairs={{0,8},{4,12},{8,0},{12,4},{16,24},{20,28},{24,16},{28,20},{1,9},{5... | collective-permute-start | bytes 786440 | tf_op jit(solution)/shard_map/ppermute | solution.py:20
  17.0 15.9 %collective-permute-start.13 = (bf16[512,256]{1,0:T(8,128)(2,1)S(1)}, bf16[512,256]{1,0:T(8,128)(2,1)S(1)}, u32[]{:S(2)}, u32[]{:S(2)}) collective-permute-start(bf16[512,256]{1,0:T(8,128)(2,1)S(1)} %collective-permute-done.11.refs_4_), channel_id=1, source_target_pairs={{0,8},{4,12},{8,0},{12,4},{16,24},{20,28},{24,16},{28,20},{1,9},{5... | collective-permute-start | bytes 786440 | tf_op jit(solution)/shard_map/ppermute | solution.py:20
  17.8 9.9 %collective-permute-start.3 = (bf16[2,16,256]{2,1,0:T(8,128)(2,1)S(1)}, bf16[2,16,256]{2,1,0:T(8,128)(2,1)S(1)}, u32[]{:S(2)}, u32[]{:S(2)}) collective-permute-start(bf16[2,16,256]{2,1,0:T(8,128)(2,1)S(1)} %get-tuple-element.54), channel_id=1, source_target_pairs={{0,24},{4,28},{8,16},{12,20},{16,8},{20,12},{24,0},{28,4},{1,25},{... | collective-permute-start | bytes 49160 | tf_op jit(solution)/shard_map/ppermute | solution.py:20
  20.6 7.1 %collective-permute-start.1 = (bf16[2,16,256]{2,1,0:T(8,128)(2,1)S(1)}, bf16[2,16,256]{2,1,0:T(8,128)(2,1)S(1)}, u32[]{:S(2)}, u32[]{:S(2)}) collective-permute-start(bf16[2,16,256]{2,1,0:T(8,128)(2,1)S(1)} %get-tuple-element.56), channel_id=1, source_target_pairs={{0,8},{4,12},{8,0},{12,4},{16,24},{20,28},{24,16},{28,20},{1,9},{5... | collective-permute-start | bytes 49160 | tf_op jit(solution)/shard_map/ppermute | solution.py:20
  21.8 5.9 %collective-permute-start.2 = (bf16[2,16,256]{2,1,0:T(8,128)(2,1)S(1)}, bf16[2,16,256]{2,1,0:T(8,128)(2,1)S(1)}, u32[]{:S(2)}, u32[]{:S(2)}) collective-permute-start(bf16[2,16,256]{2,1,0:T(8,128)(2,1)S(1)} %get-tuple-element.57), channel_id=1, source_target_pairs={{0,16},{4,20},{8,24},{12,28},{16,0},{20,4},{24,8},{28,12},{1,17},{... | collective-permute-start | bytes 49160 | tf_op jit(solution)/shard_map/ppermute | solution.py:20
  27.7 1.0 copy-start.5
  28.6 0.9 copy-start.6
  29.6 0.9 copy-start.7
  30.5 0.9 copy-start.8
  31.5 23.6 %copy-start.9 = (bf16[512,256]{1,0:T(8,128)(2,1)S(1)}, bf16[512,256]{1,0:T(8,128)(2,1)}, u32[]{:S(2)}) copy-start(bf16[512,256]{1,0:T(8,128)(2,1)} %refs_0_.1) | copy-start | bytes 786436
  31.8 1.6 %collective-permute-start.4 = (bf16[4,16,2048]{2,1,0:T(8,128)(2,1)S(1)}, bf16[4,16,2048]{2,1,0:T(8,128)(2,1)S(1)}, u32[]{:S(2)}, u32[]{:S(2)}) collective-permute-start(bf16[4,16,2048]{2,1,0:T(8,128)(2,1)S(1)} %get-tuple-element.34), channel_id=1, source_target_pairs={{0,4},{4,0},{8,12},{12,8},{16,20},{20,16},{24,28},{28,24},{1,5},{5... | collective-permute-start | bytes 786440 | tf_op jit(solution)/shard_map/ppermute | solution.py:20
  31.9 22.6 %collective-permute-start.8 = (bf16[512,256]{1,0:T(8,128)(2,1)}, bf16[512,256]{1,0:T(8,128)(2,1)S(1)}, u32[]{:S(2)}, u32[]{:S(2)}) collective-permute-start(bf16[512,256]{1,0:T(8,128)(2,1)} %refs_0_.1), channel_id=1, source_target_pairs={{0,4},{4,0},{8,12},{12,8},{16,20},{20,16},{24,28},{28,24},{1,5},{5... | collective-permute-start | bytes 786440 | tf_op jit(solution)/shard_map/ppermute | solution.py:20
  32.4 22.7 %collective-permute-start.12 = (bf16[512,256]{1,0:T(8,128)(2,1)S(1)}, bf16[512,256]{1,0:T(8,128)(2,1)S(1)}, u32[]{:S(2)}, u32[]{:S(2)}) collective-permute-start(bf16[512,256]{1,0:T(8,128)(2,1)S(1)} %collective-permute-done.11.refs_4_), channel_id=1, source_target_pairs={{0,4},{4,0},{8,12},{12,8},{16,20},{20,16},{24,28},{28,24},{1,5},{5... | collective-permute-start | bytes 786440 | tf_op jit(solution)/shard_map/ppermute | solution.py:20
  32.5 22.6 %collective-permute-start.10 = (bf16[512,256]{1,0:T(8,128)(2,1)S(1)}, bf16[512,256]{1,0:T(8,128)(2,1)S(1)}, u32[]{:S(2)}, u32[]{:S(2)}) collective-permute-start(bf16[512,256]{1,0:T(8,128)(2,1)S(1)} %collective-permute-done.9.refs_2_), channel_id=1, source_target_pairs={{0,4},{4,0},{8,12},{12,8},{16,20},{20,16},{24,28},{28,24},{1,5},{5... | collective-permute-start | bytes 786440 | tf_op jit(solution)/shard_map/ppermute | solution.py:20
  32.9 22.2 %collective-permute-start.14 = (bf16[512,256]{1,0:T(8,128)(2,1)S(1)}, bf16[512,256]{1,0:T(8,128)(2,1)S(1)}, u32[]{:S(2)}, u32[]{:S(2)}) collective-permute-start(bf16[512,256]{1,0:T(8,128)(2,1)S(1)} %collective-permute-done.13.refs_6_), channel_id=1, source_target_pairs={{0,4},{4,0},{8,12},{12,8},{16,20},{20,16},{24,28},{28,24},{1,5},{5... | collective-permute-start | bytes 786440 | tf_op jit(solution)/shard_map/ppermute | solution.py:20
  33.4 4.3 %collective-permute-start.5 = (bf16[16,2048]{1,0:T(8,128)(2,1)S(1)}, bf16[16,2048]{1,0:T(8,128)(2,1)S(1)}, u32[]{:S(2)}, u32[]{:S(2)}) collective-permute-start(bf16[16,2048]{1,0:T(8,128)(2,1)S(1)} %get-tuple-element.36), channel_id=1, source_target_pairs={{0,8},{4,12},{8,0},{12,4},{16,24},{20,28},{24,16},{28,20},{1,9},{5... | collective-permute-start | bytes 196616 | tf_op jit(solution)/shard_map/ppermute | solution.py:20
  37.8 5.9 %collective-permute-start.6 = (bf16[16,2048]{1,0:T(8,128)(2,1)S(1)}, bf16[16,2048]{1,0:T(8,128)(2,1)S(1)}, u32[]{:S(2)}, u32[]{:S(2)}) collective-permute-start(bf16[16,2048]{1,0:T(8,128)(2,1)S(1)} %get-tuple-element.37), channel_id=1, source_target_pairs={{0,16},{4,20},{8,24},{12,28},{16,0},{20,4},{24,8},{28,12},{1,17},{... | collective-permute-start | bytes 196616 | tf_op jit(solution)/shard_map/ppermute | solution.py:20
  43.6 6.1 %collective-permute-start.7 = (bf16[16,2048]{1,0:T(8,128)(2,1)S(1)}, bf16[16,2048]{1,0:T(8,128)(2,1)S(1)}, u32[]{:S(2)}, u32[]{:S(2)}) collective-permute-start(bf16[16,2048]{1,0:T(8,128)(2,1)S(1)} %get-tuple-element.38), channel_id=1, source_target_pairs={{0,24},{4,28},{8,16},{12,20},{16,8},{20,12},{24,0},{28,4},{1,25},{... | collective-permute-start | bytes 196616 | tf_op jit(solution)/shard_map/ppermute | solution.py:20
  49.7 21.9 %collective-permute-start.26 = (bf16[256,1536]{1,0:T(8,128)(2,1)}, bf16[256,1536]{1,0:T(8,128)(2,1)S(1)}, u32[]{:S(2)}, u32[]{:S(2)}) collective-permute-start(bf16[256,1536]{1,0:T(8,128)(2,1)} %refs_2_.11), channel_id=1, source_target_pairs={{0,4},{4,0},{8,12},{12,8},{16,20},{20,16},{24,28},{28,24},{1,5},{5... | collective-permute-start | bytes 2359304 | tf_op jit(solution)/shard_map/ppermute | solution.py:20
  49.7 2.2 %copy-start = (f32[16,4,128,128]{3,2,1,0:T(8,128)S(1)}, f32[16,4,128,128]{3,2,1,0:T(8,128)}, u32[]{:S(2)}) copy-start(f32[16,4,128,128]{3,2,1,0:T(8,128)} %state_ref.3) | copy-start | bytes 12582916
  54.5 21.9 %collective-permute-start.27 = (bf16[256,1536]{1,0:T(8,128)(2,1)S(1)}, bf16[256,1536]{1,0:T(8,128)(2,1)}, u32[]{:S(2)}, u32[]{:S(2)}) collective-permute-start(bf16[256,1536]{1,0:T(8,128)(2,1)S(1)} %copy-done.3), channel_id=1, source_target_pairs={{0,4},{4,0},{8,12},{12,8},{16,20},{20,16},{24,28},{28,24},{1,5},{5... | collective-permute-start | bytes 2359304 | tf_op jit(solution)/shard_map/ppermute | solution.py:20
  55.4 5.2 %collective-permute-start.17 = (bf16[16,2048]{1,0:T(8,128)(2,1)S(1)}, bf16[16,2048]{1,0:T(8,128)(2,1)S(1)}, u32[]{:S(2)}, u32[]{:S(2)}) collective-permute-start(bf16[16,2048]{1,0:T(8,128)(2,1)S(1)} %shard_map.197.refs_4_), channel_id=1, source_target_pairs={{0,3},{1,2},{2,1},{3,0},{4,7},{5,6},{6,5},{7,4},{8,11},{9,10},{10,... | collective-permute-start | bytes 196616 | tf_op jit(solution)/shard_map/ppermute | solution.py:20
  57.9 4.3 %collective-permute-start.16 = (bf16[16,2048]{1,0:T(8,128)(2,1)S(1)}, bf16[16,2048]{1,0:T(8,128)(2,1)S(1)}, u32[]{:S(2)}, u32[]{:S(2)}) collective-permute-start(bf16[16,2048]{1,0:T(8,128)(2,1)S(1)} %shard_map.197.refs_4_), channel_id=1, source_target_pairs={{0,2},{1,3},{2,0},{3,1},{4,6},{5,7},{6,4},{7,5},{8,10},{9,11},{10,... | collective-permute-start | bytes 196616 | tf_op jit(solution)/shard_map/ppermute | solution.py:20
  58.4 4.4 %collective-permute-start.15 = (bf16[16,2048]{1,0:T(8,128)(2,1)S(1)}, bf16[16,2048]{1,0:T(8,128)(2,1)}, u32[]{:S(2)}, u32[]{:S(2)}) collective-permute-start(bf16[16,2048]{1,0:T(8,128)(2,1)S(1)} %shard_map.197.refs_4_), channel_id=1, source_target_pairs={{0,1},{1,0},{2,3},{3,2},{4,5},{5,4},{6,7},{7,6},{8,9},{9,8},{10,11... | collective-permute-start | bytes 196616 | tf_op jit(solution)/shard_map/ppermute | solution.py:20
  58.9 12.7 %copy-start.4 = (bf16[1536,256]{1,0:T(8,128)(2,1)S(1)}, bf16[1536,256]{1,0:T(8,128)(2,1)}, u32[]{:S(2)}) copy-start(bf16[1536,256]{1,0:T(8,128)(2,1)} %refs_2_.15) | copy-start | bytes 2359300
  59.0 17.4 %copy-start.2 = (bf16[256,1536]{1,0:T(8,128)(2,1)S(1)}, bf16[256,1536]{1,0:T(8,128)(2,1)}, u32[]{:S(2)}) copy-start(bf16[256,1536]{1,0:T(8,128)(2,1)} %refs_2_.11) | copy-start | bytes 2359300
  59.9 18.1 %copy-start.11 = (bf16[1,2048,896]{2,1,0:T(8,128)(2,1)S(1)}, bf16[1,2048,896]{2,1,0:T(8,128)(2,1)}, u32[]{:S(2)}) copy-start(bf16[1,2048,896]{2,1,0:T(8,128)(2,1)} %param.31) | copy-start | bytes 11010052
  64.0 8.2 %collective-permute-start.23 = (bf16[16,2304]{1,0:T(8,128)(2,1)S(1)}, bf16[16,2304]{1,0:T(8,128)(2,1)S(1)}, u32[]{:S(2)}, u32[]{:S(2)}) collective-permute-start(bf16[16,2304]{1,0:T(8,128)(2,1)S(1)} %get-tuple-element.42.refs_0_), channel_id=1, source_target_pairs={{0,24},{4,28},{8,16},{12,20},{16,8},{20,12},{24,0},{28,4},{1,25},{... | collective-permute-start | bytes 221192 | tf_op jit(solution)/shard_map/ppermute | solution.py:20
  65.7 5.1 %collective-permute-start.19 = (bf16[16,2304]{1,0:T(8,128)(2,1)S(1)}, bf16[16,2304]{1,0:T(8,128)(2,1)S(1)}, u32[]{:S(2)}, u32[]{:S(2)}) collective-permute-start(bf16[16,2304]{1,0:T(8,128)(2,1)S(1)} %get-tuple-element.42.refs_0_), channel_id=1, source_target_pairs={{0,8},{4,12},{8,0},{12,4},{16,24},{20,28},{24,16},{28,20},{1,9},{5... | collective-permute-start | bytes 221192 | tf_op jit(solution)/shard_map/ppermute | solution.py:20
  65.7 5.8 %collective-permute-start.18 = (bf16[16,2304]{1,0:T(8,128)(2,1)S(1)}, bf16[16,2304]{1,0:T(8,128)(2,1)S(1)}, u32[]{:S(2)}, u32[]{:S(2)}) collective-permute-start(bf16[16,2304]{1,0:T(8,128)(2,1)S(1)} %get-tuple-element.42.refs_0_), channel_id=1, source_target_pairs={{0,4},{4,0},{8,12},{12,8},{16,20},{20,16},{24,28},{28,24},{1,5},{5... | collective-permute-start | bytes 221192 | tf_op jit(solution)/shard_map/ppermute | solution.py:20
  70.9 5.5 %collective-permute-start.21 = (bf16[16,2304]{1,0:T(8,128)(2,1)S(1)}, bf16[16,2304]{1,0:T(8,128)(2,1)S(1)}, u32[]{:S(2)}, u32[]{:S(2)}) collective-permute-start(bf16[16,2304]{1,0:T(8,128)(2,1)S(1)} %get-tuple-element.42.refs_0_), channel_id=1, source_target_pairs={{0,16},{4,20},{8,24},{12,28},{16,0},{20,4},{24,8},{28,12},{1,17},{... | collective-permute-start | bytes 221192 | tf_op jit(solution)/shard_map/ppermute | solution.py:20
  71.6 6.3 %collective-permute-start.20 = (bf16[16,2304]{1,0:T(8,128)(2,1)S(1)}, bf16[16,2304]{1,0:T(8,128)(2,1)S(1)}, u32[]{:S(2)}, u32[]{:S(2)}) collective-permute-start(bf16[16,2304]{1,0:T(8,128)(2,1)S(1)} %collective-permute-done.19.refs_0_), channel_id=1, source_target_pairs={{0,4},{4,0},{8,12},{12,8},{16,20},{20,16},{24,28},{28,24},{1,5},{5... | collective-permute-start | bytes 221192 | tf_op jit(solution)/shard_map/ppermute | solution.py:20
  71.6 26.5 %collective-permute-start.25 = (bf16[1536,256]{1,0:T(8,128)(2,1)S(1)}, bf16[1536,256]{1,0:T(8,128)(2,1)S(1)}, u32[]{:S(2)}, u32[]{:S(2)}) collective-permute-start(bf16[1536,256]{1,0:T(8,128)(2,1)S(1)} %copy-done.4), channel_id=1, source_target_pairs={{0,4},{4,0},{8,12},{12,8},{16,20},{20,16},{24,28},{28,24},{1,5},{5... | collective-permute-start | bytes 2359304 | tf_op jit(solution)/shard_map/ppermute | solution.py:20
  72.2 5.8 %collective-permute-start.24 = (bf16[16,2304]{1,0:T(8,128)(2,1)S(1)}, bf16[16,2304]{1,0:T(8,128)(2,1)S(1)}, u32[]{:S(2)}, u32[]{:S(2)}) collective-permute-start(bf16[16,2304]{1,0:T(8,128)(2,1)S(1)} %collective-permute-done.23.refs_0_), channel_id=1, source_target_pairs={{0,4},{4,0},{8,12},{12,8},{16,20},{20,16},{24,28},{28,24},{1,5},{5... | collective-permute-start | bytes 221192 | tf_op jit(solution)/shard_map/ppermute | solution.py:20
  76.4 1.6 %collective-permute-start.22 = (bf16[16,2304]{1,0:T(8,128)(2,1)S(1)}, bf16[16,2304]{1,0:T(8,128)(2,1)S(1)}, u32[]{:S(2)}, u32[]{:S(2)}) collective-permute-start(bf16[16,2304]{1,0:T(8,128)(2,1)S(1)} %collective-permute-done.21.refs_0_), channel_id=1, source_target_pairs={{0,4},{4,0},{8,12},{12,8},{16,20},{20,16},{24,28},{28,24},{1,5},{5... | collective-permute-start | bytes 221192 | tf_op jit(solution)/shard_map/ppermute | solution.py:20
  80.2 7.6 %copy-start.12 = (bf16[1,2048,896]{2,1,0:T(8,128)(2,1)S(1)}, bf16[1,2048,896]{2,1,0:T(8,128)(2,1)}, u32[]{:S(2)}) copy-start(bf16[1,2048,896]{2,1,0:T(8,128)(2,1)} %param.32) | copy-start | bytes 11010052
  80.2 8.5 %collective-permute-start.28 = (bf16[32,1536]{1,0:T(8,128)(2,1)S(1)}, bf16[32,1536]{1,0:T(8,128)(2,1)S(1)}, u32[]{:S(2)}, u32[]{:S(2)}) collective-permute-start(bf16[32,1536]{1,0:T(8,128)(2,1)S(1)} %shard_map.200), channel_id=1, source_target_pairs={{0,8},{4,12},{8,0},{12,4},{16,24},{20,28},{24,16},{28,20},{1,9},{5... | collective-permute-start | bytes 294920 | tf_op jit(solution)/shard_map/ppermute | solution.py:20
  82.0 10.8 %collective-permute-start.29 = (bf16[32,1536]{1,0:T(8,128)(2,1)S(1)}, bf16[32,1536]{1,0:T(8,128)(2,1)S(1)}, u32[]{:S(2)}, u32[]{:S(2)}) collective-permute-start(bf16[32,1536]{1,0:T(8,128)(2,1)S(1)} %shard_map.201), channel_id=1, source_target_pairs={{0,16},{4,20},{8,24},{12,28},{16,0},{20,4},{24,8},{28,12},{1,17},{... | collective-permute-start | bytes 294920 | tf_op jit(solution)/shard_map/ppermute | solution.py:20
  86.0 11.3 %copy-start.10 = (bf16[1,896,2048]{2,1,0:T(8,128)(2,1)S(1)}, bf16[1,896,2048]{2,1,0:T(8,128)(2,1)}, u32[]{:S(2)}) copy-start(bf16[1,896,2048]{2,1,0:T(8,128)(2,1)} %param.33) | copy-start | bytes 11010052
  86.0 6.8 %collective-permute-start.30 = (bf16[32,1536]{1,0:T(8,128)(2,1)S(1)}, bf16[32,1536]{1,0:T(8,128)(2,1)S(1)}, u32[]{:S(2)}, u32[]{:S(2)}) collective-permute-start(bf16[32,1536]{1,0:T(8,128)(2,1)S(1)} %shard_map.202), channel_id=1, source_target_pairs={{0,24},{4,28},{8,16},{12,20},{16,8},{20,12},{24,0},{28,4},{1,25},{... | collective-permute-start | bytes 294920 | tf_op jit(solution)/shard_map/ppermute | solution.py:20
  92.9 6.2 %collective-permute-start.38 = (bf16[32,768]{1,0:T(8,128)(2,1)S(1)}, bf16[32,768]{1,0:T(8,128)(2,1)S(1)}, u32[]{:S(2)}, u32[]{:S(2)}) collective-permute-start(bf16[32,768]{1,0:T(8,128)(2,1)S(1)} %fusion.11.refs_4_), channel_id=1, source_target_pairs={{0,24},{4,28},{8,16},{12,20},{16,8},{20,12},{24,0},{28,4},{1,25},{... | collective-permute-start | bytes 147464 | tf_op jit(solution)/shard_map/ppermute | solution.py:20
  95.1 5.2 %collective-permute-start.35 = (bf16[32,768]{1,0:T(8,128)(2,1)S(1)}, bf16[32,768]{1,0:T(8,128)(2,1)S(1)}, u32[]{:S(2)}, u32[]{:S(2)}) collective-permute-start(bf16[32,768]{1,0:T(8,128)(2,1)S(1)} %fusion.11.refs_4_), channel_id=1, source_target_pairs={{0,16},{4,20},{8,24},{12,28},{16,0},{20,4},{24,8},{28,12},{1,17},{... | collective-permute-start | bytes 147464 | tf_op jit(solution)/shard_map/ppermute | solution.py:20
  96.6 4.2 %collective-permute-start.32 = (bf16[32,768]{1,0:T(8,128)(2,1)S(1)}, bf16[32,768]{1,0:T(8,128)(2,1)S(1)}, u32[]{:S(2)}, u32[]{:S(2)}) collective-permute-start(bf16[32,768]{1,0:T(8,128)(2,1)S(1)} %fusion.11.refs_4_), channel_id=1, source_target_pairs={{0,8},{4,12},{8,0},{12,4},{16,24},{20,28},{24,16},{28,20},{1,9},{5... | collective-permute-start | bytes 147464 | tf_op jit(solution)/shard_map/ppermute | solution.py:20
  99.3 2.6 %collective-permute-start.39 = (bf16[16,2048]{1,0:T(8,128)(2,1)S(1)}, bf16[16,2048]{1,0:T(8,128)(2,1)S(1)}, u32[]{:S(2)}, u32[]{:S(2)}) collective-permute-start(bf16[16,2048]{1,0:T(8,128)(2,1)S(1)} %get-tuple-element.50), channel_id=1, source_target_pairs={{0,4},{4,0},{8,12},{12,8},{16,20},{20,16},{24,28},{28,24},{1,5},{5... | collective-permute-start | bytes 196616 | tf_op jit(solution)/shard_map/ppermute | solution.py:20
  100.5 4.1 %collective-permute-start.36 = (bf16[16,2048]{1,0:T(8,128)(2,1)S(1)}, bf16[16,2048]{1,0:T(8,128)(2,1)S(1)}, u32[]{:S(2)}, u32[]{:S(2)}) collective-permute-start(bf16[16,2048]{1,0:T(8,128)(2,1)S(1)} %get-tuple-element.48), channel_id=1, source_target_pairs={{0,4},{4,0},{8,12},{12,8},{16,20},{20,16},{24,28},{28,24},{1,5},{5... | collective-permute-start | bytes 196616 | tf_op jit(solution)/shard_map/ppermute | solution.py:20
  101.0 3.7 %collective-permute-start.33 = (bf16[16,2048]{1,0:T(8,128)(2,1)S(1)}, bf16[16,2048]{1,0:T(8,128)(2,1)S(1)}, u32[]{:S(2)}, u32[]{:S(2)}) collective-permute-start(bf16[16,2048]{1,0:T(8,128)(2,1)S(1)} %get-tuple-element.46), channel_id=1, source_target_pairs={{0,4},{4,0},{8,12},{12,8},{16,20},{20,16},{24,28},{28,24},{1,5},{5... | collective-permute-start | bytes 196616 | tf_op jit(solution)/shard_map/ppermute | solution.py:20
  101.7 4.9 %collective-permute-start.31 = (bf16[16,2048]{1,0:T(8,128)(2,1)S(1)}, bf16[16,2048]{1,0:T(8,128)(2,1)S(1)}, u32[]{:S(2)}, u32[]{:S(2)}) collective-permute-start(bf16[16,2048]{1,0:T(8,128)(2,1)S(1)} %get-tuple-element.44), channel_id=1, source_target_pairs={{0,4},{4,0},{8,12},{12,8},{16,20},{20,16},{24,28},{28,24},{1,5},{5... | collective-permute-start | bytes 196616 | tf_op jit(solution)/shard_map/ppermute | solution.py:20
  102.0 6.9 %collective-permute-start.40 = (bf16[16,2048]{1,0:T(8,128)(2,1)S(1)}, bf16[16,2048]{1,0:T(8,128)(2,1)S(1)}, u32[]{:S(2)}, u32[]{:S(2)}) collective-permute-start(bf16[16,2048]{1,0:T(8,128)(2,1)S(1)} %shard_map.210), channel_id=1, source_target_pairs={{0,24},{4,28},{8,16},{12,20},{16,8},{20,12},{24,0},{28,4},{1,25},{... | collective-permute-start | bytes 196616 | tf_op jit(solution)/shard_map/ppermute | solution.py:20
  104.7 6.5 %collective-permute-start.37 = (bf16[16,2048]{1,0:T(8,128)(2,1)S(1)}, bf16[16,2048]{1,0:T(8,128)(2,1)S(1)}, u32[]{:S(2)}, u32[]{:S(2)}) collective-permute-start(bf16[16,2048]{1,0:T(8,128)(2,1)S(1)} %shard_map.208), channel_id=1, source_target_pairs={{0,16},{4,20},{8,24},{12,28},{16,0},{20,4},{24,8},{28,12},{1,17},{... | collective-permute-start | bytes 196616 | tf_op jit(solution)/shard_map/ppermute | solution.py:20
  104.8 6.3 %collective-permute-start.34 = (bf16[16,2048]{1,0:T(8,128)(2,1)S(1)}, bf16[16,2048]{1,0:T(8,128)(2,1)S(1)}, u32[]{:S(2)}, u32[]{:S(2)}) collective-permute-start(bf16[16,2048]{1,0:T(8,128)(2,1)S(1)} %shard_map.206), channel_id=1, source_target_pairs={{0,8},{4,12},{8,0},{12,4},{16,24},{20,28},{24,16},{28,20},{1,9},{5... | collective-permute-start | bytes 196616 | tf_op jit(solution)/shard_map/ppermute | solution.py:20
  111.2 9.9 %collective-permute-start.43 = (bf16[16,2048]{1,0:T(8,128)(2,1)S(1)}, bf16[16,2048]{1,0:T(8,128)(2,1)S(1)}, u32[]{:S(2)}, u32[]{:S(2)}) collective-permute-start(bf16[16,2048]{1,0:T(8,128)(2,1)S(1)} %add_convert_fusion.refs_2_), channel_id=1, source_target_pairs={{0,3},{1,2},{2,1},{3,0},{4,7},{5,6},{6,5},{7,4},{8,11},{9,10},{10,... | collective-permute-start | bytes 196616 | tf_op jit(solution)/shard_map/ppermute | solution.py:20
  112.7 8.4 %collective-permute-start.42 = (bf16[16,2048]{1,0:T(8,128)(2,1)S(1)}, bf16[16,2048]{1,0:T(8,128)(2,1)S(1)}, u32[]{:S(2)}, u32[]{:S(2)}) collective-permute-start(bf16[16,2048]{1,0:T(8,128)(2,1)S(1)} %add_convert_fusion.refs_2_), channel_id=1, source_target_pairs={{0,2},{1,3},{2,0},{3,1},{4,6},{5,7},{6,4},{7,5},{8,10},{9,11},{10,... | collective-permute-start | bytes 196616 | tf_op jit(solution)/shard_map/ppermute | solution.py:20
  113.8 7.3 %collective-permute-start.41 = (bf16[16,2048]{1,0:T(8,128)(2,1)S(1)}, bf16[16,2048]{1,0:T(8,128)(2,1)S(1)}, u32[]{:S(2)}, u32[]{:S(2)}) collective-permute-start(bf16[16,2048]{1,0:T(8,128)(2,1)S(1)} %add_convert_fusion.refs_2_), channel_id=1, source_target_pairs={{0,1},{1,0},{2,3},{3,2},{4,5},{5,4},{6,7},{7,6},{8,9},{9,8},{10,11... | collective-permute-start | bytes 196616 | tf_op jit(solution)/shard_map/ppermute | solution.py:20
  114.7 3.8 %copy-start.1 = (f32[16,4,128,128]{3,2,1,0:T(8,128)S(1)}, f32[16,4,128,128]{3,2,1,0:T(8,128)}, u32[]{:S(2)}) copy-start(f32[16,4,128,128]{3,2,1,0:T(8,128)} %state_ref.3) | copy-start | bytes 12582916

commit v3 on v2

--- a/solution.py
+++ b/solution.py
@@ -145,6 +145,7 @@
 def table_kernel(routes_in, scores_in, gate_in, table_ref, gate_ref, routes_ref, scores_ref, sems):
     fetch((routes_in, scores_in, gate_in), (routes_ref, scores_ref, gate_ref), sems)
     seqs = table_ref.shape[0]
+    low = lax.axis_size("ep") + 1
     place = lax.broadcasted_iota(jnp.int32, table_ref.shape, 1)
     across = lax.broadcasted_iota(jnp.int32, (seqs, seqs), 1)
     diagonal = across == lax.broadcasted_iota(jnp.int32, (seqs, seqs), 0)
@@ -156,7 +157,8 @@
     for k in range(2):
         margin = scores_ref[k : k + 1, :] - scores_ref[1 - k : 2 - k, :]
         expert = upright(routes_ref[k : k + 1, :].astype(F32)).astype(jnp.int32)
-        table = jnp.where(place == expert, upright(jax.nn.sigmoid(margin)), table)
+        picked = (place == expert) | (place == expert + low)
+        table = jnp.where(picked, upright(jax.nn.sigmoid(margin)), table)
     table_ref[...] = table
 
 
@@ -229,6 +231,11 @@
 def mix_heads(mixed_heads, weights):
     shape = (mixed_heads.shape[0], weights[0].shape[1] * len(weights))
     return call(mix_kernel, jax.ShapeDtypeStruct(shape, BF16))(mixed_heads, *weights)
+
+
+def two_part(values, place, low):
+    high = values.astype(BF16).astype(F32)
+    return jnp.where(place < low, high, values - high).astype(BF16)
 
 
 def middle_kernel(parts, tokens_ref, gains_ref, gate_ref, table_ref, *refs):
@@ -255,10 +262,9 @@
         products = products + piece * gate_ref[j : j + 1, :].astype(F32)
     dots = jnp.sum(products, axis=1, keepdims=True)
     place = lax.broadcasted_iota(jnp.int32, (seqs, lanes), 1)
-    extra = jnp.where(place == ep_size, jax.nn.sigmoid(dots), table_ref[...])
-    high = extra.astype(BF16)
-    packed_ref[:, width : width + lanes] = high
-    packed_ref[:, width + lanes :] = (extra - high.astype(F32)).astype(BF16)
+    last = (place == ep_size) | (place == 2 * ep_size + 1)
+    extra = jnp.where(last, jax.nn.sigmoid(dots), table_ref[...])
+    packed_ref[:, width:] = two_part(extra, place, ep_size + 1)
 
 
 def to_absolute(values, index, ep_size):
@@ -276,10 +282,9 @@
     ffn_in = (after_mix * rms_scale(after_mix) * norm_gains[2]).astype(BF16)
     dots = jnp.sum(ffn_in.astype(F32) * dense_mix.reshape(1, -1).astype(F32), axis=1, keepdims=True)
     place = jnp.arange(table.shape[1], dtype=jnp.int32)[None]
-    extra = jnp.where(place == ep_size, jax.nn.sigmoid(dots), table)
-    high = extra.astype(BF16)
-    low = (extra - high.astype(F32)).astype(BF16)
-    return after_mix, jnp.concatenate([ffn_in, high, low], axis=1)
+    last = (place == ep_size) | (place == 2 * ep_size + 1)
+    extra = two_part(jnp.where(last, jax.nn.sigmoid(dots), table), place, ep_size + 1)
+    return after_mix, jnp.concatenate([ffn_in, extra], axis=1)
 
 
 def middle(tokens, norm_gains, dense_mix, table, pieces):
@@ -291,7 +296,7 @@
         lambda *refs: middle_kernel(len(pieces), *refs),
         (
             jax.ShapeDtypeStruct((seqs, width), F32),
-            jax.ShapeDtypeStruct((seqs, width + 2 * lanes), BF16),
+            jax.ShapeDtypeStruct((seqs, width + lanes), BF16),
         ),
     )(tokens, norm_gains, dense_mix, table, *near(pieces))
 
@@ -525,7 +530,8 @@
         swap(w, "ep", 1) for w in (w_dense_gate, w_dense_up)
     )
     down_other = swap(w_dense_down, "ep", 1)
-    lanes = -(-(ep_size + 1) // 128) * 128
+    low = ep_size + 1
+    lanes = -(-2 * low // 128) * 128
 
     table, gate = route_table(routes, route_scores, dense_mix, lanes)
     even, odd, tokens, norm_gains, head_rows = front(
@@ -553,7 +559,8 @@
 
     gathered = jnp.concatenate([item for pair in row_pairs for item in pair], axis=0)
     rows = gathered[:, :width]
-    side = gathered[:, width : width + lanes].astype(F32) + gathered[:, width + lanes :].astype(F32)
+    side = gathered[:, width:].astype(F32)
+    side = side[:, :low] + side[:, low : 2 * low]
     expert_scale = lax.dynamic_slice_in_dim(side, ep_index, 1, 1)
     dense_scale = side[:, ep_size : ep_size + 1]
 

time: 122 us -> 122 us (level)
  no operation moved by 1% of the time
where the time goes in v3:
time: 122 us
  waiting for transfers between devices  50.7 us (42%)
  starting transfers between devices  40.6 us (33%)
  Pallas kernels  20.7 us (17%)
  local copies, waits for them, and re-layouts  6.31 us (5%)
  matrix products  2.22 us (2%)
    ppermute x44, waiting for transfers between devices, swap(): return lax.ppermute(value, axis, [(i, i ^ step) for i in range(size)])  50.7 us
    ppermute x44, starting transfers between devices, swap(): return lax.ppermute(value, axis, [(i, i ^ step) for i in range(size)])  40.6 us
    pallas_call x2, Pallas kernels, write_state(): pl.pallas_call(state_kernel, grid=(count,), in_specs=[pl.BlockSpec((3, se...  6.36 us
    pallas_call x4, Pallas kernels, dense_part(): call(lambda *refs: dense_kernel(feats, *refs), jax.ShapeDtypeStruct((2 *...  6.14 us
    unnamed x33, local copies, waits for them, and re-layouts  6.11 us
    pallas_call x1, Pallas kernels, read_heads(): call(lambda *refs: read_kernel(len(arrived), *refs), (jax.ShapeDtypeStruc...  2.54 us
  transfers between devices with their start and end apart: 44, of which 17 were waited for; matrix products, arithmetic and copies ran while one was open for 2% of the time, Pallas kernels for 16%

profile of v3, /device:TPU:0, one launch (start us, length us, event | category | flops | bytes accessed | tf_op | source)
XLA Modules:
  0.0 121.7 jit_solution(12359288765644369069)
XLA Ops:
  0.6 4.1 %collective-permute-start.11 = (bf16[512,256]{1,0:T(8,128)(2,1)}, bf16[512,256]{1,0:T(8,128)(2,1)S(1)}, u32[]{:S(2)}, u32[]{:S(2)}) collective-permute-start(bf16[512,256]{1,0:T(8,128)(2,1)} %refs_0_.1), channel_id=1, source_target_pairs={{0,16},{4,20},{8,24},{12,28},{16,0},{20,4},{24,8},{28,12},{1,17},{... | collective-permute-start | bytes 786440 | tf_op jit(solution)/shard_map/ppermute | solution.py:20
  4.8 1.0 front.1
  5.9 1.6 %collective-permute-start.9 = (bf16[512,256]{1,0:T(8,128)(2,1)}, bf16[512,256]{1,0:T(8,128)(2,1)S(1)}, u32[]{:S(2)}, u32[]{:S(2)}) collective-permute-start(bf16[512,256]{1,0:T(8,128)(2,1)} %refs_0_.1), channel_id=1, source_target_pairs={{0,8},{4,12},{8,0},{12,4},{16,24},{20,28},{24,16},{28,20},{1,9},{5... | collective-permute-start | bytes 786440 | tf_op jit(solution)/shard_map/ppermute | solution.py:20
  7.5 9.5 %collective-permute-done.11.refs_4_ = bf16[512,256]{1,0:T(8,128)(2,1)S(1)} collective-permute-done((bf16[512,256]{1,0:T(8,128)(2,1)}, bf16[512,256]{1,0:T(8,128)(2,1)S(1)}, u32[]{:S(2)}, u32[]{:S(2)}) %collective-permute-start.11) | collective-permute-done | bytes 262176 | tf_op jit(solution)/shard_map/ppermute | solution.py:20
  17.0 0.8 collective-permute-start.13
  17.8 2.8 %collective-permute-start.3 = (bf16[2,16,256]{2,1,0:T(8,128)(2,1)S(1)}, bf16[2,16,256]{2,1,0:T(8,128)(2,1)S(1)}, u32[]{:S(2)}, u32[]{:S(2)}) collective-permute-start(bf16[2,16,256]{2,1,0:T(8,128)(2,1)S(1)} %get-tuple-element.54), channel_id=1, source_target_pairs={{0,24},{4,28},{8,16},{12,20},{16,8},{20,12},{24,0},{28,4},{1,25},{... | collective-permute-start | bytes 49160 | tf_op jit(solution)/shard_map/ppermute | solution.py:20
  20.6 1.1 collective-permute-start.1
  21.8 0.5 collective-permute-start.2
  22.2 5.4 %collective-permute-done.3.refs_3_ = bf16[2,16,256]{2,1,0:T(8,128)(2,1)S(1)} collective-permute-done((bf16[2,16,256]{2,1,0:T(8,128)(2,1)S(1)}, bf16[2,16,256]{2,1,0:T(8,128)(2,1)S(1)}, u32[]{:S(2)}, u32[]{:S(2)}) %collective-permute-start.3) | collective-permute-done | bytes 16416 | tf_op jit(solution)/shard_map/ppermute | solution.py:20
  27.7 0.9 copy-done.5
  28.6 0.9 copy-done.6
  29.6 0.9 copy-done.7
  30.5 0.9 copy-done.8
  31.9 0.5 collective-permute-start.8
  32.5 0.4 collective-permute-start.10
  33.0 0.4 collective-permute-done.4.crossed_ref
  33.4 1.0 collective-permute-start.5
  34.4 3.4 %collective-permute-done.5.refs_1_ = bf16[16,2048]{1,0:T(8,128)(2,1)S(1)} collective-permute-done((bf16[16,2048]{1,0:T(8,128)(2,1)S(1)}, bf16[16,2048]{1,0:T(8,128)(2,1)S(1)}, u32[]{:S(2)}, u32[]{:S(2)}) %collective-permute-start.5) | collective-permute-done | bytes 65568 | tf_op jit(solution)/shard_map/ppermute | solution.py:20
  37.8 0.8 collective-permute-start.6
  38.6 5.1 %collective-permute-done.6.refs_2_ = bf16[16,2048]{1,0:T(8,128)(2,1)S(1)} collective-permute-done((bf16[16,2048]{1,0:T(8,128)(2,1)S(1)}, bf16[16,2048]{1,0:T(8,128)(2,1)S(1)}, u32[]{:S(2)}, u32[]{:S(2)}) %collective-permute-start.6) | collective-permute-done | bytes 65568 | tf_op jit(solution)/shard_map/ppermute | solution.py:20
  43.6 1.7 %collective-permute-start.7 = (bf16[16,2048]{1,0:T(8,128)(2,1)S(1)}, bf16[16,2048]{1,0:T(8,128)(2,1)S(1)}, u32[]{:S(2)}, u32[]{:S(2)}) collective-permute-start(bf16[16,2048]{1,0:T(8,128)(2,1)S(1)} %get-tuple-element.38), channel_id=1, source_target_pairs={{0,24},{4,28},{8,16},{12,20},{16,8},{20,12},{24,0},{28,4},{1,25},{... | collective-permute-start | bytes 196616 | tf_op jit(solution)/shard_map/ppermute | solution.py:20
  45.3 4.4 %collective-permute-done.7.refs_3_ = bf16[16,2048]{1,0:T(8,128)(2,1)S(1)} collective-permute-done((bf16[16,2048]{1,0:T(8,128)(2,1)S(1)}, bf16[16,2048]{1,0:T(8,128)(2,1)S(1)}, u32[]{:S(2)}, u32[]{:S(2)}) %collective-permute-start.7) | collective-permute-done | bytes 65568 | tf_op jit(solution)/shard_map/ppermute | solution.py:20
  49.7 2.2 %copy-done = f32[16,4,128,128]{3,2,1,0:T(8,128)S(1)} copy-done((f32[16,4,128,128]{3,2,1,0:T(8,128)S(1)}, f32[16,4,128,128]{3,2,1,0:T(8,128)}, u32[]{:S(2)}) %copy-start) | copy-done | bytes 4194328
  51.9 2.5 %shard_map.196 = (bf16[16,512]{1,0:T(8,128)(2,1)S(1)}, f32[3,16,512]{2,1,0:T(8,128)S(1)}) custom-call(f32[16,2048]{1,0:T(8,128)S(1)} %get-tuple-element.35.refs_0_, bf16[16,2048]{1,0:T(8,128)(2,1)S(1)} %collective-permute-done.5.refs_1_, bf16[16,2048]{1,0:T(8,128)(2,1)S(1)} %collective-permute-done.6.refs_2_, ...), custom_call_target="tpu_custom_call" | custom-call | flops 1048576 | bytes 1048576 | tf_op jit(solution)/shard_map/pallas_call | solution.py:461
  54.5 0.6 collective-permute-start.27
  55.1 0.4 shard_map.197.refs_4_
  55.4 2.5 %collective-permute-start.17 = (bf16[16,2048]{1,0:T(8,128)(2,1)S(1)}, bf16[16,2048]{1,0:T(8,128)(2,1)S(1)}, u32[]{:S(2)}, u32[]{:S(2)}) collective-permute-start(bf16[16,2048]{1,0:T(8,128)(2,1)S(1)} %shard_map.197.refs_4_), channel_id=1, source_target_pairs={{0,3},{1,2},{2,1},{3,0},{4,7},{5,6},{6,5},{7,4},{8,11},{9,10},{10,... | collective-permute-start | bytes 196616 | tf_op jit(solution)/shard_map/ppermute | solution.py:20
  57.9 0.5 collective-permute-start.16
  58.4 0.5 collective-permute-start.15
  59.0 1.0 table.1
  59.9 0.7 collective-permute-done.17.refs_7_
  60.7 1.5 %collective-permute-done.16.refs_6_ = bf16[16,2048]{1,0:T(8,128)(2,1)S(1)} collective-permute-done((bf16[16,2048]{1,0:T(8,128)(2,1)S(1)}, bf16[16,2048]{1,0:T(8,128)(2,1)S(1)}, u32[]{:S(2)}, u32[]{:S(2)}) %collective-permute-start.16) | collective-permute-done | bytes 65568 | tf_op jit(solution)/shard_map/ppermute | solution.py:20
  62.2 0.6 collective-permute-done.15.refs_5_
  62.8 1.2 shard_map.198
  64.0 1.7 %collective-permute-start.23 = (bf16[16,2176]{1,0:T(8,128)(2,1)S(1)}, bf16[16,2176]{1,0:T(8,128)(2,1)S(1)}, u32[]{:S(2)}, u32[]{:S(2)}) collective-permute-start(bf16[16,2176]{1,0:T(8,128)(2,1)S(1)} %get-tuple-element.42.refs_0_), channel_id=1, source_target_pairs={{0,24},{4,28},{8,16},{12,20},{16,8},{20,12},{24,0},{28,4},{1,25},{... | collective-permute-start | bytes 208904 | tf_op jit(solution)/shard_map/ppermute | solution.py:20
  65.7 5.0 %collective-permute-done.19.refs_0_ = bf16[16,2176]{1,0:T(8,128)(2,1)S(1)} collective-permute-done((bf16[16,2176]{1,0:T(8,128)(2,1)S(1)}, bf16[16,2176]{1,0:T(8,128)(2,1)S(1)}, u32[]{:S(2)}, u32[]{:S(2)}) %collective-permute-start.19) | collective-permute-done | bytes 69664 | tf_op jit(solution)/shard_map/ppermute | solution.py:20
  70.8 0.7 collective-permute-start.21
  71.5 0.6 collective-permute-start.25
  72.2 4.0 %collective-permute-done.21.refs_0_ = bf16[16,2176]{1,0:T(8,128)(2,1)S(1)} collective-permute-done((bf16[16,2176]{1,0:T(8,128)(2,1)S(1)}, bf16[16,2176]{1,0:T(8,128)(2,1)S(1)}, u32[]{:S(2)}, u32[]{:S(2)}) %collective-permute-start.21) | collective-permute-done | bytes 69664 | tf_op jit(solution)/shard_map/ppermute | solution.py:20
  76.2 1.5 %shard_map.199 = f32[32,1536]{1,0:T(8,128)S(1)} custom-call(bf16[16,2176]{1,0:T(8,128)(2,1)S(1)} %get-tuple-element.42.refs_0_, bf16[16,2176]{1,0:T(8,128)(2,1)S(1)} %collective-permute-done.18.refs_1_, bf16[256,1536]{1,0:T(8,128)(2,1)S(1)} %copy-done.2, bf16[256,1536]{1,0:T(8,128)(2,1)S(1)} %copy-done.3, ...), custom_call_target="tpu_custom_call" | custom-call | flops 1048576 | bytes 1048576 | tf_op jit(solution)/shard_map/pallas_call | solution.py:338
  77.9 0.7 fusion.4
  78.7 1.5 %shard_map.200 = bf16[32,1536]{1,0:T(8,128)(2,1)S(1)} custom-call(bf16[16,2176]{1,0:T(8,128)(2,1)S(1)} %collective-permute-done.19.refs_0_, bf16[16,2176]{1,0:T(8,128)(2,1)S(1)} %collective-permute-done.20.refs_1_, bf16[256,1536]{1,0:T(8,128)(2,1)S(1)} %copy-done.2, bf16[256,1536]{1,0:T(8,128)(2,1)S(1)} %copy-done.3, ...), custom_call_target="tpu_custom_call" | custom-call | flops 1048576 | bytes 1048576 | tf_op jit(solution)/shard_map/pallas_call | solution.py:338
  80.2 1.6 %shard_map.201 = bf16[32,1536]{1,0:T(8,128)(2,1)S(1)} custom-call(bf16[16,2176]{1,0:T(8,128)(2,1)S(1)} %collective-permute-done.21.refs_0_, bf16[16,2176]{1,0:T(8,128)(2,1)S(1)} %collective-permute-done.22.refs_1_, bf16[256,1536]{1,0:T(8,128)(2,1)S(1)} %copy-done.2, bf16[256,1536]{1,0:T(8,128)(2,1)S(1)} %copy-done.3, ...), custom_call_target="tpu_custom_call" | custom-call | flops 1048576 | bytes 1048576 | tf_op jit(solution)/shard_map/pallas_call | solution.py:338
  81.9 2.6 %collective-permute-start.29 = (bf16[32,1536]{1,0:T(8,128)(2,1)S(1)}, bf16[32,1536]{1,0:T(8,128)(2,1)S(1)}, u32[]{:S(2)}, u32[]{:S(2)}) collective-permute-start(bf16[32,1536]{1,0:T(8,128)(2,1)S(1)} %shard_map.201), channel_id=1, source_target_pairs={{0,16},{4,20},{8,24},{12,28},{16,0},{20,4},{24,8},{28,12},{1,17},{... | collective-permute-start | bytes 294920 | tf_op jit(solution)/shard_map/ppermute | solution.py:20
  84.5 1.5 %shard_map.202 = bf16[32,1536]{1,0:T(8,128)(2,1)S(1)} custom-call(bf16[16,2176]{1,0:T(8,128)(2,1)S(1)} %collective-permute-done.23.refs_0_, bf16[16,2176]{1,0:T(8,128)(2,1)S(1)} %collective-permute-done.24.refs_1_, bf16[256,1536]{1,0:T(8,128)(2,1)S(1)} %copy-done.2, bf16[256,1536]{1,0:T(8,128)(2,1)S(1)} %copy-done.3, ...), custom_call_target="tpu_custom_call" | custom-call | flops 1048576 | bytes 1048576 | tf_op jit(solution)/shard_map/pallas_call | solution.py:338
  86.0 1.8 %collective-permute-start.30 = (bf16[32,1536]{1,0:T(8,128)(2,1)S(1)}, bf16[32,1536]{1,0:T(8,128)(2,1)S(1)}, u32[]{:S(2)}, u32[]{:S(2)}) collective-permute-start(bf16[32,1536]{1,0:T(8,128)(2,1)S(1)} %shard_map.202), channel_id=1, source_target_pairs={{0,24},{4,28},{8,16},{12,20},{16,8},{20,12},{24,0},{28,4},{1,25},{... | collective-permute-start | bytes 294920 | tf_op jit(solution)/shard_map/ppermute | solution.py:20
  87.7 0.7 multiply_convert_fusion
  88.7 4.1 %collective-permute-done.29 = bf16[32,1536]{1,0:T(8,128)(2,1)S(1)} collective-permute-done((bf16[32,1536]{1,0:T(8,128)(2,1)S(1)}, bf16[32,1536]{1,0:T(8,128)(2,1)S(1)}, u32[]{:S(2)}, u32[]{:S(2)}) %collective-permute-start.29) | collective-permute-done | bytes 98336 | tf_op jit(solution)/shard_map/ppermute | solution.py:20
  92.8 2.2 %collective-permute-start.38 = (bf16[32,768]{1,0:T(8,128)(2,1)S(1)}, bf16[32,768]{1,0:T(8,128)(2,1)S(1)}, u32[]{:S(2)}, u32[]{:S(2)}) collective-permute-start(bf16[32,768]{1,0:T(8,128)(2,1)S(1)} %fusion.11.refs_4_), channel_id=1, source_target_pairs={{0,24},{4,28},{8,16},{12,20},{16,8},{20,12},{24,0},{28,4},{1,25},{... | collective-permute-start | bytes 147464 | tf_op jit(solution)/shard_map/ppermute | solution.py:20
  95.0 1.5 %collective-permute-start.35 = (bf16[32,768]{1,0:T(8,128)(2,1)S(1)}, bf16[32,768]{1,0:T(8,128)(2,1)S(1)}, u32[]{:S(2)}, u32[]{:S(2)}) collective-permute-start(bf16[32,768]{1,0:T(8,128)(2,1)S(1)} %fusion.11.refs_4_), channel_id=1, source_target_pairs={{0,16},{4,20},{8,24},{12,28},{16,0},{20,4},{24,8},{28,12},{1,17},{... | collective-permute-start | bytes 147464 | tf_op jit(solution)/shard_map/ppermute | solution.py:20
  96.5 0.7 collective-permute-start.32
  97.3 0.7 fusion.6.refs_0_
  98.0 1.0 collective-permute-done.38.refs_4_
  99.4 0.8 collective-permute-done.35.refs_4_
  101.9 2.7 %collective-permute-start.40 = (bf16[16,2048]{1,0:T(8,128)(2,1)S(1)}, bf16[16,2048]{1,0:T(8,128)(2,1)S(1)}, u32[]{:S(2)}, u32[]{:S(2)}) collective-permute-start(bf16[16,2048]{1,0:T(8,128)(2,1)S(1)} %shard_map.210), channel_id=1, source_target_pairs={{0,24},{4,28},{8,16},{12,20},{16,8},{20,12},{24,0},{28,4},{1,25},{... | collective-permute-start | bytes 196616 | tf_op jit(solution)/shard_map/ppermute | solution.py:20
  104.7 1.8 %collective-permute-start.34 = (bf16[16,2048]{1,0:T(8,128)(2,1)S(1)}, bf16[16,2048]{1,0:T(8,128)(2,1)S(1)}, u32[]{:S(2)}, u32[]{:S(2)}) collective-permute-start(bf16[16,2048]{1,0:T(8,128)(2,1)S(1)} %shard_map.206), channel_id=1, source_target_pairs={{0,8},{4,12},{8,0},{12,4},{16,24},{20,28},{24,16},{28,20},{1,9},{5... | collective-permute-start | bytes 196616 | tf_op jit(solution)/shard_map/ppermute | solution.py:20
  106.5 2.3 %collective-permute-done.40 = bf16[16,2048]{1,0:T(8,128)(2,1)S(1)} collective-permute-done((bf16[16,2048]{1,0:T(8,128)(2,1)S(1)}, bf16[16,2048]{1,0:T(8,128)(2,1)S(1)}, u32[]{:S(2)}, u32[]{:S(2)}) %collective-permute-start.40) | collective-permute-done | bytes 65568 | tf_op jit(solution)/shard_map/ppermute | solution.py:20
  108.8 2.2 %collective-permute-done.37 = bf16[16,2048]{1,0:T(8,128)(2,1)S(1)} collective-permute-done((bf16[16,2048]{1,0:T(8,128)(2,1)S(1)}, bf16[16,2048]{1,0:T(8,128)(2,1)S(1)}, u32[]{:S(2)}, u32[]{:S(2)}) %collective-permute-start.37) | collective-permute-done | bytes 65568 | tf_op jit(solution)/shard_map/ppermute | solution.py:20
  111.1 1.6 %collective-permute-start.43 = (bf16[16,2048]{1,0:T(8,128)(2,1)S(1)}, bf16[16,2048]{1,0:T(8,128)(2,1)S(1)}, u32[]{:S(2)}, u32[]{:S(2)}) collective-permute-start(bf16[16,2048]{1,0:T(8,128)(2,1)S(1)} %add_convert_fusion.refs_2_), channel_id=1, source_target_pairs={{0,3},{1,2},{2,1},{3,0},{4,7},{5,6},{6,5},{7,4},{8,11},{9,10},{10,... | collective-permute-start | bytes 196616 | tf_op jit(solution)/shard_map/ppermute | solution.py:20
  112.6 1.0 collective-permute-start.42
  113.6 1.0 collective-permute-start.41
  114.6 3.8 %write_state.2.refs_0_ = f32[16,4,128,128]{3,2,1,0:T(8,128)} custom-call(f32[3,16,512]{2,1,0:T(8,128)S(1)} %get-tuple-element.51.gates_ref, f32[16,4,128,128]{3,2,1,0:T(8,128)} %state_ref.3), custom_call_target="tpu_custom_call" | custom-call | flops 4194304 | bytes 8388608 | tf_op jit(solution)/shard_map/write_state/pallas_call | solution.py:486
  118.4 2.6 %write_state.3 = f32[16,4,128,128]{3,2,1,0:T(8,128)} custom-call(f32[3,16,512]{2,1,0:T(8,128)S(1)} %get-tuple-element.51.gates_ref, f32[16,4,128,128]{3,2,1,0:T(8,128)S(1)} %copy-done.1, f32[16,4,128,128]{3,2,1,0:T(8,128)} %write_state.2.refs_0_), custom_call_target="tpu_custom_call", output_to_operand_aliasing={{}: (2, {})} | custom-call | flops 4194304 | bytes 8388608 | tf_op jit(solution)/shard_map/write_state/pallas_call | solution.py:486
  121.0 0.7 shard_map.211
  (90 shorter events, 3.5 us)
Async XLA Ops:
  0.6 53.8 %copy-start.3 = (bf16[256,1536]{1,0:T(8,128)(2,1)S(1)}, bf16[256,1536]{1,0:T(8,128)(2,1)}, u32[]{:S(2)}) copy-start(bf16[256,1536]{1,0:T(8,128)(2,1)} %refs_3_.7) | copy-start | bytes 2359300
  0.6 16.4 %collective-permute-start.11 = (bf16[512,256]{1,0:T(8,128)(2,1)}, bf16[512,256]{1,0:T(8,128)(2,1)S(1)}, u32[]{:S(2)}, u32[]{:S(2)}) collective-permute-start(bf16[512,256]{1,0:T(8,128)(2,1)} %refs_0_.1), channel_id=1, source_target_pairs={{0,16},{4,20},{8,24},{12,28},{16,0},{20,4},{24,8},{28,12},{1,17},{... | collective-permute-start | bytes 786440 | tf_op jit(solution)/shard_map/ppermute | solution.py:20
  5.8 12.0 %collective-permute-start = (bf16[4,16,256]{2,1,0:T(8,128)(2,1)S(1)}, bf16[4,16,256]{2,1,0:T(8,128)(2,1)S(1)}, u32[]{:S(2)}, u32[]{:S(2)}) collective-permute-start(bf16[4,16,256]{2,1,0:T(8,128)(2,1)S(1)} %get-tuple-element.32), channel_id=1, source_target_pairs={{0,4},{4,0},{8,12},{12,8},{16,20},{20,16},{24,28},{28,24},{1,5},{5... | collective-permute-start | bytes 98312 | tf_op jit(solution)/shard_map/ppermute | solution.py:20
  5.9 26.6 %collective-permute-start.9 = (bf16[512,256]{1,0:T(8,128)(2,1)}, bf16[512,256]{1,0:T(8,128)(2,1)S(1)}, u32[]{:S(2)}, u32[]{:S(2)}) collective-permute-start(bf16[512,256]{1,0:T(8,128)(2,1)} %refs_0_.1), channel_id=1, source_target_pairs={{0,8},{4,12},{8,0},{12,4},{16,24},{20,28},{24,16},{28,20},{1,9},{5... | collective-permute-start | bytes 786440 | tf_op jit(solution)/shard_map/ppermute | solution.py:20
  17.0 15.9 %collective-permute-start.13 = (bf16[512,256]{1,0:T(8,128)(2,1)S(1)}, bf16[512,256]{1,0:T(8,128)(2,1)S(1)}, u32[]{:S(2)}, u32[]{:S(2)}) collective-permute-start(bf16[512,256]{1,0:T(8,128)(2,1)S(1)} %collective-permute-done.11.refs_4_), channel_id=1, source_target_pairs={{0,8},{4,12},{8,0},{12,4},{16,24},{20,28},{24,16},{28,20},{1,9},{5... | collective-permute-start | bytes 786440 | tf_op jit(solution)/shard_map/ppermute | solution.py:20
  17.8 9.9 %collective-permute-start.3 = (bf16[2,16,256]{2,1,0:T(8,128)(2,1)S(1)}, bf16[2,16,256]{2,1,0:T(8,128)(2,1)S(1)}, u32[]{:S(2)}, u32[]{:S(2)}) collective-permute-start(bf16[2,16,256]{2,1,0:T(8,128)(2,1)S(1)} %get-tuple-element.54), channel_id=1, source_target_pairs={{0,24},{4,28},{8,16},{12,20},{16,8},{20,12},{24,0},{28,4},{1,25},{... | collective-permute-start | bytes 49160 | tf_op jit(solution)/shard_map/ppermute | solution.py:20
  20.6 7.1 %collective-permute-start.1 = (bf16[2,16,256]{2,1,0:T(8,128)(2,1)S(1)}, bf16[2,16,256]{2,1,0:T(8,128)(2,1)S(1)}, u32[]{:S(2)}, u32[]{:S(2)}) collective-permute-start(bf16[2,16,256]{2,1,0:T(8,128)(2,1)S(1)} %get-tuple-element.56), channel_id=1, source_target_pairs={{0,8},{4,12},{8,0},{12,4},{16,24},{20,28},{24,16},{28,20},{1,9},{5... | collective-permute-start | bytes 49160 | tf_op jit(solution)/shard_map/ppermute | solution.py:20
  21.8 5.9 %collective-permute-start.2 = (bf16[2,16,256]{2,1,0:T(8,128)(2,1)S(1)}, bf16[2,16,256]{2,1,0:T(8,128)(2,1)S(1)}, u32[]{:S(2)}, u32[]{:S(2)}) collective-permute-start(bf16[2,16,256]{2,1,0:T(8,128)(2,1)S(1)} %get-tuple-element.57), channel_id=1, source_target_pairs={{0,16},{4,20},{8,24},{12,28},{16,0},{20,4},{24,8},{28,12},{1,17},{... | collective-permute-start | bytes 49160 | tf_op jit(solution)/shard_map/ppermute | solution.py:20
  27.7 1.0 copy-start.5
  28.6 0.9 copy-start.6
  29.6 0.9 copy-start.7
  30.5 0.9 copy-start.8
  31.5 23.6 %copy-start.9 = (bf16[512,256]{1,0:T(8,128)(2,1)S(1)}, bf16[512,256]{1,0:T(8,128)(2,1)}, u32[]{:S(2)}) copy-start(bf16[512,256]{1,0:T(8,128)(2,1)} %refs_0_.1) | copy-start | bytes 786436
  31.8 1.6 %collective-permute-start.4 = (bf16[4,16,2048]{2,1,0:T(8,128)(2,1)S(1)}, bf16[4,16,2048]{2,1,0:T(8,128)(2,1)S(1)}, u32[]{:S(2)}, u32[]{:S(2)}) collective-permute-start(bf16[4,16,2048]{2,1,0:T(8,128)(2,1)S(1)} %get-tuple-element.34), channel_id=1, source_target_pairs={{0,4},{4,0},{8,12},{12,8},{16,20},{20,16},{24,28},{28,24},{1,5},{5... | collective-permute-start | bytes 786440 | tf_op jit(solution)/shard_map/ppermute | solution.py:20
  31.9 22.6 %collective-permute-start.8 = (bf16[512,256]{1,0:T(8,128)(2,1)}, bf16[512,256]{1,0:T(8,128)(2,1)S(1)}, u32[]{:S(2)}, u32[]{:S(2)}) collective-permute-start(bf16[512,256]{1,0:T(8,128)(2,1)} %refs_0_.1), channel_id=1, source_target_pairs={{0,4},{4,0},{8,12},{12,8},{16,20},{20,16},{24,28},{28,24},{1,5},{5... | collective-permute-start | bytes 786440 | tf_op jit(solution)/shard_map/ppermute | solution.py:20
  32.4 22.7 %collective-permute-start.12 = (bf16[512,256]{1,0:T(8,128)(2,1)S(1)}, bf16[512,256]{1,0:T(8,128)(2,1)S(1)}, u32[]{:S(2)}, u32[]{:S(2)}) collective-permute-start(bf16[512,256]{1,0:T(8,128)(2,1)S(1)} %collective-permute-done.11.refs_4_), channel_id=1, source_target_pairs={{0,4},{4,0},{8,12},{12,8},{16,20},{20,16},{24,28},{28,24},{1,5},{5... | collective-permute-start | bytes 786440 | tf_op jit(solution)/shard_map/ppermute | solution.py:20
  32.5 22.6 %collective-permute-start.10 = (bf16[512,256]{1,0:T(8,128)(2,1)S(1)}, bf16[512,256]{1,0:T(8,128)(2,1)S(1)}, u32[]{:S(2)}, u32[]{:S(2)}) collective-permute-start(bf16[512,256]{1,0:T(8,128)(2,1)S(1)} %collective-permute-done.9.refs_2_), channel_id=1, source_target_pairs={{0,4},{4,0},{8,12},{12,8},{16,20},{20,16},{24,28},{28,24},{1,5},{5... | collective-permute-start | bytes 786440 | tf_op jit(solution)/shard_map/ppermute | solution.py:20
  32.9 22.2 %collective-permute-start.14 = (bf16[512,256]{1,0:T(8,128)(2,1)S(1)}, bf16[512,256]{1,0:T(8,128)(2,1)S(1)}, u32[]{:S(2)}, u32[]{:S(2)}) collective-permute-start(bf16[512,256]{1,0:T(8,128)(2,1)S(1)} %collective-permute-done.13.refs_6_), channel_id=1, source_target_pairs={{0,4},{4,0},{8,12},{12,8},{16,20},{20,16},{24,28},{28,24},{1,5},{5... | collective-permute-start | bytes 786440 | tf_op jit(solution)/shard_map/ppermute | solution.py:20
  33.4 4.3 %collective-permute-start.5 = (bf16[16,2048]{1,0:T(8,128)(2,1)S(1)}, bf16[16,2048]{1,0:T(8,128)(2,1)S(1)}, u32[]{:S(2)}, u32[]{:S(2)}) collective-permute-start(bf16[16,2048]{1,0:T(8,128)(2,1)S(1)} %get-tuple-element.36), channel_id=1, source_target_pairs={{0,8},{4,12},{8,0},{12,4},{16,24},{20,28},{24,16},{28,20},{1,9},{5... | collective-permute-start | bytes 196616 | tf_op jit(solution)/shard_map/ppermute | solution.py:20
  37.8 5.9 %collective-permute-start.6 = (bf16[16,2048]{1,0:T(8,128)(2,1)S(1)}, bf16[16,2048]{1,0:T(8,128)(2,1)S(1)}, u32[]{:S(2)}, u32[]{:S(2)}) collective-permute-start(bf16[16,2048]{1,0:T(8,128)(2,1)S(1)} %get-tuple-element.37), channel_id=1, source_target_pairs={{0,16},{4,20},{8,24},{12,28},{16,0},{20,4},{24,8},{28,12},{1,17},{... | collective-permute-start | bytes 196616 | tf_op jit(solution)/shard_map/ppermute | solution.py:20
  43.6 6.1 %collective-permute-start.7 = (bf16[16,2048]{1,0:T(8,128)(2,1)S(1)}, bf16[16,2048]{1,0:T(8,128)(2,1)S(1)}, u32[]{:S(2)}, u32[]{:S(2)}) collective-permute-start(bf16[16,2048]{1,0:T(8,128)(2,1)S(1)} %get-tuple-element.38), channel_id=1, source_target_pairs={{0,24},{4,28},{8,16},{12,20},{16,8},{20,12},{24,0},{28,4},{1,25},{... | collective-permute-start | bytes 196616 | tf_op jit(solution)/shard_map/ppermute | solution.py:20
  49.7 21.8 %collective-permute-start.26 = (bf16[256,1536]{1,0:T(8,128)(2,1)}, bf16[256,1536]{1,0:T(8,128)(2,1)S(1)}, u32[]{:S(2)}, u32[]{:S(2)}) collective-permute-start(bf16[256,1536]{1,0:T(8,128)(2,1)} %refs_2_.11), channel_id=1, source_target_pairs={{0,4},{4,0},{8,12},{12,8},{16,20},{20,16},{24,28},{28,24},{1,5},{5... | collective-permute-start | bytes 2359304 | tf_op jit(solution)/shard_map/ppermute | solution.py:20
  49.7 2.2 %copy-start = (f32[16,4,128,128]{3,2,1,0:T(8,128)S(1)}, f32[16,4,128,128]{3,2,1,0:T(8,128)}, u32[]{:S(2)}) copy-start(f32[16,4,128,128]{3,2,1,0:T(8,128)} %state_ref.3) | copy-start | bytes 12582916
  54.5 21.7 %collective-permute-start.27 = (bf16[256,1536]{1,0:T(8,128)(2,1)S(1)}, bf16[256,1536]{1,0:T(8,128)(2,1)}, u32[]{:S(2)}, u32[]{:S(2)}) collective-permute-start(bf16[256,1536]{1,0:T(8,128)(2,1)S(1)} %copy-done.3), channel_id=1, source_target_pairs={{0,4},{4,0},{8,12},{12,8},{16,20},{20,16},{24,28},{28,24},{1,5},{5... | collective-permute-start | bytes 2359304 | tf_op jit(solution)/shard_map/ppermute | solution.py:20
  55.4 5.2 %collective-permute-start.17 = (bf16[16,2048]{1,0:T(8,128)(2,1)S(1)}, bf16[16,2048]{1,0:T(8,128)(2,1)S(1)}, u32[]{:S(2)}, u32[]{:S(2)}) collective-permute-start(bf16[16,2048]{1,0:T(8,128)(2,1)S(1)} %shard_map.197.refs_4_), channel_id=1, source_target_pairs={{0,3},{1,2},{2,1},{3,0},{4,7},{5,6},{6,5},{7,4},{8,11},{9,10},{10,... | collective-permute-start | bytes 196616 | tf_op jit(solution)/shard_map/ppermute | solution.py:20
  57.9 4.3 %collective-permute-start.16 = (bf16[16,2048]{1,0:T(8,128)(2,1)S(1)}, bf16[16,2048]{1,0:T(8,128)(2,1)S(1)}, u32[]{:S(2)}, u32[]{:S(2)}) collective-permute-start(bf16[16,2048]{1,0:T(8,128)(2,1)S(1)} %shard_map.197.refs_4_), channel_id=1, source_target_pairs={{0,2},{1,3},{2,0},{3,1},{4,6},{5,7},{6,4},{7,5},{8,10},{9,11},{10,... | collective-permute-start | bytes 196616 | tf_op jit(solution)/shard_map/ppermute | solution.py:20
  58.4 4.4 %collective-permute-start.15 = (bf16[16,2048]{1,0:T(8,128)(2,1)S(1)}, bf16[16,2048]{1,0:T(8,128)(2,1)}, u32[]{:S(2)}, u32[]{:S(2)}) collective-permute-start(bf16[16,2048]{1,0:T(8,128)(2,1)S(1)} %shard_map.197.refs_4_), channel_id=1, source_target_pairs={{0,1},{1,0},{2,3},{3,2},{4,5},{5,4},{6,7},{7,6},{8,9},{9,8},{10,11... | collective-permute-start | bytes 196616 | tf_op jit(solution)/shard_map/ppermute | solution.py:20
  58.9 12.6 %copy-start.4 = (bf16[1536,256]{1,0:T(8,128)(2,1)S(1)}, bf16[1536,256]{1,0:T(8,128)(2,1)}, u32[]{:S(2)}) copy-start(bf16[1536,256]{1,0:T(8,128)(2,1)} %refs_2_.15) | copy-start | bytes 2359300
  59.0 17.2 %copy-start.2 = (bf16[256,1536]{1,0:T(8,128)(2,1)S(1)}, bf16[256,1536]{1,0:T(8,128)(2,1)}, u32[]{:S(2)}) copy-start(bf16[256,1536]{1,0:T(8,128)(2,1)} %refs_2_.11) | copy-start | bytes 2359300
  59.9 18.0 %copy-start.11 = (bf16[1,2048,896]{2,1,0:T(8,128)(2,1)S(1)}, bf16[1,2048,896]{2,1,0:T(8,128)(2,1)}, u32[]{:S(2)}) copy-start(bf16[1,2048,896]{2,1,0:T(8,128)(2,1)} %param.31) | copy-start | bytes 11010052
  64.0 8.1 %collective-permute-start.23 = (bf16[16,2176]{1,0:T(8,128)(2,1)S(1)}, bf16[16,2176]{1,0:T(8,128)(2,1)S(1)}, u32[]{:S(2)}, u32[]{:S(2)}) collective-permute-start(bf16[16,2176]{1,0:T(8,128)(2,1)S(1)} %get-tuple-element.42.refs_0_), channel_id=1, source_target_pairs={{0,24},{4,28},{8,16},{12,20},{16,8},{20,12},{24,0},{28,4},{1,25},{... | collective-permute-start | bytes 208904 | tf_op jit(solution)/shard_map/ppermute | solution.py:20
  65.7 5.1 %collective-permute-start.19 = (bf16[16,2176]{1,0:T(8,128)(2,1)S(1)}, bf16[16,2176]{1,0:T(8,128)(2,1)S(1)}, u32[]{:S(2)}, u32[]{:S(2)}) collective-permute-start(bf16[16,2176]{1,0:T(8,128)(2,1)S(1)} %get-tuple-element.42.refs_0_), channel_id=1, source_target_pairs={{0,8},{4,12},{8,0},{12,4},{16,24},{20,28},{24,16},{28,20},{1,9},{5... | collective-permute-start | bytes 208904 | tf_op jit(solution)/shard_map/ppermute | solution.py:20
  65.7 5.7 %collective-permute-start.18 = (bf16[16,2176]{1,0:T(8,128)(2,1)S(1)}, bf16[16,2176]{1,0:T(8,128)(2,1)S(1)}, u32[]{:S(2)}, u32[]{:S(2)}) collective-permute-start(bf16[16,2176]{1,0:T(8,128)(2,1)S(1)} %get-tuple-element.42.refs_0_), channel_id=1, source_target_pairs={{0,4},{4,0},{8,12},{12,8},{16,20},{20,16},{24,28},{28,24},{1,5},{5... | collective-permute-start | bytes 208904 | tf_op jit(solution)/shard_map/ppermute | solution.py:20
  70.8 5.4 %collective-permute-start.21 = (bf16[16,2176]{1,0:T(8,128)(2,1)S(1)}, bf16[16,2176]{1,0:T(8,128)(2,1)S(1)}, u32[]{:S(2)}, u32[]{:S(2)}) collective-permute-start(bf16[16,2176]{1,0:T(8,128)(2,1)S(1)} %get-tuple-element.42.refs_0_), channel_id=1, source_target_pairs={{0,16},{4,20},{8,24},{12,28},{16,0},{20,4},{24,8},{28,12},{1,17},{... | collective-permute-start | bytes 208904 | tf_op jit(solution)/shard_map/ppermute | solution.py:20
  71.5 6.2 %collective-permute-start.20 = (bf16[16,2176]{1,0:T(8,128)(2,1)S(1)}, bf16[16,2176]{1,0:T(8,128)(2,1)S(1)}, u32[]{:S(2)}, u32[]{:S(2)}) collective-permute-start(bf16[16,2176]{1,0:T(8,128)(2,1)S(1)} %collective-permute-done.19.refs_0_), channel_id=1, source_target_pairs={{0,4},{4,0},{8,12},{12,8},{16,20},{20,16},{24,28},{28,24},{1,5},{5... | collective-permute-start | bytes 208904 | tf_op jit(solution)/shard_map/ppermute | solution.py:20
  71.5 26.5 %collective-permute-start.25 = (bf16[1536,256]{1,0:T(8,128)(2,1)S(1)}, bf16[1536,256]{1,0:T(8,128)(2,1)S(1)}, u32[]{:S(2)}, u32[]{:S(2)}) collective-permute-start(bf16[1536,256]{1,0:T(8,128)(2,1)S(1)} %copy-done.4), channel_id=1, source_target_pairs={{0,4},{4,0},{8,12},{12,8},{16,20},{20,16},{24,28},{28,24},{1,5},{5... | collective-permute-start | bytes 2359304 | tf_op jit(solution)/shard_map/ppermute | solution.py:20
  72.1 5.7 %collective-permute-start.24 = (bf16[16,2176]{1,0:T(8,128)(2,1)S(1)}, bf16[16,2176]{1,0:T(8,128)(2,1)S(1)}, u32[]{:S(2)}, u32[]{:S(2)}) collective-permute-start(bf16[16,2176]{1,0:T(8,128)(2,1)S(1)} %collective-permute-done.23.refs_0_), channel_id=1, source_target_pairs={{0,4},{4,0},{8,12},{12,8},{16,20},{20,16},{24,28},{28,24},{1,5},{5... | collective-permute-start | bytes 208904 | tf_op jit(solution)/shard_map/ppermute | solution.py:20
  76.2 1.6 %collective-permute-start.22 = (bf16[16,2176]{1,0:T(8,128)(2,1)S(1)}, bf16[16,2176]{1,0:T(8,128)(2,1)S(1)}, u32[]{:S(2)}, u32[]{:S(2)}) collective-permute-start(bf16[16,2176]{1,0:T(8,128)(2,1)S(1)} %collective-permute-done.21.refs_0_), channel_id=1, source_target_pairs={{0,4},{4,0},{8,12},{12,8},{16,20},{20,16},{24,28},{28,24},{1,5},{5... | collective-permute-start | bytes 208904 | tf_op jit(solution)/shard_map/ppermute | solution.py:20
  80.1 7.6 %copy-start.12 = (bf16[1,2048,896]{2,1,0:T(8,128)(2,1)S(1)}, bf16[1,2048,896]{2,1,0:T(8,128)(2,1)}, u32[]{:S(2)}) copy-start(bf16[1,2048,896]{2,1,0:T(8,128)(2,1)} %param.32) | copy-start | bytes 11010052
  80.2 8.5 %collective-permute-start.28 = (bf16[32,1536]{1,0:T(8,128)(2,1)S(1)}, bf16[32,1536]{1,0:T(8,128)(2,1)S(1)}, u32[]{:S(2)}, u32[]{:S(2)}) collective-permute-start(bf16[32,1536]{1,0:T(8,128)(2,1)S(1)} %shard_map.200), channel_id=1, source_target_pairs={{0,8},{4,12},{8,0},{12,4},{16,24},{20,28},{24,16},{28,20},{1,9},{5... | collective-permute-start | bytes 294920 | tf_op jit(solution)/shard_map/ppermute | solution.py:20
  81.9 10.8 %collective-permute-start.29 = (bf16[32,1536]{1,0:T(8,128)(2,1)S(1)}, bf16[32,1536]{1,0:T(8,128)(2,1)S(1)}, u32[]{:S(2)}, u32[]{:S(2)}) collective-permute-start(bf16[32,1536]{1,0:T(8,128)(2,1)S(1)} %shard_map.201), channel_id=1, source_target_pairs={{0,16},{4,20},{8,24},{12,28},{16,0},{20,4},{24,8},{28,12},{1,17},{... | collective-permute-start | bytes 294920 | tf_op jit(solution)/shard_map/ppermute | solution.py:20
  86.0 11.3 %copy-start.10 = (bf16[1,896,2048]{2,1,0:T(8,128)(2,1)S(1)}, bf16[1,896,2048]{2,1,0:T(8,128)(2,1)}, u32[]{:S(2)}) copy-start(bf16[1,896,2048]{2,1,0:T(8,128)(2,1)} %param.33) | copy-start | bytes 11010052
  86.0 6.8 %collective-permute-start.30 = (bf16[32,1536]{1,0:T(8,128)(2,1)S(1)}, bf16[32,1536]{1,0:T(8,128)(2,1)S(1)}, u32[]{:S(2)}, u32[]{:S(2)}) collective-permute-start(bf16[32,1536]{1,0:T(8,128)(2,1)S(1)} %shard_map.202), channel_id=1, source_target_pairs={{0,24},{4,28},{8,16},{12,20},{16,8},{20,12},{24,0},{28,4},{1,25},{... | collective-permute-start | bytes 294920 | tf_op jit(solution)/shard_map/ppermute | solution.py:20
  92.8 6.2 %collective-permute-start.38 = (bf16[32,768]{1,0:T(8,128)(2,1)S(1)}, bf16[32,768]{1,0:T(8,128)(2,1)S(1)}, u32[]{:S(2)}, u32[]{:S(2)}) collective-permute-start(bf16[32,768]{1,0:T(8,128)(2,1)S(1)} %fusion.11.refs_4_), channel_id=1, source_target_pairs={{0,24},{4,28},{8,16},{12,20},{16,8},{20,12},{24,0},{28,4},{1,25},{... | collective-permute-start | bytes 147464 | tf_op jit(solution)/shard_map/ppermute | solution.py:20
  95.0 5.2 %collective-permute-start.35 = (bf16[32,768]{1,0:T(8,128)(2,1)S(1)}, bf16[32,768]{1,0:T(8,128)(2,1)S(1)}, u32[]{:S(2)}, u32[]{:S(2)}) collective-permute-start(bf16[32,768]{1,0:T(8,128)(2,1)S(1)} %fusion.11.refs_4_), channel_id=1, source_target_pairs={{0,16},{4,20},{8,24},{12,28},{16,0},{20,4},{24,8},{28,12},{1,17},{... | collective-permute-start | bytes 147464 | tf_op jit(solution)/shard_map/ppermute | solution.py:20
  96.5 4.2 %collective-permute-start.32 = (bf16[32,768]{1,0:T(8,128)(2,1)S(1)}, bf16[32,768]{1,0:T(8,128)(2,1)S(1)}, u32[]{:S(2)}, u32[]{:S(2)}) collective-permute-start(bf16[32,768]{1,0:T(8,128)(2,1)S(1)} %fusion.11.refs_4_), channel_id=1, source_target_pairs={{0,8},{4,12},{8,0},{12,4},{16,24},{20,28},{24,16},{28,20},{1,9},{5... | collective-permute-start | bytes 147464 | tf_op jit(solution)/shard_map/ppermute | solution.py:20
  99.3 2.6 %collective-permute-start.39 = (bf16[16,2048]{1,0:T(8,128)(2,1)S(1)}, bf16[16,2048]{1,0:T(8,128)(2,1)S(1)}, u32[]{:S(2)}, u32[]{:S(2)}) collective-permute-start(bf16[16,2048]{1,0:T(8,128)(2,1)S(1)} %get-tuple-element.50), channel_id=1, source_target_pairs={{0,4},{4,0},{8,12},{12,8},{16,20},{20,16},{24,28},{28,24},{1,5},{5... | collective-permute-start | bytes 196616 | tf_op jit(solution)/shard_map/ppermute | solution.py:20
  100.4 4.1 %collective-permute-start.36 = (bf16[16,2048]{1,0:T(8,128)(2,1)S(1)}, bf16[16,2048]{1,0:T(8,128)(2,1)S(1)}, u32[]{:S(2)}, u32[]{:S(2)}) collective-permute-start(bf16[16,2048]{1,0:T(8,128)(2,1)S(1)} %get-tuple-element.48), channel_id=1, source_target_pairs={{0,4},{4,0},{8,12},{12,8},{16,20},{20,16},{24,28},{28,24},{1,5},{5... | collective-permute-start | bytes 196616 | tf_op jit(solution)/shard_map/ppermute | solution.py:20
  101.0 3.7 %collective-permute-start.33 = (bf16[16,2048]{1,0:T(8,128)(2,1)S(1)}, bf16[16,2048]{1,0:T(8,128)(2,1)S(1)}, u32[]{:S(2)}, u32[]{:S(2)}) collective-permute-start(bf16[16,2048]{1,0:T(8,128)(2,1)S(1)} %get-tuple-element.46), channel_id=1, source_target_pairs={{0,4},{4,0},{8,12},{12,8},{16,20},{20,16},{24,28},{28,24},{1,5},{5... | collective-permute-start | bytes 196616 | tf_op jit(solution)/shard_map/ppermute | solution.py:20
  101.6 4.9 %collective-permute-start.31 = (bf16[16,2048]{1,0:T(8,128)(2,1)S(1)}, bf16[16,2048]{1,0:T(8,128)(2,1)S(1)}, u32[]{:S(2)}, u32[]{:S(2)}) collective-permute-start(bf16[16,2048]{1,0:T(8,128)(2,1)S(1)} %get-tuple-element.44), channel_id=1, source_target_pairs={{0,4},{4,0},{8,12},{12,8},{16,20},{20,16},{24,28},{28,24},{1,5},{5... | collective-permute-start | bytes 196616 | tf_op jit(solution)/shard_map/ppermute | solution.py:20
  101.9 6.9 %collective-permute-start.40 = (bf16[16,2048]{1,0:T(8,128)(2,1)S(1)}, bf16[16,2048]{1,0:T(8,128)(2,1)S(1)}, u32[]{:S(2)}, u32[]{:S(2)}) collective-permute-start(bf16[16,2048]{1,0:T(8,128)(2,1)S(1)} %shard_map.210), channel_id=1, source_target_pairs={{0,24},{4,28},{8,16},{12,20},{16,8},{20,12},{24,0},{28,4},{1,25},{... | collective-permute-start | bytes 196616 | tf_op jit(solution)/shard_map/ppermute | solution.py:20
  104.6 6.5 %collective-permute-start.37 = (bf16[16,2048]{1,0:T(8,128)(2,1)S(1)}, bf16[16,2048]{1,0:T(8,128)(2,1)S(1)}, u32[]{:S(2)}, u32[]{:S(2)}) collective-permute-start(bf16[16,2048]{1,0:T(8,128)(2,1)S(1)} %shard_map.208), channel_id=1, source_target_pairs={{0,16},{4,20},{8,24},{12,28},{16,0},{20,4},{24,8},{28,12},{1,17},{... | collective-permute-start | bytes 196616 | tf_op jit(solution)/shard_map/ppermute | solution.py:20
  104.7 6.3 %collective-permute-start.34 = (bf16[16,2048]{1,0:T(8,128)(2,1)S(1)}, bf16[16,2048]{1,0:T(8,128)(2,1)S(1)}, u32[]{:S(2)}, u32[]{:S(2)}) collective-permute-start(bf16[16,2048]{1,0:T(8,128)(2,1)S(1)} %shard_map.206), channel_id=1, source_target_pairs={{0,8},{4,12},{8,0},{12,4},{16,24},{20,28},{24,16},{28,20},{1,9},{5... | collective-permute-start | bytes 196616 | tf_op jit(solution)/shard_map/ppermute | solution.py:20
  111.1 9.9 %collective-permute-start.43 = (bf16[16,2048]{1,0:T(8,128)(2,1)S(1)}, bf16[16,2048]{1,0:T(8,128)(2,1)S(1)}, u32[]{:S(2)}, u32[]{:S(2)}) collective-permute-start(bf16[16,2048]{1,0:T(8,128)(2,1)S(1)} %add_convert_fusion.refs_2_), channel_id=1, source_target_pairs={{0,3},{1,2},{2,1},{3,0},{4,7},{5,6},{6,5},{7,4},{8,11},{9,10},{10,... | collective-permute-start | bytes 196616 | tf_op jit(solution)/shard_map/ppermute | solution.py:20
  112.6 8.4 %collective-permute-start.42 = (bf16[16,2048]{1,0:T(8,128)(2,1)S(1)}, bf16[16,2048]{1,0:T(8,128)(2,1)S(1)}, u32[]{:S(2)}, u32[]{:S(2)}) collective-permute-start(bf16[16,2048]{1,0:T(8,128)(2,1)S(1)} %add_convert_fusion.refs_2_), channel_id=1, source_target_pairs={{0,2},{1,3},{2,0},{3,1},{4,6},{5,7},{6,4},{7,5},{8,10},{9,11},{10,... | collective-permute-start | bytes 196616 | tf_op jit(solution)/shard_map/ppermute | solution.py:20
  113.6 7.4 %collective-permute-start.41 = (bf16[16,2048]{1,0:T(8,128)(2,1)S(1)}, bf16[16,2048]{1,0:T(8,128)(2,1)S(1)}, u32[]{:S(2)}, u32[]{:S(2)}) collective-permute-start(bf16[16,2048]{1,0:T(8,128)(2,1)S(1)} %add_convert_fusion.refs_2_), channel_id=1, source_target_pairs={{0,1},{1,0},{2,3},{3,2},{4,5},{5,4},{6,7},{7,6},{8,9},{9,8},{10,11... | collective-permute-start | bytes 196616 | tf_op jit(solution)/shard_map/ppermute | solution.py:20
  114.6 3.8 %copy-start.1 = (f32[16,4,128,128]{3,2,1,0:T(8,128)S(1)}, f32[16,4,128,128]{3,2,1,0:T(8,128)}, u32[]{:S(2)}) copy-start(f32[16,4,128,128]{3,2,1,0:T(8,128)} %state_ref.3) | copy-start | bytes 12582916
